TPU v7x, 32 devices: a whole 2x2x4 slice. The times are simulated.
32 devices in a mesh: ep: 4 (over y, x), tp: 8 (over z, core).
Axes of the slice: x: 2, y: 2, z: 4, core: 2. Of those that a mesh axis runs over, the one named last changes fastest.
Arguments:
- hidden: bfloat16 [160, 4096], P('ep', 'tp'), may hold values from -6 to 6
- positions: int32 [160], P('ep'), may hold values from 0 to 16383
- ret_state: float32 [160, 16, 128, 128], P('ep', 'tp'), may hold values from -1.5 to 1.5
- query_weight: bfloat16 [4096, 2048], P('ep', 'tp'), may hold values from -0.09375 to 0.09375
- key_weight: bfloat16 [4096, 2048], P('ep', 'tp'), may hold values from -0.09375 to 0.09375
- value_weight: bfloat16 [4096, 2048], P('ep', 'tp'), may hold values from -0.09375 to 0.09375
- gate_weight: bfloat16 [4096, 2048], P('ep', 'tp'), may hold values from -0.09375 to 0.09375
- head_gain: float32 [2048], P('tp'), may hold values from 0.1 to 1.9
- out_weight: bfloat16 [2048, 4096], P(None, 'tp'), may hold values from -0.125 to 0.125
- mix_gain: float32 [4096], replicated, may hold values from 0.1 to 1.9
- ffn_gain: float32 [4096], replicated, may hold values from 0.1 to 1.9
- expert_gate: bfloat16 [8, 4096, 2048], P('ep', None, 'tp'), may hold values from -0.09375 to 0.09375
- expert_up: bfloat16 [8, 4096, 2048], P('ep', None, 'tp'), may hold values from -0.09375 to 0.09375
- expert_down: bfloat16 [8, 2048, 4096], P('ep', None, 'tp'), may hold values from -0.125 to 0.125
- route_ids: int32 [160, 2], P('ep'), may hold values from 0 to 7, as said below
- route_weight: float32 [160, 2], P('ep'), may hold values from 0.25 to 1
Outputs:
- updated: bfloat16 [160, 4096], P('ep', 'tp')
- next_state: float32 [160, 16, 128, 128], P('ep', 'tp')
Inputs may be any that keep to these rules, and one draw needn't show every extreme that they name: `route_ids`: each row names two different experts of one group, the group being the numbers g * 2 to g * 2 + 1; in the rows of one device (aligned blocks of 40 rows) no expert is named more than 10 times, and some expert is named exactly 10 times.
All inputs are finite; a program needn't handle non-finite values.
Results may differ from a plain program's by a relative error of at most 0.014.
Values may be sent and summed in bfloat16 or wider, within the bound.
No kernel may reach another device: no remote copies, remote signals or barrier semaphores. Data moves between devices by JAX's collectives and lax.ppermute only.
A program may use at most 64 MiB of HBM per device.

v0:
```python
import functools

import jax
import jax.numpy as jnp
from jax import lax
from jax.experimental import pallas as pl
from jax.experimental.pallas import tpu as pltpu
from jax.sharding import PartitionSpec as P

HEADS = 16
HEAD = 128
GROUPS = 4
TOP = 2
CORES = 2


epsilon = 1e-06
rope_base = 10000.0
f32 = jnp.float32
bf16 = jnp.bfloat16


def swap_cores(array):
    size = lax.axis_size("tp")
    return lax.ppermute(array, "tp", [(i, i ^ 1) for i in range(size)])


def along_z(array):
    size = lax.axis_size("tp")
    found = [array]
    for k in range(1, size // CORES):
        found.append(lax.ppermute(array, "tp", [(i, i ^ (CORES * k)) for i in range(size)]))
    return found


def to_peers(arrays):
    size = lax.axis_size("ep")
    found = [arrays[0]]
    for k in range(1, size):
        found.append(lax.ppermute(arrays[k], "ep", [(i, i ^ k) for i in range(size)]))
    return found


def split_pieces(refs, levels):
    own, rest, other, others = refs
    rows = own.shape[-2]
    found = []
    for one, many in ((own, rest), (other, others)):
        found.append(one)
        found += [many.at[..., pl.ds(k * rows, rows), :] for k in range(levels - 1)]
    return found


def spots(count, width):
    level, core = lax.axis_index("tp") // CORES, lax.axis_index("tp") % CORES
    half = count // 2
    tables = [(level ^ k) * CORES + core for k in range(half)]
    tables += [(level ^ k) * CORES + (1 - core) for k in range(half)]
    return [pl.multiple_of(table * width, 128) for table in tables]


def near(array):
    return pltpu.with_memory_space_constraint(array, pltpu.VMEM)


def held():
    return pl.BlockSpec(memory_space=pltpu.VMEM)


def near_shape(shape, dtype):
    return pltpu.VMEM(shape, dtype)


def limit(mebibytes):
    return pltpu.CompilerParams(vmem_limit_bytes=mebibytes << 20)


def cost(microseconds):
    work = int(microseconds * 2.5e9)
    return pl.CostEstimate(flops=work, bytes_accessed=int(microseconds * 1.5e7), transcendentals=0)


def whole(shape):
    rank = len(shape)
    return pl.BlockSpec(shape, lambda *_: (0,) * rank)


def prepare_kernel(peers, experts, slots, ids_ref, share_ref, *outs):
    me = lax.axis_index("ep")
    rows = ids_ref.shape[1]
    ids = ids_ref[...]
    picks = [ids[number : number + 1, :] for number in range(TOP)]
    line = lax.broadcasted_iota(jnp.int32, (max(peers, 8), rows), 0)
    goes = None
    for pick in picks:
        hit = pick // experts == (line ^ me)
        goes = hit if goes is None else goes | hit
    row = lax.broadcasted_iota(jnp.int32, (rows, rows), 0)
    column = lax.broadcasted_iota(jnp.int32, (rows, rows), 1)
    before = (row < column).astype(f32).astype(bf16)
    counts = jnp.dot(goes.astype(f32).astype(bf16), before, preferred_element_type=f32)
    slot = jnp.where(goes, counts, -1.0)
    share = share_ref[...]
    line = lax.broadcasted_iota(jnp.int32, (HEAD, rows), 0)
    target = lax.broadcasted_iota(jnp.int32, (slots, rows), 0).astype(f32)
    for peer in range(peers):
        spot = (slot[peer : peer + 1, :] == target).astype(f32).astype(bf16)
        outs[peer][...] = spot
        table = jnp.zeros((HEAD, rows), f32)
        for expert in range(experts):
            number = (me ^ peer) * experts + expert
            weight = jnp.zeros((1, rows), f32)
            for pick in range(TOP):
                weight += jnp.where(picks[pick] == number, share[pick : pick + 1, :], 0.0)
            high = weight.astype(bf16).astype(f32)
            mid = (weight - high).astype(bf16).astype(f32)
            low = weight - high - mid
            table = jnp.where(line == expert, high, table)
            table = jnp.where(line == experts + expert, mid, table)
            table = jnp.where(line == 2 * experts + expert, low, table)
        moved = lax.dot_general(
            spot, table.astype(bf16), (((1,), (1,)), ((), ())), preferred_element_type=f32
        )
        outs[peers + peer][...] = moved.astype(bf16)


def prepare(route_ids, route_weight, peers, experts, slots):
    rows = route_ids.shape[0]
    outs = pl.pallas_call(
        functools.partial(prepare_kernel, peers, experts, slots),
        out_shape=[near_shape((slots, rows), bf16)] * peers
        + [near_shape((slots, HEAD), bf16)] * peers,
        in_specs=[held()] * 2,
        out_specs=[held()] * (2 * peers),
        compiler_params=limit(4),
        cost_estimate=cost(2),
        name="prepare",
    )(near(route_ids.T), near(route_weight.T))
    return outs[:peers], outs[peers:]


def sort_kernel(count, *refs):
    pieces = refs[:count]
    outs = refs[-1 - count : -1]
    squares_ref = refs[-1]
    level = lax.axis_index("tp") // CORES
    me = lax.axis_index("ep")
    values = [piece[...] for piece in pieces]
    for peer in range(count):
        wanted = level ^ me ^ peer
        chosen = values[0]
        for number in range(1, count):
            chosen = jnp.where(wanted == number, values[number], chosen)
        outs[peer][...] = chosen
    total = None
    for value in values:
        wide = value.astype(f32)
        here = jnp.sum(wide * wide, axis=-1, keepdims=True)
        total = here if total is None else total + here
    squares_ref[...] = jnp.broadcast_to(total, squares_ref.shape)


def sort_pieces(pieces, earlier):
    rows, width = pieces[0].shape
    count = len(pieces)
    outs = pl.pallas_call(
        functools.partial(sort_kernel, count),
        out_shape=[near_shape((rows, width), bf16)] * count + [near_shape((rows, HEAD), f32)],
        in_specs=[held()] * (count + len(earlier)),
        out_specs=[held()] * (count + 1),
        compiler_params=limit(4),
        cost_estimate=cost(1),
        name="sort",
    )(*[near(array) for array in (*pieces, *earlier)])
    return outs[:count], outs[count]


def project_kernel(count, peers, rows, *refs):
    gain_ref = refs[0]
    parts = refs[1 : 1 + count]
    weights = refs[1 + count : 5 + count]
    outs = refs[5 + count :]
    slab, width = weights[0].shape
    core = lax.axis_index("tp") % CORES
    base = lax.axis_index("ep") * slab
    totals = [None] * 4
    for number in range(count):
        part = parts[number]
        span = part.shape[1]
        place = (core ^ number) * span if count > 1 else 0
        start = pl.multiple_of(place, 128)
        gain = gain_ref[:, pl.ds(pl.multiple_of(base + place, 128), span)]
        scaled = (part[...].astype(f32) * gain).astype(bf16)
        for which in range(4):
            block = weights[which][pl.ds(start, span), :]
            product = jnp.dot(scaled, block, preferred_element_type=f32)
            totals[which] = product if totals[which] is None else totals[which] + product
    for peer in range(peers):
        for which in range(4):
            rows_here = totals[which][peer * rows : (peer + 1) * rows, :]
            outs[peer][:, which * width : (which + 1) * width] = rows_here.astype(outs[peer].dtype)


def project(parts, gain, weights, peers, rows):
    width = weights[0].shape[1]
    out_shape = [near_shape((rows, 4 * width), f32)]
    out_shape += [near_shape((rows, 4 * width), bf16)] * (peers - 1)
    operands = [near(array) for array in (gain, *parts, *weights)]
    return pl.pallas_call(
        functools.partial(project_kernel, len(parts), peers, rows),
        out_shape=out_shape,
        in_specs=[held()] * len(operands),
        out_specs=[held()] * peers,
        compiler_params=limit(8),
        cost_estimate=cost(2),
        name="project",
    )(*operands)


def blocks_of(block):
    row = lax.broadcasted_iota(jnp.int32, (block, block * HEAD), 0)
    lane = lax.broadcasted_iota(jnp.int32, (block, block * HEAD), 1)
    return (lane // HEAD == row).astype(f32)


def columns_times(rows, table):
    high = rows.astype(bf16).astype(f32)
    mid = (rows - high).astype(bf16).astype(f32)
    split = jnp.concatenate([high, mid, rows - high - mid], axis=0).astype(bf16)
    return lax.dot_general(split, table, (((0,), (0,)), ((), ())), preferred_element_type=f32)


def decay_of(head, heads):
    number = (lax.axis_index("tp") * heads + head).astype(f32)
    power = jnp.full((1, HEAD), -5.0, f32) - number * (5.0 / (HEADS - 1))
    return 1.0 - jnp.exp2(power)


def read_kernel(peers, heads, width_model, *refs):
    squares, cos_ref, sin_ref, gain_ref = refs[0:2], refs[2], refs[3], refs[4]
    parts = refs[5 : 5 + peers]
    state_ref = refs[5 + peers]
    mixed_ref, key_ref, value_ref = refs[6 + peers : 9 + peers]
    query_ref, read_ref = refs[9 + peers :]
    rows, width = mixed_ref.shape
    mean = (squares[0][:, :1] + squares[1][:, :1]) * (1.0 / width_model)
    factor = lax.rsqrt(mean + epsilon)

    def total(which):
        cut = slice(which * width, (which + 1) * width)
        summed = parts[0][:, cut]
        for part in parts[1:]:
            summed = summed + part[:, cut].astype(f32)
        return (summed * factor).astype(bf16).astype(f32)

    query, key, value = total(0), total(1), total(2)
    value_ref[...] = value
    gate = total(3)
    gate = gate * jax.nn.sigmoid(gate) * gain_ref[...]
    own = []
    for head in range(heads):
        cut = slice(head * HEAD, (head + 1) * HEAD)
        one, two = query[:, cut], key[:, cut]
        one = one * cos_ref[...] + pltpu.roll(one, HEAD // 2, 1) * sin_ref[...]
        two = two * cos_ref[...] + pltpu.roll(two, HEAD // 2, 1) * sin_ref[...]
        two = two * HEAD ** (-0.5)
        query_ref[:, cut] = one
        key_ref[:, cut] = two
        own.append(jnp.sum(one * two, axis=-1, keepdims=True) * value[:, cut])
    block = 8
    mask = blocks_of(block)
    ones = jnp.concatenate([mask] * 3, axis=0).astype(bf16)

    def some(number, carry):
        start = pl.multiple_of(number * block, block)
        for head in range(heads):
            cut = slice(head * HEAD, (head + 1) * HEAD)
            spread = columns_times(query_ref[pl.ds(start, block), cut], ones)
            found = [
                jnp.sum(
                    spread[:, row * HEAD : (row + 1) * HEAD] * state_ref[start + row, head],
                    axis=0,
                    keepdims=True,
                )
                for row in range(block)
            ]
            read_ref[pl.ds(start, block), cut] = jnp.concatenate(found, axis=0)
        return carry

    lax.fori_loop(0, rows // block, some, 0)
    for head in range(heads):
        cut = slice(head * HEAD, (head + 1) * HEAD)
        read = decay_of(head, heads) * read_ref[:, cut] + own[head]
        centered = read - jnp.mean(read, axis=-1, keepdims=True)
        spread = jnp.mean(centered * centered, axis=-1, keepdims=True)
        normal = centered * lax.rsqrt(spread + epsilon)
        mixed_ref[:, cut] = (normal * gate[:, cut]).astype(bf16)


def read_state(parts, squares, cosine, sine, head_gain, ret_state, width_model):
    rows, heads = ret_state.shape[:2]
    width = heads * HEAD
    operands = [near(a) for a in (*squares, cosine, sine, head_gain, *parts, ret_state)]
    return pl.pallas_call(
        functools.partial(read_kernel, len(parts), heads, width_model),
        out_shape=[
            near_shape((rows, width), bf16),
            near_shape((rows, width), f32),
            near_shape((rows, width), f32),
        ],
        in_specs=[held()] * len(operands),
        out_specs=[held()] * 3,
        scratch_shapes=[pltpu.VMEM((rows, width), f32)] * 2,
        compiler_params=limit(4),
        cost_estimate=cost(2),
        name="read_state",
    )(*operands)


def update_kernel(heads, first, *refs):
    key_ref, value_ref, state_ref, next_ref = *refs[:3], refs[-1]
    block = next_ref.shape[0]
    start = pl.multiple_of((pl.program_id(0) + first) * block, block)
    mask = blocks_of(block)
    for head in range(heads):
        cut = slice(head * HEAD, (head + 1) * HEAD)
        values = value_ref[pl.ds(start, block), cut]
        table = jnp.concatenate([values] * block, axis=1) * mask
        table = jnp.concatenate([table] * 3, axis=0).astype(bf16)
        outer = columns_times(key_ref[pl.ds(start, block), cut], table)
        decay = decay_of(head, heads)
        for row in range(block):
            next_ref[row, head] = (
                decay * state_ref[start + row, head] + outer[:, row * HEAD : (row + 1) * HEAD]
            )


def update_state(key, value, ret_state, first, last, so_far, after):
    _, heads = ret_state.shape[:2]
    block = 8
    operands = [near(key), near(value), near(ret_state)] + [near(array) for array in after]
    specs = [held()] * len(operands)
    aliases = {}
    if so_far is not None:
        aliases = {len(operands): 0}
        operands.append(so_far)
        specs.append(pl.BlockSpec(memory_space=pl.ANY))
    return pl.pallas_call(
        functools.partial(update_kernel, heads, first),
        grid=(last - first,),
        out_shape=jax.ShapeDtypeStruct(ret_state.shape, f32),
        in_specs=specs,
        out_specs=pl.BlockSpec((block, heads, HEAD, HEAD), lambda i: (i + first, 0, 0, 0)),
        input_output_aliases=aliases,
        compiler_params=limit(6),
        cost_estimate=cost(2),
        name="update_state",
    )(*operands)


def out_kernel(count, peers, *refs):
    pieces = split_pieces(refs[:4], count // CORES)
    weight_ref, hidden_ref = refs[4:6]
    placing = refs[6 : 6 + peers]
    shares = refs[6 + peers : 6 + 2 * peers]
    after_ref = refs[6 + 2 * peers]
    outs = refs[7 + 2 * peers :]
    width = pieces[0].shape[1]
    places = spots(count, width)
    total = hidden_ref[...].astype(f32)
    for number in range(count):
        block = weight_ref[pl.ds(places[number], width), :]
        total = total + jnp.dot(pieces[number][...], block, preferred_element_type=f32)
    after = total.astype(bf16)
    after_ref[...] = after
    cut = after.shape[1]
    for peer in range(peers):
        sent = jnp.dot(placing[peer][...], after, preferred_element_type=f32)
        outs[peer][:, :cut] = sent.astype(bf16)
        outs[peer][:, cut:] = shares[peer][...]


def out_project(pieces, weight, hidden, placing, shares):
    rows, width = hidden.shape
    slots = placing[0].shape[0]
    peers = len(placing)
    operands = [near(array) for array in (*pieces, weight, hidden, *placing, *shares)]
    return pl.pallas_call(
        functools.partial(out_kernel, weight.shape[0] // pieces[0].shape[1], peers),
        out_shape=[near_shape((rows, width), bf16)]
        + [near_shape((slots, width + HEAD), bf16)] * peers,
        in_specs=[held()] * len(operands),
        out_specs=[held()] * (1 + peers),
        compiler_params=limit(8),
        cost_estimate=cost(2),
        name="out_project",
    )(*operands)


def lift_kernel(count, depth, *refs):
    pieces = split_pieces(refs[:4], count // CORES)
    gain_ref, gate_ref, up_ref, active_ref = refs[4:]
    width = pieces[0].shape[1]
    places = spots(count, width)
    squares = None
    for piece in pieces:
        values = piece[...].astype(f32)
        here = jnp.sum(values * values, axis=-1, keepdims=True)
        squares = here if squares is None else squares + here
    factor = lax.rsqrt(squares * (1.0 / depth) + epsilon)
    experts = gate_ref.shape[0]
    gates, ups = [None] * experts, [None] * experts
    for number in range(count):
        start = places[number]
        gain = gain_ref[:, pl.ds(start, width)]
        scaled = (pieces[number][...].astype(f32) * factor * gain).astype(bf16)
        for expert in range(experts):
            one = gate_ref[expert, pl.ds(start, width), :]
            two = up_ref[expert, pl.ds(start, width), :]
            gate = jnp.dot(scaled, one, preferred_element_type=f32)
            up = jnp.dot(scaled, two, preferred_element_type=f32)
            gates[expert] = gate if number == 0 else gates[expert] + gate
            ups[expert] = up if number == 0 else ups[expert] + up
    for expert in range(experts):
        gate = gates[expert]
        active_ref[expert] = (gate * jax.nn.sigmoid(gate) * ups[expert]).astype(bf16)


def lift(pieces, gain, expert_gate, expert_up):
    experts, depth, width = expert_gate.shape
    rows = pieces[0].shape[0]
    operands = [near(array) for array in (*pieces, gain, expert_gate, expert_up)]
    return pl.pallas_call(
        functools.partial(lift_kernel, depth // pieces[0].shape[1], depth),
        out_shape=near_shape((experts, rows, width), bf16),
        in_specs=[held()] * len(operands),
        out_specs=held(),
        compiler_params=limit(8),
        cost_estimate=cost(3),
        name="lift",
    )(*operands)


def lower_kernel(count, peers, slots, *refs):
    pieces = split_pieces(refs[:4], count // CORES)
    down_ref = refs[4]
    tables = refs[5 : 5 + peers]
    outs = refs[5 + peers : 5 + 2 * peers]
    mean_ref = refs[-1]
    experts, _, width = pieces[0].shape
    places = spots(count, width)
    totals = [None] * experts
    for number in range(count):
        start = places[number]
        for expert in range(experts):
            block = down_ref[expert, pl.ds(start, width), :]
            product = jnp.dot(pieces[number][expert], block, preferred_element_type=f32)
            totals[expert] = product if number == 0 else totals[expert] + product
    for expert in range(experts):
        mean_ref[expert] = totals[expert].astype(bf16).astype(f32)
    cut = tables[0].shape[1] - HEAD
    for peer in range(peers):
        table = tables[peer][:, cut:].astype(f32)
        sent = None
        for expert in range(experts):
            share = (
                table[:, expert : expert + 1]
                + table[:, experts + expert : experts + expert + 1]
                + table[:, 2 * experts + expert : 2 * experts + expert + 1]
            )
            here = mean_ref[expert, peer * slots : (peer + 1) * slots, :] * share
            sent = here if sent is None else sent + here
        outs[peer][...] = sent.astype(bf16)


def lower(pieces, expert_down, tables):
    experts, depth, width = expert_down.shape
    rows = pieces[0].shape[1]
    peers, slots = len(tables), tables[0].shape[0]
    operands = [near(array) for array in (*pieces, expert_down, *tables)]
    return pl.pallas_call(
        functools.partial(lower_kernel, depth // pieces[0].shape[2], peers, slots),
        out_shape=[near_shape((slots, width), bf16)] * peers,
        in_specs=[held()] * len(operands),
        out_specs=[held()] * peers,
        scratch_shapes=[pltpu.VMEM((experts, rows, width), f32)],
        compiler_params=limit(8),
        cost_estimate=cost(2),
        name="lower",
    )(*operands)


def finish_kernel(peers, *refs):
    after_ref = refs[0]
    placing = refs[1 : 1 + peers]
    back = refs[1 + peers : 1 + 2 * peers]
    updated_ref = refs[-1]
    total = after_ref[...].astype(f32)
    for peer in range(peers):
        total = total + lax.dot_general(
            placing[peer][...],
            back[peer][...],
            (((0,), (0,)), ((), ())),
            preferred_element_type=f32,
        )
    updated_ref[...] = total.astype(bf16)


def finish(after, placing, back):
    operands = [near(array) for array in (after, *placing, *back)]
    return pl.pallas_call(
        functools.partial(finish_kernel, len(placing)),
        out_shape=jax.ShapeDtypeStruct(after.shape, bf16),
        in_specs=[held()] * len(operands),
        out_specs=whole(after.shape),
        compiler_params=limit(4),
        cost_estimate=cost(1),
        name="finish",
    )(*operands)


def shared(lines):
    rest = jnp.concatenate(lines[1:], axis=-2)
    return [lines[0], rest, swap_cores(lines[0]), swap_cores(rest)]


def layer(
    hidden,
    positions,
    ret_state,
    query_weight,
    key_weight,
    value_weight,
    gate_weight,
    head_gain,
    out_weight,
    mix_gain,
    ffn_gain,
    expert_gate,
    expert_up,
    expert_down,
    route_ids,
    route_weight,
):
    own_rows, slice_width = hidden.shape
    peers = lax.axis_size("ep")
    ranks = lax.axis_size("tp")
    depth = slice_width * ranks
    slab, width = query_weight.shape

    local_experts = expert_gate.shape[0]
    group_size = local_experts * peers // GROUPS
    capacity = 2 * ((own_rows // GROUPS + group_size - 1) // group_size)
    slots = local_experts * capacity
    if local_experts % group_size == 0:
        slots = slots // TOP
    placing, shares = prepare(route_ids, route_weight, peers, local_experts, slots)

    inverse = 1.0 / rope_base ** (jnp.arange(0, HEAD, 2, dtype=f32) / HEAD)
    angle = positions.astype(f32)[:, None] * inverse[None, :]
    cosine, sine = jnp.cos(angle), jnp.sin(angle)
    cosine = jnp.concatenate([cosine, cosine], axis=1)
    sine = jnp.concatenate([-sine, sine], axis=1)

    if ranks == CORES * peers:
        sorted_pieces, squares = sort_pieces(along_z(hidden), (shares[0], cosine, sine))
        squares = [squares, swap_cores(squares)]
        half = jnp.concatenate(to_peers(sorted_pieces), axis=0)
        parts = [half, swap_cores(half)]
    else:
        me = lax.axis_index("ep")
        full_rows = lax.all_gather(hidden, "tp", axis=1, tiled=True)
        squares = jnp.sum(jnp.square(full_rows.astype(f32)), axis=1, keepdims=True)
        squares = [squares, jnp.zeros_like(squares)]
        columns = lax.all_to_all(full_rows, "ep", split_axis=1, concat_axis=0, tiled=True)
        columns = columns.reshape(peers, own_rows, slab)
        parts = [columns[me ^ jnp.arange(peers)].reshape(peers * own_rows, slab)]
    weights = (query_weight, key_weight, value_weight, gate_weight)
    partial = project(parts, mix_gain.reshape(1, depth), weights, peers, own_rows)
    sums = to_peers(partial)

    mixed, key, value = read_state(
        sums, squares, cosine, sine, head_gain.reshape(1, width), ret_state, depth
    )
    blocks = own_rows // 8
    split = max(1, 2 * blocks // 5)
    next_state = update_state(key, value, ret_state, 0, split, None, ())

    lines, next_state = lax.optimization_barrier((along_z(mixed), next_state))
    pieces = shared(lines)
    after, *packed = out_project(pieces, out_weight, hidden, placing, shares)

    next_state = update_state(key, value, ret_state, split, blocks, next_state, (after,))
    arrived = to_peers(packed)
    arrived, next_state = lax.optimization_barrier((arrived, next_state))
    rows = jnp.concatenate([table[:, :slice_width] for table in arrived], axis=0)
    pieces = shared(along_z(rows))
    active = lift(pieces, ffn_gain.reshape(1, depth), expert_gate, expert_up)

    pieces = shared(along_z(active))
    back = lower(pieces, expert_down, arrived)
    back = to_peers(back)
    return (finish(after, placing, back), next_state)


def solution(mesh):
    return jax.shard_map(
        layer,
        mesh=mesh,
        in_specs=(
            P("ep", "tp"),
            P("ep"),
            P("ep", "tp", None, None),
            P("ep", "tp"),
            P("ep", "tp"),
            P("ep", "tp"),
            P("ep", "tp"),
            P("tp"),
            P(None, "tp"),
            P(),
            P(),
            P("ep", None, "tp"),
            P("ep", None, "tp"),
            P("ep", None, "tp"),
            P("ep", None),
            P("ep", None),
        ),
        out_specs=(P("ep", "tp"), P("ep", "tp", None, None)),
        check_vma=False,
    )
```

profile of v0, /device:TPU:0, one launch (start us, length us, event | category | flops | bytes accessed | tf_op | source)
XLA Modules:
  0.0 76.9 jit_solution(15744693941063136385)
XLA Ops:
  0.6 3.1 %collective-permute-start = (bf16[40,512]{1,0:T(8,128)(2,1)}, bf16[40,512]{1,0:T(8,128)(2,1)S(1)}, u32[]{:S(2)}, u32[]{:S(2)}) collective-permute-start(bf16[40,512]{1,0:T(8,128)(2,1)} %refs_5_.4), channel_id=1, source_target_pairs={{0,2},{1,3},{2,0},{3,1},{4,6},{5,7},{6,4},{7,5},{8,10},{9,11},{10,... | collective-permute-start | bytes 122888 | tf_op jit(solution)/shard_map/ppermute | solution.py:32
  3.7 2.6 %collective-permute-start.1 = (bf16[40,512]{1,0:T(8,128)(2,1)}, bf16[40,512]{1,0:T(8,128)(2,1)S(1)}, u32[]{:S(2)}, u32[]{:S(2)}) collective-permute-start(bf16[40,512]{1,0:T(8,128)(2,1)} %refs_5_.4), channel_id=1, source_target_pairs={{0,4},{1,5},{2,6},{3,7},{4,0},{5,1},{6,2},{7,3},{8,12},{9,13},{10,... | collective-permute-start | bytes 122888 | tf_op jit(solution)/shard_map/ppermute | solution.py:32
  6.3 0.7 convert_element_type.3
  7.0 0.7 copy-done.11
  7.7 0.7 copy-done.12
  8.4 0.3 prepare.1
  8.6 0.2 fusion
  8.8 0.1 pad_maximum_fusion.1
  8.9 0.7 collective-permute-done.1.refs_2_
  9.6 2.7 %collective-permute-done.2.refs_3_ = bf16[40,512]{1,0:T(8,128)(2,1)S(1)} collective-permute-done((bf16[40,512]{1,0:T(8,128)(2,1)}, bf16[40,512]{1,0:T(8,128)(2,1)S(1)}, u32[]{:S(2)}, u32[]{:S(2)}) %collective-permute-start.2) | collective-permute-done | bytes 40992 | tf_op jit(solution)/shard_map/ppermute | solution.py:32
  12.4 0.1 sort.1
  12.5 1.6 %collective-permute-start.4 = (bf16[40,512]{1,0:T(8,128)(2,1)S(1)}, bf16[40,512]{1,0:T(8,128)(2,1)S(1)}, u32[]{:S(2)}, u32[]{:S(2)}) collective-permute-start(bf16[40,512]{1,0:T(8,128)(2,1)S(1)} %get-tuple-element.44), channel_id=1, source_target_pairs={{0,8},{8,0},{16,24},{24,16},{1,9},{9,1},{17,25},{25,17},{2,10},{10... | collective-permute-start | bytes 122888 | tf_op jit(solution)/shard_map/ppermute | solution.py:40
  14.1 1.5 %collective-permute-start.5 = (bf16[40,512]{1,0:T(8,128)(2,1)S(1)}, bf16[40,512]{1,0:T(8,128)(2,1)S(1)}, u32[]{:S(2)}, u32[]{:S(2)}) collective-permute-start(bf16[40,512]{1,0:T(8,128)(2,1)S(1)} %get-tuple-element.45), channel_id=1, source_target_pairs={{0,16},{8,24},{16,0},{24,8},{1,17},{9,25},{17,1},{25,9},{2,18},{10... | collective-permute-start | bytes 122888 | tf_op jit(solution)/shard_map/ppermute | solution.py:40
  15.6 0.5 collective-permute-start.6
  16.1 0.6 collective-permute-done.4
  16.7 1.4 %collective-permute-done.5 = bf16[40,512]{1,0:T(8,128)(2,1)S(1)} collective-permute-done((bf16[40,512]{1,0:T(8,128)(2,1)S(1)}, bf16[40,512]{1,0:T(8,128)(2,1)S(1)}, u32[]{:S(2)}, u32[]{:S(2)}) %collective-permute-start.5) | collective-permute-done | bytes 40992 | tf_op jit(solution)/shard_map/ppermute | solution.py:40
  18.1 2.4 %collective-permute-done.6 = bf16[40,512]{1,0:T(8,128)(2,1)S(1)} collective-permute-done((bf16[40,512]{1,0:T(8,128)(2,1)S(1)}, bf16[40,512]{1,0:T(8,128)(2,1)S(1)}, u32[]{:S(2)}, u32[]{:S(2)}) %collective-permute-start.6) | collective-permute-done | bytes 40992 | tf_op jit(solution)/shard_map/ppermute | solution.py:40
  20.5 1.4 %collective-permute-done.7.refs_2_ = bf16[160,512]{1,0:T(8,128)(2,1)S(1)} collective-permute-done((bf16[160,512]{1,0:T(8,128)(2,1)S(1)}, bf16[160,512]{1,0:T(8,128)(2,1)S(1)}, u32[]{:S(2)}, u32[]{:S(2)}) %collective-permute-start.7) | collective-permute-done | bytes 163872 | tf_op jit(solution)/shard_map/ppermute | solution.py:25
  21.9 0.0 slice-start.1
  22.0 0.5 project.1
  22.5 0.6 collective-permute-start.8
  23.1 0.5 collective-permute-start.9
  23.6 2.5 %collective-permute-start.10 = (bf16[40,1024]{1,0:T(8,128)(2,1)S(1)}, bf16[40,1024]{1,0:T(8,128)(2,1)S(1)}, u32[]{:S(2)}, u32[]{:S(2)}) collective-permute-start(bf16[40,1024]{1,0:T(8,128)(2,1)S(1)} %get-tuple-element.50), channel_id=1, source_target_pairs={{0,24},{8,16},{16,8},{24,0},{1,25},{9,17},{17,9},{25,1},{2,26},{10... | collective-permute-start | bytes 245768 | tf_op jit(solution)/shard_map/ppermute | solution.py:40
  26.1 1.2 %collective-permute-done.3.refs_1_ = f32[40,128]{1,0:T(8,128)S(1)} collective-permute-done((f32[40,128]{1,0:T(8,128)S(1)}, f32[40,128]{1,0:T(8,128)S(1)}, u32[]{:S(2)}, u32[]{:S(2)}) %collective-permute-start.3) | collective-permute-done | bytes 20512 | tf_op jit(solution)/shard_map/ppermute | solution.py:25
  27.3 0.1 collective-permute-done.8.refs_6_
  27.4 1.9 %collective-permute-done.9.refs_7_ = bf16[40,1024]{1,0:T(8,128)(2,1)S(1)} collective-permute-done((bf16[40,1024]{1,0:T(8,128)(2,1)S(1)}, bf16[40,1024]{1,0:T(8,128)(2,1)S(1)}, u32[]{:S(2)}, u32[]{:S(2)}) %collective-permute-start.9) | collective-permute-done | bytes 81952 | tf_op jit(solution)/shard_map/ppermute | solution.py:40
  29.3 2.1 %read_state.1 = (bf16[40,256]{1,0:T(8,128)(2,1)S(1)}, f32[40,256]{1,0:T(8,128)S(1)}, f32[40,256]{1,0:T(8,128)S(1)}) custom-call(f32[40,128]{1,0:T(8,128)S(1)} %get-tuple-element.42.refs_0_, f32[40,128]{1,0:T(8,128)S(1)} %collective-permute-done.3.refs_1_, f32[40,128]{1,0:T(8,128)S(1)} %get-tuple-element.83.refs_5_.refs_2_, ...), custom_call_target="tpu_custom_call" | custom-call | flops 5000000000 | bytes 30000000 | tf_op jit(solution)/shard_map/read_state/pallas_call | solution.py:304
  31.5 0.1 collective-permute-start.11
  31.5 1.2 %collective-permute-start.12 = (bf16[40,256]{1,0:T(8,128)(2,1)S(1)}, bf16[40,256]{1,0:T(8,128)(2,1)S(1)}, u32[]{:S(2)}, u32[]{:S(2)}) collective-permute-start(bf16[40,256]{1,0:T(8,128)(2,1)S(1)} %get-tuple-element.54.refs_0_), channel_id=1, source_target_pairs={{0,4},{1,5},{2,6},{3,7},{4,0},{5,1},{6,2},{7,3},{8,12},{9,13},{10,... | collective-permute-start | bytes 61448 | tf_op jit(solution)/shard_map/ppermute | solution.py:32
  32.7 3.2 %collective-permute-start.13 = (bf16[40,256]{1,0:T(8,128)(2,1)S(1)}, bf16[40,256]{1,0:T(8,128)(2,1)S(1)}, u32[]{:S(2)}, u32[]{:S(2)}) collective-permute-start(bf16[40,256]{1,0:T(8,128)(2,1)S(1)} %get-tuple-element.54.refs_0_), channel_id=1, source_target_pairs={{0,6},{1,7},{2,4},{3,5},{4,2},{5,3},{6,0},{7,1},{8,14},{9,15},{10,... | collective-permute-start | bytes 61448 | tf_op jit(solution)/shard_map/ppermute | solution.py:32
  35.9 1.6 %update_state.2.refs_4_ = f32[40,2,128,128]{3,2,1,0:T(8,128)} custom-call(f32[40,256]{1,0:T(8,128)S(1)} %get-tuple-element.52.refs_0_, f32[40,256]{1,0:T(8,128)S(1)} %get-tuple-element.53.refs_1_, f32[40,2,128,128]{3,2,1,0:T(8,128)S(1)} %bitcast.6), custom_call_target="tpu_custom_call" | custom-call | flops 5000000000 | bytes 30000000 | tf_op jit(solution)/shard_map/update_state/pallas_call | solution.py:348
  37.6 0.7 collective-permute-done.13
  38.3 0.1 collective-permute-start.15
  38.4 0.5 collective-permute-start.14
  38.9 0.8 %collective-permute-done.14.refs_2_ = bf16[40,256]{1,0:T(8,128)(2,1)S(1)} collective-permute-done((bf16[40,256]{1,0:T(8,128)(2,1)S(1)}, bf16[40,256]{1,0:T(8,128)(2,1)S(1)}, u32[]{:S(2)}, u32[]{:S(2)}) %collective-permute-start.14) | collective-permute-done | bytes 20512 | tf_op jit(solution)/shard_map/ppermute | solution.py:25
  39.7 0.6 out_project.1
  40.3 1.6 %collective-permute-start.16 = (bf16[10,640]{1,0:T(8,128)(2,1)S(1)}, bf16[10,640]{1,0:T(8,128)(2,1)S(1)}, u32[]{:S(2)}, u32[]{:S(2)}) collective-permute-start(bf16[10,640]{1,0:T(8,128)(2,1)S(1)} %get-tuple-element.67), channel_id=1, source_target_pairs={{0,8},{8,0},{16,24},{24,16},{1,9},{9,1},{17,25},{25,17},{2,10},{10... | collective-permute-start | bytes 38408 | tf_op jit(solution)/shard_map/ppermute | solution.py:40
  41.9 1.2 %collective-permute-start.17 = (bf16[10,640]{1,0:T(8,128)(2,1)S(1)}, bf16[10,640]{1,0:T(8,128)(2,1)S(1)}, u32[]{:S(2)}, u32[]{:S(2)}) collective-permute-start(bf16[10,640]{1,0:T(8,128)(2,1)S(1)} %get-tuple-element.68), channel_id=1, source_target_pairs={{0,16},{8,24},{16,0},{24,8},{1,17},{9,25},{17,1},{25,9},{2,18},{10... | collective-permute-start | bytes 38408 | tf_op jit(solution)/shard_map/ppermute | solution.py:40
  43.0 0.8 %collective-permute-start.18 = (bf16[10,640]{1,0:T(8,128)(2,1)S(1)}, bf16[10,640]{1,0:T(8,128)(2,1)S(1)}, u32[]{:S(2)}, u32[]{:S(2)}) collective-permute-start(bf16[10,640]{1,0:T(8,128)(2,1)S(1)} %get-tuple-element.69), channel_id=1, source_target_pairs={{0,24},{8,16},{16,8},{24,0},{1,25},{9,17},{17,9},{25,1},{2,26},{10... | collective-permute-start | bytes 38408 | tf_op jit(solution)/shard_map/ppermute | solution.py:40
  43.9 2.6 %update_state.3 = f32[40,2,128,128]{3,2,1,0:T(8,128)} custom-call(f32[40,256]{1,0:T(8,128)S(1)} %get-tuple-element.52.refs_0_, f32[40,256]{1,0:T(8,128)S(1)} %get-tuple-element.53.refs_1_, f32[40,2,128,128]{3,2,1,0:T(8,128)S(1)} %bitcast.6, bf16[40,512]{1,0:T(8,128)(2,1)S(1)} %get-tuple-element.65.refs_3_.refs_0_, ...), custom_call_target="tpu_custom_call", output_to_operand_aliasing={{}: (4, {})} | custom-call | flops 5000000000 | bytes 30000000 | tf_op jit(solution)/shard_map/update_state/pallas_call | solution.py:348
  46.5 1.2 %collective-permute-done.18.refs_8_ = bf16[10,640]{1,0:T(8,128)(2,1)S(1)} collective-permute-done((bf16[10,640]{1,0:T(8,128)(2,1)S(1)}, bf16[10,640]{1,0:T(8,128)(2,1)S(1)}, u32[]{:S(2)}, u32[]{:S(2)}) %collective-permute-start.18) | collective-permute-done | bytes 12832 | tf_op jit(solution)/shard_map/ppermute | solution.py:40
  47.8 0.1 collective-permute-start.19
  47.9 3.8 %collective-permute-start.20 = (bf16[40,512]{1,0:T(8,128)(2,1)S(1)}, bf16[40,512]{1,0:T(8,128)(2,1)S(1)}, u32[]{:S(2)}, u32[]{:S(2)}) collective-permute-start(bf16[40,512]{1,0:T(8,128)(2,1)S(1)} %pad_maximum_fusion.refs_0_), channel_id=1, source_target_pairs={{0,4},{1,5},{2,6},{3,7},{4,0},{5,1},{6,2},{7,3},{8,12},{9,13},{10,... | collective-permute-start | bytes 122888 | tf_op jit(solution)/shard_map/ppermute | solution.py:32
  51.6 0.6 collective-permute-start.21
  52.2 1.4 %collective-permute-done.20 = bf16[40,512]{1,0:T(8,128)(2,1)S(1)} collective-permute-done((bf16[40,512]{1,0:T(8,128)(2,1)S(1)}, bf16[40,512]{1,0:T(8,128)(2,1)S(1)}, u32[]{:S(2)}, u32[]{:S(2)}) %collective-permute-start.20) | collective-permute-done | bytes 40992 | tf_op jit(solution)/shard_map/ppermute | solution.py:32
  53.6 3.8 %collective-permute-done.21 = bf16[40,512]{1,0:T(8,128)(2,1)S(1)} collective-permute-done((bf16[40,512]{1,0:T(8,128)(2,1)S(1)}, bf16[40,512]{1,0:T(8,128)(2,1)S(1)}, u32[]{:S(2)}, u32[]{:S(2)}) %collective-permute-start.21) | collective-permute-done | bytes 40992 | tf_op jit(solution)/shard_map/ppermute | solution.py:32
  57.4 0.5 collective-permute-start.22
  57.9 0.9 %collective-permute-done.22.refs_2_ = bf16[40,512]{1,0:T(8,128)(2,1)S(1)} collective-permute-done((bf16[40,512]{1,0:T(8,128)(2,1)S(1)}, bf16[40,512]{1,0:T(8,128)(2,1)S(1)}, u32[]{:S(2)}, u32[]{:S(2)}) %collective-permute-start.22) | collective-permute-done | bytes 40992 | tf_op jit(solution)/shard_map/ppermute | solution.py:25
  58.9 1.7 %lift.1.refs_0_ = bf16[2,40,256]{2,1,0:T(8,128)(2,1)S(1)} custom-call(bf16[40,512]{1,0:T(8,128)(2,1)S(1)} %pad_maximum_fusion.refs_0_, bf16[120,512]{1,0:T(8,128)(2,1)S(1)} %constant_dynamic-update-slice_fusion.7.refs_1_, bf16[40,512]{1,0:T(8,128)(2,1)S(1)} %collective-permute-done.22.refs_2_, bf16[120,512]{1,0:T(8,128)(2,1)S(1)} %collective-permute-done.23.refs_3_, ...), custom_call_target="tpu_custom_call" | custom-call | flops 7500000256 | bytes 45000000 | tf_op jit(solution)/shard_map/lift/pallas_call | solution.py:433
  60.5 0.1 collective-permute-start.24
  60.6 1.2 %collective-permute-start.25 = (bf16[2,40,256]{2,1,0:T(8,128)(2,1)S(1)}, bf16[2,40,256]{2,1,0:T(8,128)(2,1)S(1)}, u32[]{:S(2)}, u32[]{:S(2)}) collective-permute-start(bf16[2,40,256]{2,1,0:T(8,128)(2,1)S(1)} %lift.1.refs_0_), channel_id=1, source_target_pairs={{0,4},{1,5},{2,6},{3,7},{4,0},{5,1},{6,2},{7,3},{8,12},{9,13},{10,... | collective-permute-start | bytes 122888 | tf_op jit(solution)/shard_map/ppermute | solution.py:32
  61.8 3.2 %collective-permute-start.26 = (bf16[2,40,256]{2,1,0:T(8,128)(2,1)S(1)}, bf16[2,40,256]{2,1,0:T(8,128)(2,1)S(1)}, u32[]{:S(2)}, u32[]{:S(2)}) collective-permute-start(bf16[2,40,256]{2,1,0:T(8,128)(2,1)S(1)} %lift.1.refs_0_), channel_id=1, source_target_pairs={{0,6},{1,7},{2,4},{3,5},{4,2},{5,3},{6,0},{7,1},{8,14},{9,15},{10,... | collective-permute-start | bytes 122888 | tf_op jit(solution)/shard_map/ppermute | solution.py:32
  65.0 2.6 %collective-permute-done.25 = bf16[2,40,256]{2,1,0:T(8,128)(2,1)S(1)} collective-permute-done((bf16[2,40,256]{2,1,0:T(8,128)(2,1)S(1)}, bf16[2,40,256]{2,1,0:T(8,128)(2,1)S(1)}, u32[]{:S(2)}, u32[]{:S(2)}) %collective-permute-start.25) | collective-permute-done | bytes 40992 | tf_op jit(solution)/shard_map/ppermute | solution.py:32
  67.6 0.1 collective-permute-start.28
  67.7 0.5 collective-permute-start.27
  68.2 0.9 %collective-permute-done.27.refs_2_ = bf16[2,40,256]{2,1,0:T(8,128)(2,1)S(1)} collective-permute-done((bf16[2,40,256]{2,1,0:T(8,128)(2,1)S(1)}, bf16[2,40,256]{2,1,0:T(8,128)(2,1)S(1)}, u32[]{:S(2)}, u32[]{:S(2)}) %collective-permute-start.27) | collective-permute-done | bytes 40992 | tf_op jit(solution)/shard_map/ppermute | solution.py:25
  69.1 0.9 %lower.1 = (bf16[10,512]{1,0:T(8,128)(2,1)S(1)}, bf16[10,512]{1,0:T(8,128)(2,1)S(1)}, bf16[10,512]{1,0:T(8,128)(2,1)S(1)}, bf16[10,512]{1,0:T(8,128)(2,1)S(1)}) custom-call(bf16[2,40,256]{2,1,0:T(8,128)(2,1)S(1)} %lift.1.refs_0_, bf16[2,120,256]{2,1,0:T(8,128)(2,1)S(1)} %constant_dynamic-update-slice_fusion.10.refs_1_, ...), custom_call_target="tpu_custom_call" | custom-call | flops 5000000000 | bytes 30000000 | tf_op jit(solution)/shard_map/lower/pallas_call | solution.py:481
  69.9 0.5 collective-permute-start.29
  70.4 0.9 %collective-permute-start.30 = (bf16[10,512]{1,0:T(8,128)(2,1)S(1)}, bf16[10,512]{1,0:T(8,128)(2,1)S(1)}, u32[]{:S(2)}, u32[]{:S(2)}) collective-permute-start(bf16[10,512]{1,0:T(8,128)(2,1)S(1)} %get-tuple-element.77), channel_id=1, source_target_pairs={{0,16},{8,24},{16,0},{24,8},{1,17},{9,25},{17,1},{25,9},{2,18},{10... | collective-permute-start | bytes 30728 | tf_op jit(solution)/shard_map/ppermute | solution.py:40
  71.4 2.1 %collective-permute-start.31 = (bf16[10,512]{1,0:T(8,128)(2,1)S(1)}, bf16[10,512]{1,0:T(8,128)(2,1)S(1)}, u32[]{:S(2)}, u32[]{:S(2)}) collective-permute-start(bf16[10,512]{1,0:T(8,128)(2,1)S(1)} %get-tuple-element.78), channel_id=1, source_target_pairs={{0,24},{8,16},{16,8},{24,0},{1,25},{9,17},{17,9},{25,1},{2,26},{10... | collective-permute-start | bytes 30728 | tf_op jit(solution)/shard_map/ppermute | solution.py:40
  73.5 0.2 collective-permute-done.29.refs_6_
  73.7 0.5 collective-permute-done.30.refs_7_
  74.2 1.8 %collective-permute-done.31.refs_8_ = bf16[10,512]{1,0:T(8,128)(2,1)S(1)} collective-permute-done((bf16[10,512]{1,0:T(8,128)(2,1)S(1)}, bf16[10,512]{1,0:T(8,128)(2,1)S(1)}, u32[]{:S(2)}, u32[]{:S(2)}) %collective-permute-start.31) | collective-permute-done | bytes 10272 | tf_op jit(solution)/shard_map/ppermute | solution.py:40
  76.0 0.8 %finish.1 = bf16[40,512]{1,0:T(8,128)(2,1)} custom-call(bf16[40,512]{1,0:T(8,128)(2,1)S(1)} %get-tuple-element.65.refs_3_.refs_0_, bf16[10,40]{1,0:T(8,128)(2,1)S(1)} %get-tuple-element.58.refs_6_.refs_1_, bf16[10,40]{1,0:T(8,128)(2,1)S(1)} %get-tuple-element.59.refs_7_.refs_2_, bf16[10,40]{1,0:T(8,128)(2,1)S(1)} %get-tuple-element.60.refs_8_.refs_3_, ...), custom_call_target="tpu_custom_call" | custom-call | flops 2500000000 | bytes 15000000 | tf_op jit(solution)/shard_map/finish/pallas_call | solution.py:511
  (65 shorter events, 0.2 us)
Async XLA Ops:
  0.6 8.2 %collective-permute-start = (bf16[40,512]{1,0:T(8,128)(2,1)}, bf16[40,512]{1,0:T(8,128)(2,1)S(1)}, u32[]{:S(2)}, u32[]{:S(2)}) collective-permute-start(bf16[40,512]{1,0:T(8,128)(2,1)} %refs_5_.4), channel_id=1, source_target_pairs={{0,2},{1,3},{2,0},{3,1},{4,6},{5,7},{6,4},{7,5},{8,10},{9,11},{10,... | collective-permute-start | bytes 122888 | tf_op jit(solution)/shard_map/ppermute | solution.py:32
  3.7 5.9 %collective-permute-start.1 = (bf16[40,512]{1,0:T(8,128)(2,1)}, bf16[40,512]{1,0:T(8,128)(2,1)S(1)}, u32[]{:S(2)}, u32[]{:S(2)}) collective-permute-start(bf16[40,512]{1,0:T(8,128)(2,1)} %refs_5_.4), channel_id=1, source_target_pairs={{0,4},{1,5},{2,6},{3,7},{4,0},{5,1},{6,2},{7,3},{8,12},{9,13},{10,... | collective-permute-start | bytes 122888 | tf_op jit(solution)/shard_map/ppermute | solution.py:32
  6.3 6.0 %collective-permute-start.2 = (bf16[40,512]{1,0:T(8,128)(2,1)}, bf16[40,512]{1,0:T(8,128)(2,1)S(1)}, u32[]{:S(2)}, u32[]{:S(2)}) collective-permute-start(bf16[40,512]{1,0:T(8,128)(2,1)} %refs_5_.4), channel_id=1, source_target_pairs={{0,6},{1,7},{2,4},{3,5},{4,2},{5,3},{6,0},{7,1},{8,14},{9,15},{10,... | collective-permute-start | bytes 122888 | tf_op jit(solution)/shard_map/ppermute | solution.py:32
  7.0 0.7 copy-start.11
  7.7 0.7 copy-start.12
  8.4 4.0 %copy-start.8 = (bf16[40,512]{1,0:T(8,128)(2,1)S(1)}, bf16[40,512]{1,0:T(8,128)(2,1)}, u32[]{:S(2)}) copy-start(bf16[40,512]{1,0:T(8,128)(2,1)} %refs_5_.4) | copy-start | bytes 122884
  12.3 9.6 %copy-start.4 = (bf16[1024,256]{1,0:T(8,128)(2,1)S(1)}, bf16[1024,256]{1,0:T(8,128)(2,1)}, u32[]{:S(2)}) copy-start(bf16[1024,256]{1,0:T(8,128)(2,1)} %refs_3_.1) | copy-start | bytes 1572868
  12.4 9.6 %copy-start.5 = (bf16[1024,256]{1,0:T(8,128)(2,1)S(1)}, bf16[1024,256]{1,0:T(8,128)(2,1)}, u32[]{:S(2)}) copy-start(bf16[1024,256]{1,0:T(8,128)(2,1)} %refs_4_.3) | copy-start | bytes 1572868
  12.4 9.6 %copy-start.6 = (bf16[1024,256]{1,0:T(8,128)(2,1)S(1)}, bf16[1024,256]{1,0:T(8,128)(2,1)}, u32[]{:S(2)}) copy-start(bf16[1024,256]{1,0:T(8,128)(2,1)} %refs_5_.3) | copy-start | bytes 1572868
  12.4 9.6 %copy-start.7 = (bf16[1024,256]{1,0:T(8,128)(2,1)S(1)}, bf16[1024,256]{1,0:T(8,128)(2,1)}, u32[]{:S(2)}) copy-start(bf16[1024,256]{1,0:T(8,128)(2,1)} %refs_6_.2) | copy-start | bytes 1572868
  12.4 9.6 %copy-start.9 = (f32[4096]{0:T(1024)S(1)}, f32[4096]{0:T(1024)}, u32[]{:S(2)}) copy-start(f32[4096]{0:T(1024)} %param.25) | copy-start | bytes 49156
  12.4 16.9 %slice-start = ((s8[5242880]{0:T(1024)(128)(4,1)}), s8[4194304]{0:T(1024)(128)(4,1)S(1)}, s32[]{:S(2)}) async-start(s8[5242880]{0:T(1024)(128)(4,1)} %bitcast.5), calls=%async_computation | async-start | bytes 8388608
  12.5 4.2 %collective-permute-start.4 = (bf16[40,512]{1,0:T(8,128)(2,1)S(1)}, bf16[40,512]{1,0:T(8,128)(2,1)S(1)}, u32[]{:S(2)}, u32[]{:S(2)}) collective-permute-start(bf16[40,512]{1,0:T(8,128)(2,1)S(1)} %get-tuple-element.44), channel_id=1, source_target_pairs={{0,8},{8,0},{16,24},{24,16},{1,9},{9,1},{17,25},{25,17},{2,10},{10... | collective-permute-start | bytes 122888 | tf_op jit(solution)/shard_map/ppermute | solution.py:40
  14.1 4.0 %collective-permute-start.5 = (bf16[40,512]{1,0:T(8,128)(2,1)S(1)}, bf16[40,512]{1,0:T(8,128)(2,1)S(1)}, u32[]{:S(2)}, u32[]{:S(2)}) collective-permute-start(bf16[40,512]{1,0:T(8,128)(2,1)S(1)} %get-tuple-element.45), channel_id=1, source_target_pairs={{0,16},{8,24},{16,0},{24,8},{1,17},{9,25},{17,1},{25,9},{2,18},{10... | collective-permute-start | bytes 122888 | tf_op jit(solution)/shard_map/ppermute | solution.py:40
  15.6 4.9 %collective-permute-start.6 = (bf16[40,512]{1,0:T(8,128)(2,1)S(1)}, bf16[40,512]{1,0:T(8,128)(2,1)S(1)}, u32[]{:S(2)}, u32[]{:S(2)}) collective-permute-start(bf16[40,512]{1,0:T(8,128)(2,1)S(1)} %get-tuple-element.46), channel_id=1, source_target_pairs={{0,24},{8,16},{16,8},{24,0},{1,25},{9,17},{17,9},{25,1},{2,26},{10... | collective-permute-start | bytes 122888 | tf_op jit(solution)/shard_map/ppermute | solution.py:40
  20.5 1.4 %collective-permute-start.7 = (bf16[160,512]{1,0:T(8,128)(2,1)S(1)}, bf16[160,512]{1,0:T(8,128)(2,1)S(1)}, u32[]{:S(2)}, u32[]{:S(2)}) collective-permute-start(bf16[160,512]{1,0:T(8,128)(2,1)S(1)} %constant_dynamic-update-slice_fusion.refs_1_), channel_id=1, source_target_pairs={{0,1},{1,0},{2,3},{3,2},{4,5},{5,4},{6,7},{7,6},{8,9},{9,8},{10,11... | collective-permute-start | bytes 491528 | tf_op jit(solution)/shard_map/ppermute | solution.py:25
  21.9 7.4 %slice-start.1 = ((s8[5242880]{0:T(1024)(128)(4,1)}), s8[1048576]{0:T(1024)(128)(4,1)S(1)}, s32[]{:S(2)}) async-start(s8[5242880]{0:T(1024)(128)(4,1)} %bitcast.5), calls=%async_computation.1 | async-start | bytes 2097152
  22.0 7.4 %copy-start.13 = (f32[256]{0:T(256)S(1)}, f32[256]{0:T(256)}, u32[]{:S(2)}) copy-start(f32[256]{0:T(256)} %param.23) | copy-start | bytes 3076
  22.5 4.9 %collective-permute-start.8 = (bf16[40,1024]{1,0:T(8,128)(2,1)S(1)}, bf16[40,1024]{1,0:T(8,128)(2,1)S(1)}, u32[]{:S(2)}, u32[]{:S(2)}) collective-permute-start(bf16[40,1024]{1,0:T(8,128)(2,1)S(1)} %get-tuple-element.48), channel_id=1, source_target_pairs={{0,8},{8,0},{16,24},{24,16},{1,9},{9,1},{17,25},{25,17},{2,10},{10... | collective-permute-start | bytes 245768 | tf_op jit(solution)/shard_map/ppermute | solution.py:40
  23.1 6.2 %collective-permute-start.9 = (bf16[40,1024]{1,0:T(8,128)(2,1)S(1)}, bf16[40,1024]{1,0:T(8,128)(2,1)S(1)}, u32[]{:S(2)}, u32[]{:S(2)}) collective-permute-start(bf16[40,1024]{1,0:T(8,128)(2,1)S(1)} %get-tuple-element.49), channel_id=1, source_target_pairs={{0,16},{8,24},{16,0},{24,8},{1,17},{9,25},{17,1},{25,9},{2,18},{10... | collective-permute-start | bytes 245768 | tf_op jit(solution)/shard_map/ppermute | solution.py:40
  23.6 5.7 %collective-permute-start.10 = (bf16[40,1024]{1,0:T(8,128)(2,1)S(1)}, bf16[40,1024]{1,0:T(8,128)(2,1)S(1)}, u32[]{:S(2)}, u32[]{:S(2)}) collective-permute-start(bf16[40,1024]{1,0:T(8,128)(2,1)S(1)} %get-tuple-element.50), channel_id=1, source_target_pairs={{0,24},{8,16},{16,8},{24,0},{1,25},{9,17},{17,9},{25,1},{2,26},{10... | collective-permute-start | bytes 245768 | tf_op jit(solution)/shard_map/ppermute | solution.py:40
  26.1 1.2 %collective-permute-start.3 = (f32[40,128]{1,0:T(8,128)S(1)}, f32[40,128]{1,0:T(8,128)S(1)}, u32[]{:S(2)}, u32[]{:S(2)}) collective-permute-start(f32[40,128]{1,0:T(8,128)S(1)} %get-tuple-element.42.refs_0_), channel_id=1, source_target_pairs={{0,1},{1,0},{2,3},{3,2},{4,5},{5,4},{6,7},{7,6},{8,9},{9,8},{10,11... | collective-permute-start | bytes 61448 | tf_op jit(solution)/shard_map/ppermute | solution.py:25
  31.5 6.1 %collective-permute-start.11 = (bf16[40,256]{1,0:T(8,128)(2,1)S(1)}, bf16[40,256]{1,0:T(8,128)(2,1)S(1)}, u32[]{:S(2)}, u32[]{:S(2)}) collective-permute-start(bf16[40,256]{1,0:T(8,128)(2,1)S(1)} %get-tuple-element.54.refs_0_), channel_id=1, source_target_pairs={{0,2},{1,3},{2,0},{3,1},{4,6},{5,7},{6,4},{7,5},{8,10},{9,11},{10,... | collective-permute-start | bytes 61448 | tf_op jit(solution)/shard_map/ppermute | solution.py:32
  31.5 6.0 %collective-permute-start.12 = (bf16[40,256]{1,0:T(8,128)(2,1)S(1)}, bf16[40,256]{1,0:T(8,128)(2,1)S(1)}, u32[]{:S(2)}, u32[]{:S(2)}) collective-permute-start(bf16[40,256]{1,0:T(8,128)(2,1)S(1)} %get-tuple-element.54.refs_0_), channel_id=1, source_target_pairs={{0,4},{1,5},{2,6},{3,7},{4,0},{5,1},{6,2},{7,3},{8,12},{9,13},{10,... | collective-permute-start | bytes 61448 | tf_op jit(solution)/shard_map/ppermute | solution.py:32
  32.7 5.6 %collective-permute-start.13 = (bf16[40,256]{1,0:T(8,128)(2,1)S(1)}, bf16[40,256]{1,0:T(8,128)(2,1)S(1)}, u32[]{:S(2)}, u32[]{:S(2)}) collective-permute-start(bf16[40,256]{1,0:T(8,128)(2,1)S(1)} %get-tuple-element.54.refs_0_), channel_id=1, source_target_pairs={{0,6},{1,7},{2,4},{3,5},{4,2},{5,3},{6,0},{7,1},{8,14},{9,15},{10,... | collective-permute-start | bytes 61448 | tf_op jit(solution)/shard_map/ppermute | solution.py:32
  35.9 3.8 %copy-start.3 = (bf16[2048,512]{1,0:T(8,128)(2,1)S(1)}, bf16[2048,512]{1,0:T(8,128)(2,1)}, u32[]{:S(2)}) copy-start(bf16[2048,512]{1,0:T(8,128)(2,1)} %refs_4_.4) | copy-start | bytes 6291460
  38.3 1.4 %collective-permute-start.15 = (bf16[120,256]{1,0:T(8,128)(2,1)S(1)}, bf16[120,256]{1,0:T(8,128)(2,1)S(1)}, u32[]{:S(2)}, u32[]{:S(2)}) collective-permute-start(bf16[120,256]{1,0:T(8,128)(2,1)S(1)} %constant_dynamic-update-slice_fusion.4.refs_1_), channel_id=1, source_target_pairs={{0,1},{1,0},{2,3},{3,2},{4,5},{5,4},{6,7},{7,6},{8,9},{9,8},{10,11... | collective-permute-start | bytes 184328 | tf_op jit(solution)/shard_map/ppermute | solution.py:25
  38.4 1.3 %collective-permute-start.14 = (bf16[40,256]{1,0:T(8,128)(2,1)S(1)}, bf16[40,256]{1,0:T(8,128)(2,1)S(1)}, u32[]{:S(2)}, u32[]{:S(2)}) collective-permute-start(bf16[40,256]{1,0:T(8,128)(2,1)S(1)} %get-tuple-element.54.refs_0_), channel_id=1, source_target_pairs={{0,1},{1,0},{2,3},{3,2},{4,5},{5,4},{6,7},{7,6},{8,9},{9,8},{10,11... | collective-permute-start | bytes 61448 | tf_op jit(solution)/shard_map/ppermute | solution.py:25
  40.3 6.2 %collective-permute-start.16 = (bf16[10,640]{1,0:T(8,128)(2,1)S(1)}, bf16[10,640]{1,0:T(8,128)(2,1)S(1)}, u32[]{:S(2)}, u32[]{:S(2)}) collective-permute-start(bf16[10,640]{1,0:T(8,128)(2,1)S(1)} %get-tuple-element.67), channel_id=1, source_target_pairs={{0,8},{8,0},{16,24},{24,16},{1,9},{9,1},{17,25},{25,17},{2,10},{10... | collective-permute-start | bytes 38408 | tf_op jit(solution)/shard_map/ppermute | solution.py:40
  41.9 4.6 %collective-permute-start.17 = (bf16[10,640]{1,0:T(8,128)(2,1)S(1)}, bf16[10,640]{1,0:T(8,128)(2,1)S(1)}, u32[]{:S(2)}, u32[]{:S(2)}) collective-permute-start(bf16[10,640]{1,0:T(8,128)(2,1)S(1)} %get-tuple-element.68), channel_id=1, source_target_pairs={{0,16},{8,24},{16,0},{24,8},{1,17},{9,25},{17,1},{25,9},{2,18},{10... | collective-permute-start | bytes 38408 | tf_op jit(solution)/shard_map/ppermute | solution.py:40
  43.0 4.7 %collective-permute-start.18 = (bf16[10,640]{1,0:T(8,128)(2,1)S(1)}, bf16[10,640]{1,0:T(8,128)(2,1)S(1)}, u32[]{:S(2)}, u32[]{:S(2)}) collective-permute-start(bf16[10,640]{1,0:T(8,128)(2,1)S(1)} %get-tuple-element.69), channel_id=1, source_target_pairs={{0,24},{8,16},{16,8},{24,0},{1,25},{9,17},{17,9},{25,1},{2,26},{10... | collective-permute-start | bytes 38408 | tf_op jit(solution)/shard_map/ppermute | solution.py:40
  43.9 14.9 %copy-start = (bf16[2,4096,256]{2,1,0:T(8,128)(2,1)S(1)}, bf16[2,4096,256]{2,1,0:T(8,128)(2,1)}, u32[]{:S(2)}) copy-start(bf16[2,4096,256]{2,1,0:T(8,128)(2,1)} %refs_5_.5) | copy-start | bytes 12582916
  43.9 14.9 %copy-start.1 = (bf16[2,4096,256]{2,1,0:T(8,128)(2,1)S(1)}, bf16[2,4096,256]{2,1,0:T(8,128)(2,1)}, u32[]{:S(2)}) copy-start(bf16[2,4096,256]{2,1,0:T(8,128)(2,1)} %refs_6_.3) | copy-start | bytes 12582916
  43.9 15.0 %copy-start.10 = (f32[4096]{0:T(1024)S(1)}, f32[4096]{0:T(1024)}, u32[]{:S(2)}) copy-start(f32[4096]{0:T(1024)} %param.26) | copy-start | bytes 49156
  47.8 4.5 %collective-permute-start.19 = (bf16[40,512]{1,0:T(8,128)(2,1)S(1)}, bf16[40,512]{1,0:T(8,128)(2,1)S(1)}, u32[]{:S(2)}, u32[]{:S(2)}) collective-permute-start(bf16[40,512]{1,0:T(8,128)(2,1)S(1)} %pad_maximum_fusion.refs_0_), channel_id=1, source_target_pairs={{0,2},{1,3},{2,0},{3,1},{4,6},{5,7},{6,4},{7,5},{8,10},{9,11},{10,... | collective-permute-start | bytes 122888 | tf_op jit(solution)/shard_map/ppermute | solution.py:32
  47.9 5.7 %collective-permute-start.20 = (bf16[40,512]{1,0:T(8,128)(2,1)S(1)}, bf16[40,512]{1,0:T(8,128)(2,1)S(1)}, u32[]{:S(2)}, u32[]{:S(2)}) collective-permute-start(bf16[40,512]{1,0:T(8,128)(2,1)S(1)} %pad_maximum_fusion.refs_0_), channel_id=1, source_target_pairs={{0,4},{1,5},{2,6},{3,7},{4,0},{5,1},{6,2},{7,3},{8,12},{9,13},{10,... | collective-permute-start | bytes 122888 | tf_op jit(solution)/shard_map/ppermute | solution.py:32
  51.6 5.8 %collective-permute-start.21 = (bf16[40,512]{1,0:T(8,128)(2,1)S(1)}, bf16[40,512]{1,0:T(8,128)(2,1)S(1)}, u32[]{:S(2)}, u32[]{:S(2)}) collective-permute-start(bf16[40,512]{1,0:T(8,128)(2,1)S(1)} %pad_maximum_fusion.refs_0_), channel_id=1, source_target_pairs={{0,6},{1,7},{2,4},{3,5},{4,2},{5,3},{6,0},{7,1},{8,14},{9,15},{10,... | collective-permute-start | bytes 122888 | tf_op jit(solution)/shard_map/ppermute | solution.py:32
  57.4 1.4 %collective-permute-start.23 = (bf16[120,512]{1,0:T(8,128)(2,1)S(1)}, bf16[120,512]{1,0:T(8,128)(2,1)S(1)}, u32[]{:S(2)}, u32[]{:S(2)}) collective-permute-start(bf16[120,512]{1,0:T(8,128)(2,1)S(1)} %constant_dynamic-update-slice_fusion.7.refs_1_), channel_id=1, source_target_pairs={{0,1},{1,0},{2,3},{3,2},{4,5},{5,4},{6,7},{7,6},{8,9},{9,8},{10,11... | collective-permute-start | bytes 368648 | tf_op jit(solution)/shard_map/ppermute | solution.py:25
  57.4 1.4 %collective-permute-start.22 = (bf16[40,512]{1,0:T(8,128)(2,1)S(1)}, bf16[40,512]{1,0:T(8,128)(2,1)S(1)}, u32[]{:S(2)}, u32[]{:S(2)}) collective-permute-start(bf16[40,512]{1,0:T(8,128)(2,1)S(1)} %pad_maximum_fusion.refs_0_), channel_id=1, source_target_pairs={{0,1},{1,0},{2,3},{3,2},{4,5},{5,4},{6,7},{7,6},{8,9},{9,8},{10,11... | collective-permute-start | bytes 122888 | tf_op jit(solution)/shard_map/ppermute | solution.py:25
  58.8 10.2 %copy-start.2 = (bf16[2,2048,512]{2,1,0:T(8,128)(2,1)S(1)}, bf16[2,2048,512]{2,1,0:T(8,128)(2,1)}, u32[]{:S(2)}) copy-start(bf16[2,2048,512]{2,1,0:T(8,128)(2,1)} %refs_4_.5) | copy-start | bytes 12582916
  60.5 4.5 %collective-permute-start.24 = (bf16[2,40,256]{2,1,0:T(8,128)(2,1)S(1)}, bf16[2,40,256]{2,1,0:T(8,128)(2,1)S(1)}, u32[]{:S(2)}, u32[]{:S(2)}) collective-permute-start(bf16[2,40,256]{2,1,0:T(8,128)(2,1)S(1)} %lift.1.refs_0_), channel_id=1, source_target_pairs={{0,2},{1,3},{2,0},{3,1},{4,6},{5,7},{6,4},{7,5},{8,10},{9,11},{10,... | collective-permute-start | bytes 122888 | tf_op jit(solution)/shard_map/ppermute | solution.py:32
  60.6 7.0 %collective-permute-start.25 = (bf16[2,40,256]{2,1,0:T(8,128)(2,1)S(1)}, bf16[2,40,256]{2,1,0:T(8,128)(2,1)S(1)}, u32[]{:S(2)}, u32[]{:S(2)}) collective-permute-start(bf16[2,40,256]{2,1,0:T(8,128)(2,1)S(1)} %lift.1.refs_0_), channel_id=1, source_target_pairs={{0,4},{1,5},{2,6},{3,7},{4,0},{5,1},{6,2},{7,3},{8,12},{9,13},{10,... | collective-permute-start | bytes 122888 | tf_op jit(solution)/shard_map/ppermute | solution.py:32
  61.8 5.8 %collective-permute-start.26 = (bf16[2,40,256]{2,1,0:T(8,128)(2,1)S(1)}, bf16[2,40,256]{2,1,0:T(8,128)(2,1)S(1)}, u32[]{:S(2)}, u32[]{:S(2)}) collective-permute-start(bf16[2,40,256]{2,1,0:T(8,128)(2,1)S(1)} %lift.1.refs_0_), channel_id=1, source_target_pairs={{0,6},{1,7},{2,4},{3,5},{4,2},{5,3},{6,0},{7,1},{8,14},{9,15},{10,... | collective-permute-start | bytes 122888 | tf_op jit(solution)/shard_map/ppermute | solution.py:32
  67.6 1.5 %collective-permute-start.28 = (bf16[2,120,256]{2,1,0:T(8,128)(2,1)S(1)}, bf16[2,120,256]{2,1,0:T(8,128)(2,1)S(1)}, u32[]{:S(2)}, u32[]{:S(2)}) collective-permute-start(bf16[2,120,256]{2,1,0:T(8,128)(2,1)S(1)} %constant_dynamic-update-slice_fusion.10.refs_1_), channel_id=1, source_target_pairs={{0,1},{1,0},{2,3},{3,2},{4,5},{5,4},{6,7},{7,6},{8,9},{9,8},{10,11... | collective-permute-start | bytes 368648 | tf_op jit(solution)/shard_map/ppermute | solution.py:25
  67.7 1.4 %collective-permute-start.27 = (bf16[2,40,256]{2,1,0:T(8,128)(2,1)S(1)}, bf16[2,40,256]{2,1,0:T(8,128)(2,1)S(1)}, u32[]{:S(2)}, u32[]{:S(2)}) collective-permute-start(bf16[2,40,256]{2,1,0:T(8,128)(2,1)S(1)} %lift.1.refs_0_), channel_id=1, source_target_pairs={{0,1},{1,0},{2,3},{3,2},{4,5},{5,4},{6,7},{7,6},{8,9},{9,8},{10,11... | collective-permute-start | bytes 122888 | tf_op jit(solution)/shard_map/ppermute | solution.py:25
  69.9 3.8 %collective-permute-start.29 = (bf16[10,512]{1,0:T(8,128)(2,1)S(1)}, bf16[10,512]{1,0:T(8,128)(2,1)S(1)}, u32[]{:S(2)}, u32[]{:S(2)}) collective-permute-start(bf16[10,512]{1,0:T(8,128)(2,1)S(1)} %get-tuple-element.76), channel_id=1, source_target_pairs={{0,8},{8,0},{16,24},{24,16},{1,9},{9,1},{17,25},{25,17},{2,10},{10... | collective-permute-start | bytes 30728 | tf_op jit(solution)/shard_map/ppermute | solution.py:40
  70.4 3.7 %collective-permute-start.30 = (bf16[10,512]{1,0:T(8,128)(2,1)S(1)}, bf16[10,512]{1,0:T(8,128)(2,1)S(1)}, u32[]{:S(2)}, u32[]{:S(2)}) collective-permute-start(bf16[10,512]{1,0:T(8,128)(2,1)S(1)} %get-tuple-element.77), channel_id=1, source_target_pairs={{0,16},{8,24},{16,0},{24,8},{1,17},{9,25},{17,1},{25,9},{2,18},{10... | collective-permute-start | bytes 30728 | tf_op jit(solution)/shard_map/ppermute | solution.py:40
  71.4 4.6 %collective-permute-start.31 = (bf16[10,512]{1,0:T(8,128)(2,1)S(1)}, bf16[10,512]{1,0:T(8,128)(2,1)S(1)}, u32[]{:S(2)}, u32[]{:S(2)}) collective-permute-start(bf16[10,512]{1,0:T(8,128)(2,1)S(1)} %get-tuple-element.78), channel_id=1, source_target_pairs={{0,24},{8,16},{16,8},{24,0},{1,25},{9,17},{17,9},{25,1},{2,26},{10... | collective-permute-start | bytes 30728 | tf_op jit(solution)/shard_map/ppermute | solution.py:40
where the time goes:
time: 77 us; the launch traced here: 76.9 us
  starting transfers between devices  34.9 us (45%)
  waiting for transfers between devices  27.4 us (36%)
  Pallas kernels  11.2 us (15%)
  local copies, waits for them, and re-layouts  1.48 us (2%)
  other arithmetic  0.94 us (1%)
  between operations  0.9 us (1%)
    ppermute x12, starting transfers between devices, along_z(): lax.ppermute(array, 'tp', [(i, i ^ CORES * k) for i in range(size)])  19 us
    ppermute x12, starting transfers between devices, to_peers(): lax.ppermute(arrays[k], 'ep', [(i, i ^ k) for i in range(size)])  14.2 us
    ppermute x12, waiting for transfers between devices, along_z(): lax.ppermute(array, 'tp', [(i, i ^ CORES * k) for i in range(size)])  12 us
    ppermute x12, waiting for transfers between devices, to_peers(): lax.ppermute(arrays[k], 'ep', [(i, i ^ k) for i in range(size)])  10.2 us
    ppermute x8, waiting for transfers between devices, swap_cores(): return lax.ppermute(array, 'tp', [(i, i ^ 1) for i in range(size)])  5.2 us
    pallas_call x2, Pallas kernels, update_state(): pl.pallas_call(functools.partial(update_kernel, heads, first), grid=(last...  4.24 us
    pallas_call x1, Pallas kernels, read_state(): pl.pallas_call(functools.partial(read_kernel, len(parts), heads, width_mo...  2.12 us
    pallas_call x1, Pallas kernels, lift(): pl.pallas_call(functools.partial(lift_kernel, depth // pieces[0].shape[1]...  1.67 us
  transfers between devices with their start and end apart: 32, of which 20 were waited for; matrix products, arithmetic and copies ran while one was open for 1% of the time, Pallas kernels for 6%

commit v1 on v0

--- a/solution.py
+++ b/solution.py
@@ -139,78 +139,101 @@
     return outs[:peers], outs[peers:]
 
 
-def sort_kernel(count, *refs):
-    pieces = refs[:count]
-    outs = refs[-1 - count : -1]
-    squares_ref = refs[-1]
-    level = lax.axis_index("tp") // CORES
-    me = lax.axis_index("ep")
-    values = [piece[...] for piece in pieces]
-    for peer in range(count):
-        wanted = level ^ me ^ peer
-        chosen = values[0]
-        for number in range(1, count):
-            chosen = jnp.where(wanted == number, values[number], chosen)
-        outs[peer][...] = chosen
-    total = None
-    for value in values:
-        wide = value.astype(f32)
-        here = jnp.sum(wide * wide, axis=-1, keepdims=True)
-        total = here if total is None else total + here
-    squares_ref[...] = jnp.broadcast_to(total, squares_ref.shape)
-
-
-def sort_pieces(pieces, earlier):
-    rows, width = pieces[0].shape
-    count = len(pieces)
-    outs = pl.pallas_call(
-        functools.partial(sort_kernel, count),
-        out_shape=[near_shape((rows, width), bf16)] * count + [near_shape((rows, HEAD), f32)],
-        in_specs=[held()] * (count + len(earlier)),
-        out_specs=[held()] * (count + 1),
-        compiler_params=limit(4),
+def load_kernel(array_ref, out_ref):
+    out_ref[...] = array_ref[...]
+
+
+def load(array):
+    return pl.pallas_call(
+        load_kernel,
+        out_shape=near_shape(array.shape, array.dtype),
+        in_specs=[whole(array.shape)],
+        out_specs=held(),
+        compiler_params=limit(2),
         cost_estimate=cost(1),
-        name="sort",
-    )(*[near(array) for array in (*pieces, *earlier)])
-    return outs[:count], outs[count]
-
-
-def project_kernel(count, peers, rows, *refs):
-    gain_ref = refs[0]
-    parts = refs[1 : 1 + count]
-    weights = refs[1 + count : 5 + count]
-    outs = refs[5 + count :]
+        name="load",
+    )(array)
+
+
+def join_kernel(own_ref, other_ref, joined_ref):
+    width = own_ref.shape[1]
+    joined_ref[:, :width] = own_ref[...]
+    joined_ref[:, width:] = other_ref[...]
+
+
+def join(own, other):
+    rows, width = own.shape
+    return pl.pallas_call(
+        join_kernel,
+        out_shape=near_shape((rows, 2 * width), own.dtype),
+        in_specs=[held()] * 2,
+        out_specs=held(),
+        compiler_params=limit(2),
+        cost_estimate=cost(1),
+        name="join",
+    )(near(own), near(other))
+
+
+def turns_of(peers):
+    return [(peers - 1 - turn, turn) for turn in range(peers // CORES)]
+
+
+def project_kernel(peers, rows, gain_ref, *refs):
+    weights, outs, total_ref = refs[-5 - peers : -1 - peers], refs[-1 - peers : -1], refs[-1]
     slab, width = weights[0].shape
-    core = lax.axis_index("tp") % CORES
-    base = lax.axis_index("ep") * slab
-    totals = [None] * 4
-    for number in range(count):
-        part = parts[number]
-        span = part.shape[1]
-        place = (core ^ number) * span if count > 1 else 0
-        start = pl.multiple_of(place, 128)
-        gain = gain_ref[:, pl.ds(pl.multiple_of(base + place, 128), span)]
-        scaled = (part[...].astype(f32) * gain).astype(bf16)
+    me, rank = lax.axis_index("ep"), lax.axis_index("tp")
+    level, core = rank // CORES, rank % CORES
+    base = me * slab
+    direct = len(refs) > 6 + peers
+    halves = CORES if direct else 1
+    span = slab // halves
+    totals, squares = [None] * 4, None
+    for half in range(halves):
+        if direct:
+            one = refs[0][:, pl.ds(pl.multiple_of((core ^ half) * span, 128), span)]
+            two = refs[1][:, pl.ds(pl.multiple_of((1 - (core ^ half)) * span, 128), span)]
+            values = jnp.concatenate([one.astype(f32), two.astype(f32)], axis=0)
+        else:
+            values = refs[0][...].astype(f32)
+        here = jnp.sum(values * values, axis=-1, keepdims=True)
+        squares = here if half == 0 else squares + here
+        gain = gain_ref[:, pl.ds(pl.multiple_of(base + half * span, 128), span)]
+        scaled = (values * gain).astype(bf16)
         for which in range(4):
-            block = weights[which][pl.ds(start, span), :]
+            block = weights[which][half * span : (half + 1) * span, :]
             product = jnp.dot(scaled, block, preferred_element_type=f32)
-            totals[which] = product if totals[which] is None else totals[which] + product
+            totals[which] = product if half == 0 else totals[which] + product
+    for which in range(4):
+        total_ref[:, which * width : (which + 1) * width] = totals[which]
+    high = squares.astype(bf16).astype(f32)
+    mid = (squares - high).astype(bf16).astype(f32)
+    lane = lax.broadcasted_iota(jnp.int32, (squares.shape[0], HEAD), 1)
+    table = jnp.where(lane == 0, high, jnp.where(lane == 1, mid, 0.0))
+    total_ref[:, 4 * width :] = jnp.where(lane == 2, squares - high - mid, table)
     for peer in range(peers):
-        for which in range(4):
-            rows_here = totals[which][peer * rows : (peer + 1) * rows, :]
-            outs[peer][:, which * width : (which + 1) * width] = rows_here.astype(outs[peer].dtype)
+        place = peer
+        if direct:
+            wanted = level ^ me ^ peer
+            place = 0
+            for turn, pair in enumerate(turns_of(peers)):
+                for side in range(CORES):
+                    spot = turn + (side ^ core) * (peers // CORES)
+                    place = jnp.where(wanted == pair[side], spot, place)
+        chosen = total_ref[pl.ds(pl.multiple_of(place * rows, 8), rows), :]
+        outs[peer][...] = chosen.astype(outs[peer].dtype)
 
 
 def project(parts, gain, weights, peers, rows):
-    width = weights[0].shape[1]
-    out_shape = [near_shape((rows, 4 * width), f32)]
-    out_shape += [near_shape((rows, 4 * width), bf16)] * (peers - 1)
+    width = 4 * weights[0].shape[1] + HEAD
+    out_shape = [near_shape((rows, width), f32)]
+    out_shape += [near_shape((rows, width), bf16)] * (peers - 1)
     operands = [near(array) for array in (gain, *parts, *weights)]
     return pl.pallas_call(
-        functools.partial(project_kernel, len(parts), peers, rows),
+        functools.partial(project_kernel, peers, rows),
         out_shape=out_shape,
         in_specs=[held()] * len(operands),
         out_specs=[held()] * peers,
+        scratch_shapes=[pltpu.VMEM((peers * rows, width), f32)],
         compiler_params=limit(8),
         cost_estimate=cost(2),
         name="project",
@@ -237,13 +260,16 @@
 
 
 def read_kernel(peers, heads, width_model, *refs):
-    squares, cos_ref, sin_ref, gain_ref = refs[0:2], refs[2], refs[3], refs[4]
-    parts = refs[5 : 5 + peers]
-    state_ref = refs[5 + peers]
-    mixed_ref, key_ref, value_ref = refs[6 + peers : 9 + peers]
-    query_ref, read_ref = refs[9 + peers :]
+    cos_ref, sin_ref, gain_ref = refs[:3]
+    parts = refs[3 : 3 + peers]
+    state_ref = refs[3 + peers]
+    mixed_ref, key_ref, value_ref = refs[4 + peers : 7 + peers]
+    query_ref, read_ref = refs[7 + peers :]
     rows, width = mixed_ref.shape
-    mean = (squares[0][:, :1] + squares[1][:, :1]) * (1.0 / width_model)
+    squares = parts[0][:, 4 * width :]
+    for part in parts[1:]:
+        squares = squares + part[:, 4 * width :].astype(f32)
+    mean = jnp.sum(squares, axis=-1, keepdims=True) * (1.0 / width_model)
     factor = lax.rsqrt(mean + epsilon)
 
     def total(which):
@@ -297,10 +323,10 @@
         mixed_ref[:, cut] = (normal * gate[:, cut]).astype(bf16)
 
 
-def read_state(parts, squares, cosine, sine, head_gain, ret_state, width_model):
+def read_state(parts, cosine, sine, head_gain, ret_state, width_model):
     rows, heads = ret_state.shape[:2]
     width = heads * HEAD
-    operands = [near(a) for a in (*squares, cosine, sine, head_gain, *parts, ret_state)]
+    operands = [near(a) for a in (cosine, sine, head_gain, *parts, ret_state)]
     return pl.pallas_call(
         functools.partial(read_kernel, len(parts), heads, width_model),
         out_shape=[
@@ -554,6 +580,12 @@
     slots = local_experts * capacity
     if local_experts % group_size == 0:
         slots = slots // TOP
+    direct = ranks == CORES * peers
+    if direct:
+        joined = join(load(hidden), swap_cores(hidden))
+        positions, route_ids, route_weight, joined = lax.optimization_barrier(
+            (positions, route_ids, route_weight, joined)
+        )
     placing, shares = prepare(route_ids, route_weight, peers, local_experts, slots)
 
     inverse = 1.0 / rope_base ** (jnp.arange(0, HEAD, 2, dtype=f32) / HEAD)
@@ -562,16 +594,24 @@
     cosine = jnp.concatenate([cosine, cosine], axis=1)
     sine = jnp.concatenate([-sine, sine], axis=1)
 
-    if ranks == CORES * peers:
-        sorted_pieces, squares = sort_pieces(along_z(hidden), (shares[0], cosine, sine))
-        squares = [squares, swap_cores(squares)]
-        half = jnp.concatenate(to_peers(sorted_pieces), axis=0)
-        parts = [half, swap_cores(half)]
+    if direct:
+        came = []
+        for pair in turns_of(peers):
+            route = [
+                ((e * peers + z) * CORES + side, (z * peers + (e ^ pair[side])) * CORES + side)
+                for e in range(peers)
+                for z in range(peers)
+                for side in range(CORES)
+            ]
+            came.append(lax.ppermute(joined, ("ep", "tp"), route))
+        came, placing, shares, cosine, sine = lax.optimization_barrier(
+            (came, placing, shares, cosine, sine)
+        )
+        came = jnp.concatenate(came, axis=0)
+        parts = [came, swap_cores(came)]
     else:
         me = lax.axis_index("ep")
         full_rows = lax.all_gather(hidden, "tp", axis=1, tiled=True)
-        squares = jnp.sum(jnp.square(full_rows.astype(f32)), axis=1, keepdims=True)
-        squares = [squares, jnp.zeros_like(squares)]
         columns = lax.all_to_all(full_rows, "ep", split_axis=1, concat_axis=0, tiled=True)
         columns = columns.reshape(peers, own_rows, slab)
         parts = [columns[me ^ jnp.arange(peers)].reshape(peers * own_rows, slab)]
@@ -580,7 +620,7 @@
     sums = to_peers(partial)
 
     mixed, key, value = read_state(
-        sums, squares, cosine, sine, head_gain.reshape(1, width), ret_state, depth
+        sums, cosine, sine, head_gain.reshape(1, width), ret_state, depth
     )
     blocks = own_rows // 8
     split = max(1, 2 * blocks // 5)

time: 77 us -> 75 us (0.974)
  waiting for transfers between devices: 27.4 us -> 25.4 us
  starting transfers between devices: 34.9 us -> 36 us
    ppermute x0 -> x2, starting transfers between devices: none -> 8.4 us  [layer(): came.append(lax.ppermute(joined, ('ep', 'tp'), route))]
    ppermute x12 -> x9, starting transfers between devices: 19 us -> 13.3 us  [along_z(): lax.ppermute(array, 'tp', [(i, i ^ CORES * k) for i in range(size)])]
    ppermute x0 -> x2, waiting for transfers between devices: none -> 2.33 us  [layer(): came.append(lax.ppermute(joined, ('ep', 'tp'), route))]
    ppermute x12 -> x9, starting transfers between devices: 14.2 us -> 12.1 us  [to_peers(): lax.ppermute(arrays[k], 'ep', [(i, i ^ k) for i in range(size)])]
    ppermute x12 -> x9, waiting for transfers between devices: 12 us -> 9.87 us  [along_z(): lax.ppermute(array, 'tp', [(i, i ^ CORES * k) for i in range(size)])]
    ppermute x12 -> x9, waiting for transfers between devices: 10.2 us -> 8.91 us  [to_peers(): lax.ppermute(arrays[k], 'ep', [(i, i ^ k) for i in range(size)])]
    ppermute x8, waiting for transfers between devices: 5.2 us -> 4.25 us  [swap_cores(): return lax.ppermute(array, 'tp', [(i, i ^ 1) for i in range(size)])]
  transfers between devices with their start and end apart: 32 -> 28, of which waited for: 20 -> 17; matrix products, arithmetic and copies ran while one was open for 1% -> 0% of each run, Pallas kernels for 6% -> 6%
where the time goes in v1:
time: 75 us; the launch traced here: 74.7 us
  starting transfers between devices  36 us (48%)
  waiting for transfers between devices  25.4 us (34%)
  Pallas kernels  11.2 us (15%)
  between operations  0.94 us (1%)
  local copies, waits for them, and re-layouts  0.92 us (1%)
    ppermute x9, starting transfers between devices, along_z(): lax.ppermute(array, 'tp', [(i, i ^ CORES * k) for i in range(size)])  13.3 us
    ppermute x9, starting transfers between devices, to_peers(): lax.ppermute(arrays[k], 'ep', [(i, i ^ k) for i in range(size)])  12.1 us
    ppermute x9, waiting for transfers between devices, along_z(): lax.ppermute(array, 'tp', [(i, i ^ CORES * k) for i in range(size)])  9.87 us
    ppermute x9, waiting for transfers between devices, to_peers(): lax.ppermute(arrays[k], 'ep', [(i, i ^ k) for i in range(size)])  8.91 us
    ppermute x2, starting transfers between devices, layer(): came.append(lax.ppermute(joined, ('ep', 'tp'), route))  8.4 us
    ppermute x8, waiting for transfers between devices, swap_cores(): return lax.ppermute(array, 'tp', [(i, i ^ 1) for i in range(size)])  4.25 us
    pallas_call x2, Pallas kernels, update_state(): pl.pallas_call(functools.partial(update_kernel, heads, first), grid=(last...  4.24 us
    ppermute x2, waiting for transfers between devices, layer(): came.append(lax.ppermute(joined, ('ep', 'tp'), route))  2.33 us
  transfers between devices with their start and end apart: 28, of which 17 were waited for; matrix products, arithmetic and copies ran while one was open for 0% of the time, Pallas kernels for 6%

profile of v1, /device:TPU:0, one launch (start us, length us, event | category | flops | bytes accessed | tf_op | source)
XLA Modules:
  0.0 74.7 jit_solution(935464709137066025)
XLA Ops:
  0.6 0.6 collective-permute-start
  1.2 0.8 %copy-done.8 = bf16[40,512]{1,0:T(8,128)(2,1)S(1)} copy-done((bf16[40,512]{1,0:T(8,128)(2,1)S(1)}, bf16[40,512]{1,0:T(8,128)(2,1)}, u32[]{:S(2)}) %copy-start.8) | copy-done | bytes 40984
  2.0 0.0 copy-start.12
  2.0 0.0 copy-start.13
  2.0 0.3 collective-permute-done.other_ref
  2.3 6.8 %collective-permute-start.1 = (bf16[40,1024]{1,0:T(8,128)(2,1)S(1)}, bf16[40,1024]{1,0:T(8,128)(2,1)S(1)}, u32[]{:S(2)}, u32[]{:S(2)}) collective-permute-start(bf16[40,1024]{1,0:T(8,128)(2,1)S(1)} %join.1), channel_id=1, source_target_pairs={{0,6},{1,1},{2,14},{3,9},{4,22},{5,17},{6,30},{7,25},{8,4},{9,3},{... | collective-permute-start | bytes 245768 | tf_op jit(solution)/shard_map/ppermute | solution.py:606
  9.1 1.6 %collective-permute-start.2 = (bf16[40,1024]{1,0:T(8,128)(2,1)S(1)}, bf16[40,1024]{1,0:T(8,128)(2,1)S(1)}, u32[]{:S(2)}, u32[]{:S(2)}) collective-permute-start(bf16[40,1024]{1,0:T(8,128)(2,1)S(1)} %join.1), channel_id=1, source_target_pairs={{0,4},{1,3},{2,12},{3,11},{4,20},{5,19},{6,28},{7,27},{8,6},{9,1},... | collective-permute-start | bytes 245768 | tf_op jit(solution)/shard_map/ppermute | solution.py:606
  10.7 0.0 copy-start.4
  10.7 0.0 copy-start.5
  10.7 0.0 copy-start.6
  10.7 0.0 copy-start.7
  10.7 0.0 copy-start.10
  10.8 0.0 slice-start
  10.8 0.3 prepare.1
  11.0 0.2 fusion
  11.2 0.1 pad_maximum_fusion.1
  11.3 2.3 %collective-permute-done.2 = bf16[40,1024]{1,0:T(8,128)(2,1)S(1)} collective-permute-done((bf16[40,1024]{1,0:T(8,128)(2,1)S(1)}, bf16[40,1024]{1,0:T(8,128)(2,1)S(1)}, u32[]{:S(2)}, u32[]{:S(2)}) %collective-permute-start.2) | collective-permute-done | bytes 81952 | tf_op jit(solution)/shard_map/ppermute | solution.py:606
  13.6 0.1 collective-permute-start.3
  13.7 1.4 %collective-permute-done.3.refs_1_ = bf16[80,1024]{1,0:T(8,128)(2,1)S(1)} collective-permute-done((bf16[80,1024]{1,0:T(8,128)(2,1)S(1)}, bf16[80,1024]{1,0:T(8,128)(2,1)S(1)}, u32[]{:S(2)}, u32[]{:S(2)}) %collective-permute-start.3) | collective-permute-done | bytes 163872 | tf_op jit(solution)/shard_map/ppermute | solution.py:25
  15.1 0.0 copy-start.14
  15.1 0.6 project.1
  15.7 3.4 %collective-permute-start.4 = (bf16[40,1152]{1,0:T(8,128)(2,1)S(1)}, bf16[40,1152]{1,0:T(8,128)(2,1)S(1)}, u32[]{:S(2)}, u32[]{:S(2)}) collective-permute-start(bf16[40,1152]{1,0:T(8,128)(2,1)S(1)} %get-tuple-element.69), channel_id=1, source_target_pairs={{0,8},{8,0},{16,24},{24,16},{1,9},{9,1},{17,25},{25,17},{2,10},{10... | collective-permute-start | bytes 276488 | tf_op jit(solution)/shard_map/ppermute | solution.py:40
  19.2 0.6 collective-permute-start.5
  19.8 0.9 %collective-permute-start.6 = (bf16[40,1152]{1,0:T(8,128)(2,1)S(1)}, bf16[40,1152]{1,0:T(8,128)(2,1)S(1)}, u32[]{:S(2)}, u32[]{:S(2)}) collective-permute-start(bf16[40,1152]{1,0:T(8,128)(2,1)S(1)} %get-tuple-element.71), channel_id=1, source_target_pairs={{0,24},{8,16},{16,8},{24,0},{1,25},{9,17},{17,9},{25,1},{2,26},{10... | collective-permute-start | bytes 276488 | tf_op jit(solution)/shard_map/ppermute | solution.py:40
  20.7 1.4 %collective-permute-done.4.refs_4_ = bf16[40,1152]{1,0:T(8,128)(2,1)S(1)} collective-permute-done((bf16[40,1152]{1,0:T(8,128)(2,1)S(1)}, bf16[40,1152]{1,0:T(8,128)(2,1)S(1)}, u32[]{:S(2)}, u32[]{:S(2)}) %collective-permute-start.4) | collective-permute-done | bytes 92192 | tf_op jit(solution)/shard_map/ppermute | solution.py:40
  22.1 3.6 %collective-permute-done.5.refs_5_ = bf16[40,1152]{1,0:T(8,128)(2,1)S(1)} collective-permute-done((bf16[40,1152]{1,0:T(8,128)(2,1)S(1)}, bf16[40,1152]{1,0:T(8,128)(2,1)S(1)}, u32[]{:S(2)}, u32[]{:S(2)}) %collective-permute-start.5) | collective-permute-done | bytes 92192 | tf_op jit(solution)/shard_map/ppermute | solution.py:40
  25.7 2.1 %read_state.1 = (bf16[40,256]{1,0:T(8,128)(2,1)S(1)}, f32[40,256]{1,0:T(8,128)S(1)}, f32[40,256]{1,0:T(8,128)S(1)}) custom-call(f32[40,128]{1,0:T(8,128)S(1)} %get-tuple-element.64.refs_0_, f32[40,128]{1,0:T(8,128)S(1)} %get-tuple-element.65.refs_1_, f32[1,256]{1,0:T(1,128)S(1)} %bitcast.11, f32[40,1152]{1,0:T(8,128)S(1)} %get-tuple-element.68.refs_3_, ...), custom_call_target="tpu_custom_call" | custom-call | flops 5000000000 | bytes 30000000 | tf_op jit(solution)/shard_map/read_state/pallas_call | solution.py:330
  27.9 0.2 collective-permute-start.7
  28.1 2.4 %collective-permute-start.8 = (bf16[40,256]{1,0:T(8,128)(2,1)S(1)}, bf16[40,256]{1,0:T(8,128)(2,1)S(1)}, u32[]{:S(2)}, u32[]{:S(2)}) collective-permute-start(bf16[40,256]{1,0:T(8,128)(2,1)S(1)} %get-tuple-element.75.refs_0_), channel_id=1, source_target_pairs={{0,4},{1,5},{2,6},{3,7},{4,0},{5,1},{6,2},{7,3},{8,12},{9,13},{10,... | collective-permute-start | bytes 61448 | tf_op jit(solution)/shard_map/ppermute | solution.py:32
  30.5 1.8 %collective-permute-start.9 = (bf16[40,256]{1,0:T(8,128)(2,1)S(1)}, bf16[40,256]{1,0:T(8,128)(2,1)S(1)}, u32[]{:S(2)}, u32[]{:S(2)}) collective-permute-start(bf16[40,256]{1,0:T(8,128)(2,1)S(1)} %get-tuple-element.75.refs_0_), channel_id=1, source_target_pairs={{0,6},{1,7},{2,4},{3,5},{4,2},{5,3},{6,0},{7,1},{8,14},{9,15},{10,... | collective-permute-start | bytes 61448 | tf_op jit(solution)/shard_map/ppermute | solution.py:32
  32.3 1.6 %update_state.2.refs_4_ = f32[40,2,128,128]{3,2,1,0:T(8,128)} custom-call(f32[40,256]{1,0:T(8,128)S(1)} %get-tuple-element.73.refs_0_, f32[40,256]{1,0:T(8,128)S(1)} %get-tuple-element.74.refs_1_, f32[40,2,128,128]{3,2,1,0:T(8,128)S(1)} %bitcast.6), custom_call_target="tpu_custom_call" | custom-call | flops 5000000000 | bytes 30000000 | tf_op jit(solution)/shard_map/update_state/pallas_call | solution.py:374
  34.0 2.1 %collective-permute-done.9 = bf16[40,256]{1,0:T(8,128)(2,1)S(1)} collective-permute-done((bf16[40,256]{1,0:T(8,128)(2,1)S(1)}, bf16[40,256]{1,0:T(8,128)(2,1)S(1)}, u32[]{:S(2)}, u32[]{:S(2)}) %collective-permute-start.9) | collective-permute-done | bytes 20512 | tf_op jit(solution)/shard_map/ppermute | solution.py:32
  36.1 0.1 collective-permute-start.11
  36.2 0.5 collective-permute-start.10
  36.7 0.8 %collective-permute-done.10.refs_2_ = bf16[40,256]{1,0:T(8,128)(2,1)S(1)} collective-permute-done((bf16[40,256]{1,0:T(8,128)(2,1)S(1)}, bf16[40,256]{1,0:T(8,128)(2,1)S(1)}, u32[]{:S(2)}, u32[]{:S(2)}) %collective-permute-start.10) | collective-permute-done | bytes 20512 | tf_op jit(solution)/shard_map/ppermute | solution.py:25
  37.5 0.6 out_project.1
  38.1 1.7 %collective-permute-start.12 = (bf16[10,640]{1,0:T(8,128)(2,1)S(1)}, bf16[10,640]{1,0:T(8,128)(2,1)S(1)}, u32[]{:S(2)}, u32[]{:S(2)}) collective-permute-start(bf16[10,640]{1,0:T(8,128)(2,1)S(1)} %get-tuple-element.89), channel_id=1, source_target_pairs={{0,8},{8,0},{16,24},{24,16},{1,9},{9,1},{17,25},{25,17},{2,10},{10... | collective-permute-start | bytes 38408 | tf_op jit(solution)/shard_map/ppermute | solution.py:40
  39.9 1.1 %collective-permute-start.13 = (bf16[10,640]{1,0:T(8,128)(2,1)S(1)}, bf16[10,640]{1,0:T(8,128)(2,1)S(1)}, u32[]{:S(2)}, u32[]{:S(2)}) collective-permute-start(bf16[10,640]{1,0:T(8,128)(2,1)S(1)} %get-tuple-element.90), channel_id=1, source_target_pairs={{0,16},{8,24},{16,0},{24,8},{1,17},{9,25},{17,1},{25,9},{2,18},{10... | collective-permute-start | bytes 38408 | tf_op jit(solution)/shard_map/ppermute | solution.py:40
  40.9 0.7 %collective-permute-start.14 = (bf16[10,640]{1,0:T(8,128)(2,1)S(1)}, bf16[10,640]{1,0:T(8,128)(2,1)S(1)}, u32[]{:S(2)}, u32[]{:S(2)}) collective-permute-start(bf16[10,640]{1,0:T(8,128)(2,1)S(1)} %get-tuple-element.91), channel_id=1, source_target_pairs={{0,24},{8,16},{16,8},{24,0},{1,25},{9,17},{17,9},{25,1},{2,26},{10... | collective-permute-start | bytes 38408 | tf_op jit(solution)/shard_map/ppermute | solution.py:40
  41.7 2.6 %update_state.3 = f32[40,2,128,128]{3,2,1,0:T(8,128)} custom-call(f32[40,256]{1,0:T(8,128)S(1)} %get-tuple-element.73.refs_0_, f32[40,256]{1,0:T(8,128)S(1)} %get-tuple-element.74.refs_1_, f32[40,2,128,128]{3,2,1,0:T(8,128)S(1)} %bitcast.6, bf16[40,512]{1,0:T(8,128)(2,1)S(1)} %get-tuple-element.87.refs_3_.refs_0_, ...), custom_call_target="tpu_custom_call", output_to_operand_aliasing={{}: (4, {})} | custom-call | flops 5000000000 | bytes 30000000 | tf_op jit(solution)/shard_map/update_state/pallas_call | solution.py:374
  44.3 1.3 %collective-permute-done.14.refs_8_ = bf16[10,640]{1,0:T(8,128)(2,1)S(1)} collective-permute-done((bf16[10,640]{1,0:T(8,128)(2,1)S(1)}, bf16[10,640]{1,0:T(8,128)(2,1)S(1)}, u32[]{:S(2)}, u32[]{:S(2)}) %collective-permute-start.14) | collective-permute-done | bytes 12832 | tf_op jit(solution)/shard_map/ppermute | solution.py:40
  45.7 0.1 collective-permute-start.15
  45.8 1.2 %collective-permute-start.16 = (bf16[40,512]{1,0:T(8,128)(2,1)S(1)}, bf16[40,512]{1,0:T(8,128)(2,1)S(1)}, u32[]{:S(2)}, u32[]{:S(2)}) collective-permute-start(bf16[40,512]{1,0:T(8,128)(2,1)S(1)} %pad_maximum_fusion.refs_0_), channel_id=1, source_target_pairs={{0,4},{1,5},{2,6},{3,7},{4,0},{5,1},{6,2},{7,3},{8,12},{9,13},{10,... | collective-permute-start | bytes 122888 | tf_op jit(solution)/shard_map/ppermute | solution.py:32
  47.0 3.1 %collective-permute-start.17 = (bf16[40,512]{1,0:T(8,128)(2,1)S(1)}, bf16[40,512]{1,0:T(8,128)(2,1)S(1)}, u32[]{:S(2)}, u32[]{:S(2)}) collective-permute-start(bf16[40,512]{1,0:T(8,128)(2,1)S(1)} %pad_maximum_fusion.refs_0_), channel_id=1, source_target_pairs={{0,6},{1,7},{2,4},{3,5},{4,2},{5,3},{6,0},{7,1},{8,14},{9,15},{10,... | collective-permute-start | bytes 122888 | tf_op jit(solution)/shard_map/ppermute | solution.py:32
  50.1 0.9 %collective-permute-done.16 = bf16[40,512]{1,0:T(8,128)(2,1)S(1)} collective-permute-done((bf16[40,512]{1,0:T(8,128)(2,1)S(1)}, bf16[40,512]{1,0:T(8,128)(2,1)S(1)}, u32[]{:S(2)}, u32[]{:S(2)}) %collective-permute-start.16) | collective-permute-done | bytes 40992 | tf_op jit(solution)/shard_map/ppermute | solution.py:32
  51.1 1.7 %collective-permute-done.17 = bf16[40,512]{1,0:T(8,128)(2,1)S(1)} collective-permute-done((bf16[40,512]{1,0:T(8,128)(2,1)S(1)}, bf16[40,512]{1,0:T(8,128)(2,1)S(1)}, u32[]{:S(2)}, u32[]{:S(2)}) %collective-permute-start.17) | collective-permute-done | bytes 40992 | tf_op jit(solution)/shard_map/ppermute | solution.py:32
  52.8 0.5 collective-permute-start.18
  53.3 0.9 %collective-permute-done.18.refs_2_ = bf16[40,512]{1,0:T(8,128)(2,1)S(1)} collective-permute-done((bf16[40,512]{1,0:T(8,128)(2,1)S(1)}, bf16[40,512]{1,0:T(8,128)(2,1)S(1)}, u32[]{:S(2)}, u32[]{:S(2)}) %collective-permute-start.18) | collective-permute-done | bytes 40992 | tf_op jit(solution)/shard_map/ppermute | solution.py:25
  54.2 1.7 %lift.1.refs_0_ = bf16[2,40,256]{2,1,0:T(8,128)(2,1)S(1)} custom-call(bf16[40,512]{1,0:T(8,128)(2,1)S(1)} %pad_maximum_fusion.refs_0_, bf16[120,512]{1,0:T(8,128)(2,1)S(1)} %constant_dynamic-update-slice_fusion.5.refs_1_, bf16[40,512]{1,0:T(8,128)(2,1)S(1)} %collective-permute-done.18.refs_2_, bf16[120,512]{1,0:T(8,128)(2,1)S(1)} %collective-permute-done.19.refs_3_, ...), custom_call_target="tpu_custom_call" | custom-call | flops 7500000256 | bytes 45000000 | tf_op jit(solution)/shard_map/lift/pallas_call | solution.py:459
  55.9 0.1 collective-permute-start.20
  56.0 3.7 %collective-permute-start.21 = (bf16[2,40,256]{2,1,0:T(8,128)(2,1)S(1)}, bf16[2,40,256]{2,1,0:T(8,128)(2,1)S(1)}, u32[]{:S(2)}, u32[]{:S(2)}) collective-permute-start(bf16[2,40,256]{2,1,0:T(8,128)(2,1)S(1)} %lift.1.refs_0_), channel_id=1, source_target_pairs={{0,4},{1,5},{2,6},{3,7},{4,0},{5,1},{6,2},{7,3},{8,12},{9,13},{10,... | collective-permute-start | bytes 122888 | tf_op jit(solution)/shard_map/ppermute | solution.py:32
  59.7 0.7 collective-permute-start.22
  60.4 2.2 %collective-permute-done.21 = bf16[2,40,256]{2,1,0:T(8,128)(2,1)S(1)} collective-permute-done((bf16[2,40,256]{2,1,0:T(8,128)(2,1)S(1)}, bf16[2,40,256]{2,1,0:T(8,128)(2,1)S(1)}, u32[]{:S(2)}, u32[]{:S(2)}) %collective-permute-start.21) | collective-permute-done | bytes 40992 | tf_op jit(solution)/shard_map/ppermute | solution.py:32
  62.6 2.9 %collective-permute-done.22 = bf16[2,40,256]{2,1,0:T(8,128)(2,1)S(1)} collective-permute-done((bf16[2,40,256]{2,1,0:T(8,128)(2,1)S(1)}, bf16[2,40,256]{2,1,0:T(8,128)(2,1)S(1)}, u32[]{:S(2)}, u32[]{:S(2)}) %collective-permute-start.22) | collective-permute-done | bytes 40992 | tf_op jit(solution)/shard_map/ppermute | solution.py:32
  65.5 0.5 collective-permute-start.23
  66.0 0.9 %collective-permute-done.23.refs_2_ = bf16[2,40,256]{2,1,0:T(8,128)(2,1)S(1)} collective-permute-done((bf16[2,40,256]{2,1,0:T(8,128)(2,1)S(1)}, bf16[2,40,256]{2,1,0:T(8,128)(2,1)S(1)}, u32[]{:S(2)}, u32[]{:S(2)}) %collective-permute-start.23) | collective-permute-done | bytes 40992 | tf_op jit(solution)/shard_map/ppermute | solution.py:25
  66.9 0.9 %lower.1 = (bf16[10,512]{1,0:T(8,128)(2,1)S(1)}, bf16[10,512]{1,0:T(8,128)(2,1)S(1)}, bf16[10,512]{1,0:T(8,128)(2,1)S(1)}, bf16[10,512]{1,0:T(8,128)(2,1)S(1)}) custom-call(bf16[2,40,256]{2,1,0:T(8,128)(2,1)S(1)} %lift.1.refs_0_, bf16[2,120,256]{2,1,0:T(8,128)(2,1)S(1)} %constant_dynamic-update-slice_fusion.8.refs_1_, ...), custom_call_target="tpu_custom_call" | custom-call | flops 5000000000 | bytes 30000000 | tf_op jit(solution)/shard_map/lower/pallas_call | solution.py:507
  67.7 0.7 collective-permute-start.25
  68.5 0.8 %collective-permute-start.26 = (bf16[10,512]{1,0:T(8,128)(2,1)S(1)}, bf16[10,512]{1,0:T(8,128)(2,1)S(1)}, u32[]{:S(2)}, u32[]{:S(2)}) collective-permute-start(bf16[10,512]{1,0:T(8,128)(2,1)S(1)} %get-tuple-element.99), channel_id=1, source_target_pairs={{0,16},{8,24},{16,0},{24,8},{1,17},{9,25},{17,1},{25,9},{2,18},{10... | collective-permute-start | bytes 30728 | tf_op jit(solution)/shard_map/ppermute | solution.py:40
  69.3 2.0 %collective-permute-start.27 = (bf16[10,512]{1,0:T(8,128)(2,1)S(1)}, bf16[10,512]{1,0:T(8,128)(2,1)S(1)}, u32[]{:S(2)}, u32[]{:S(2)}) collective-permute-start(bf16[10,512]{1,0:T(8,128)(2,1)S(1)} %get-tuple-element.100), channel_id=1, source_target_pairs={{0,24},{8,16},{16,8},{24,0},{1,25},{9,17},{17,9},{25,1},{2,26},{10... | collective-permute-start | bytes 30728 | tf_op jit(solution)/shard_map/ppermute | solution.py:40
  71.3 0.2 collective-permute-done.25.refs_6_
  71.5 0.7 collective-permute-done.26.refs_7_
  72.2 1.7 %collective-permute-done.27.refs_8_ = bf16[10,512]{1,0:T(8,128)(2,1)S(1)} collective-permute-done((bf16[10,512]{1,0:T(8,128)(2,1)S(1)}, bf16[10,512]{1,0:T(8,128)(2,1)S(1)}, u32[]{:S(2)}, u32[]{:S(2)}) %collective-permute-start.27) | collective-permute-done | bytes 10272 | tf_op jit(solution)/shard_map/ppermute | solution.py:40
  73.9 0.9 %finish.1 = bf16[40,512]{1,0:T(8,128)(2,1)} custom-call(bf16[40,512]{1,0:T(8,128)(2,1)S(1)} %get-tuple-element.87.refs_3_.refs_0_, bf16[10,40]{1,0:T(8,128)(2,1)S(1)} %get-tuple-element.79.refs_6_.refs_1_, bf16[10,40]{1,0:T(8,128)(2,1)S(1)} %get-tuple-element.80.refs_7_.refs_2_, bf16[10,40]{1,0:T(8,128)(2,1)S(1)} %get-tuple-element.81.refs_8_.refs_3_, ...), custom_call_target="tpu_custom_call" | custom-call | flops 2500000000 | bytes 15000000 | tf_op jit(solution)/shard_map/finish/pallas_call | solution.py:537
  (60 shorter events, 0.2 us)
Async XLA Ops:
  0.6 1.6 %collective-permute-start = (bf16[40,512]{1,0:T(8,128)(2,1)}, bf16[40,512]{1,0:T(8,128)(2,1)S(1)}, u32[]{:S(2)}, u32[]{:S(2)}) collective-permute-start(bf16[40,512]{1,0:T(8,128)(2,1)} %refs_5_.4), channel_id=1, source_target_pairs={{0,1},{1,0},{2,3},{3,2},{4,5},{5,4},{6,7},{7,6},{8,9},{9,8},{10,11... | collective-permute-start | bytes 122888 | tf_op jit(solution)/shard_map/ppermute | solution.py:25
  1.2 0.8 %copy-start.8 = (bf16[40,512]{1,0:T(8,128)(2,1)S(1)}, bf16[40,512]{1,0:T(8,128)(2,1)}, u32[]{:S(2)}) copy-start(bf16[40,512]{1,0:T(8,128)(2,1)} %refs_5_.4) | copy-start | bytes 122884
  2.0 8.7 %copy-start.15 = (s32[40]{0:T(128)S(1)}, s32[40]{0:T(128)}, u32[]{:S(2)}) copy-start(s32[40]{0:T(128)} %param.17) | copy-start | bytes 484
  2.0 8.7 %copy-start.12 = (s32[40,2]{0,1:T(2,128)S(1)}, s32[40,2]{0,1:T(2,128)}, u32[]{:S(2)}) copy-start(s32[40,2]{0,1:T(2,128)} %param.30) | copy-start | bytes 964
  2.0 8.7 %copy-start.13 = (f32[40,2]{0,1:T(2,128)S(1)}, f32[40,2]{0,1:T(2,128)}, u32[]{:S(2)}) copy-start(f32[40,2]{0,1:T(2,128)} %param.31) | copy-start | bytes 964
  2.3 9.0 %collective-permute-start.1 = (bf16[40,1024]{1,0:T(8,128)(2,1)S(1)}, bf16[40,1024]{1,0:T(8,128)(2,1)S(1)}, u32[]{:S(2)}, u32[]{:S(2)}) collective-permute-start(bf16[40,1024]{1,0:T(8,128)(2,1)S(1)} %join.1), channel_id=1, source_target_pairs={{0,6},{1,1},{2,14},{3,9},{4,22},{5,17},{6,30},{7,25},{8,4},{9,3},{... | collective-permute-start | bytes 245768 | tf_op jit(solution)/shard_map/ppermute | solution.py:606
  9.1 4.5 %collective-permute-start.2 = (bf16[40,1024]{1,0:T(8,128)(2,1)S(1)}, bf16[40,1024]{1,0:T(8,128)(2,1)S(1)}, u32[]{:S(2)}, u32[]{:S(2)}) collective-permute-start(bf16[40,1024]{1,0:T(8,128)(2,1)S(1)} %join.1), channel_id=1, source_target_pairs={{0,4},{1,3},{2,12},{3,11},{4,20},{5,19},{6,28},{7,27},{8,6},{9,1},... | collective-permute-start | bytes 245768 | tf_op jit(solution)/shard_map/ppermute | solution.py:606
  10.7 4.4 %copy-start.4 = (bf16[1024,256]{1,0:T(8,128)(2,1)S(1)}, bf16[1024,256]{1,0:T(8,128)(2,1)}, u32[]{:S(2)}) copy-start(bf16[1024,256]{1,0:T(8,128)(2,1)} %refs_2_.3) | copy-start | bytes 1572868
  10.7 4.4 %copy-start.5 = (bf16[1024,256]{1,0:T(8,128)(2,1)S(1)}, bf16[1024,256]{1,0:T(8,128)(2,1)}, u32[]{:S(2)}) copy-start(bf16[1024,256]{1,0:T(8,128)(2,1)} %refs_3_.1) | copy-start | bytes 1572868
  10.7 4.4 %copy-start.6 = (bf16[1024,256]{1,0:T(8,128)(2,1)S(1)}, bf16[1024,256]{1,0:T(8,128)(2,1)}, u32[]{:S(2)}) copy-start(bf16[1024,256]{1,0:T(8,128)(2,1)} %refs_4_.3) | copy-start | bytes 1572868
  10.7 4.4 %copy-start.7 = (bf16[1024,256]{1,0:T(8,128)(2,1)S(1)}, bf16[1024,256]{1,0:T(8,128)(2,1)}, u32[]{:S(2)}) copy-start(bf16[1024,256]{1,0:T(8,128)(2,1)} %refs_5_.3) | copy-start | bytes 1572868
  10.7 4.4 %copy-start.10 = (f32[4096]{0:T(1024)S(1)}, f32[4096]{0:T(1024)}, u32[]{:S(2)}) copy-start(f32[4096]{0:T(1024)} %param.25) | copy-start | bytes 49156
  10.8 14.9 %slice-start = ((s8[5242880]{0:T(1024)(128)(4,1)}), s8[4194304]{0:T(1024)(128)(4,1)S(1)}, s32[]{:S(2)}) async-start(s8[5242880]{0:T(1024)(128)(4,1)} %bitcast.5), calls=%async_computation | async-start | bytes 8388608
  13.6 12.1 %slice-start.1 = ((s8[5242880]{0:T(1024)(128)(4,1)}), s8[1048576]{0:T(1024)(128)(4,1)S(1)}, s32[]{:S(2)}) async-start(s8[5242880]{0:T(1024)(128)(4,1)} %bitcast.5), calls=%async_computation.1 | async-start | bytes 2097152
  13.6 1.5 %collective-permute-start.3 = (bf16[80,1024]{1,0:T(8,128)(2,1)S(1)}, bf16[80,1024]{1,0:T(8,128)(2,1)S(1)}, u32[]{:S(2)}, u32[]{:S(2)}) collective-permute-start(bf16[80,1024]{1,0:T(8,128)(2,1)S(1)} %constant_dynamic-update-slice_fusion.refs_0_), channel_id=1, source_target_pairs={{0,1},{1,0},{2,3},{3,2},{4,5},{5,4},{6,7},{7,6},{8,9},{9,8},{10,11... | collective-permute-start | bytes 491528 | tf_op jit(solution)/shard_map/ppermute | solution.py:25
  15.1 10.6 %copy-start.14 = (f32[256]{0:T(256)S(1)}, f32[256]{0:T(256)}, u32[]{:S(2)}) copy-start(f32[256]{0:T(256)} %param.23) | copy-start | bytes 3076
  15.7 6.4 %collective-permute-start.4 = (bf16[40,1152]{1,0:T(8,128)(2,1)S(1)}, bf16[40,1152]{1,0:T(8,128)(2,1)S(1)}, u32[]{:S(2)}, u32[]{:S(2)}) collective-permute-start(bf16[40,1152]{1,0:T(8,128)(2,1)S(1)} %get-tuple-element.69), channel_id=1, source_target_pairs={{0,8},{8,0},{16,24},{24,16},{1,9},{9,1},{17,25},{25,17},{2,10},{10... | collective-permute-start | bytes 276488 | tf_op jit(solution)/shard_map/ppermute | solution.py:40
  19.2 6.5 %collective-permute-start.5 = (bf16[40,1152]{1,0:T(8,128)(2,1)S(1)}, bf16[40,1152]{1,0:T(8,128)(2,1)S(1)}, u32[]{:S(2)}, u32[]{:S(2)}) collective-permute-start(bf16[40,1152]{1,0:T(8,128)(2,1)S(1)} %get-tuple-element.70), channel_id=1, source_target_pairs={{0,16},{8,24},{16,0},{24,8},{1,17},{9,25},{17,1},{25,9},{2,18},{10... | collective-permute-start | bytes 276488 | tf_op jit(solution)/shard_map/ppermute | solution.py:40
  19.8 5.9 %collective-permute-start.6 = (bf16[40,1152]{1,0:T(8,128)(2,1)S(1)}, bf16[40,1152]{1,0:T(8,128)(2,1)S(1)}, u32[]{:S(2)}, u32[]{:S(2)}) collective-permute-start(bf16[40,1152]{1,0:T(8,128)(2,1)S(1)} %get-tuple-element.71), channel_id=1, source_target_pairs={{0,24},{8,16},{16,8},{24,0},{1,25},{9,17},{17,9},{25,1},{2,26},{10... | collective-permute-start | bytes 276488 | tf_op jit(solution)/shard_map/ppermute | solution.py:40
  27.9 6.1 %collective-permute-start.7 = (bf16[40,256]{1,0:T(8,128)(2,1)S(1)}, bf16[40,256]{1,0:T(8,128)(2,1)S(1)}, u32[]{:S(2)}, u32[]{:S(2)}) collective-permute-start(bf16[40,256]{1,0:T(8,128)(2,1)S(1)} %get-tuple-element.75.refs_0_), channel_id=1, source_target_pairs={{0,2},{1,3},{2,0},{3,1},{4,6},{5,7},{6,4},{7,5},{8,10},{9,11},{10,... | collective-permute-start | bytes 61448 | tf_op jit(solution)/shard_map/ppermute | solution.py:32
  28.1 5.9 %collective-permute-start.8 = (bf16[40,256]{1,0:T(8,128)(2,1)S(1)}, bf16[40,256]{1,0:T(8,128)(2,1)S(1)}, u32[]{:S(2)}, u32[]{:S(2)}) collective-permute-start(bf16[40,256]{1,0:T(8,128)(2,1)S(1)} %get-tuple-element.75.refs_0_), channel_id=1, source_target_pairs={{0,4},{1,5},{2,6},{3,7},{4,0},{5,1},{6,2},{7,3},{8,12},{9,13},{10,... | collective-permute-start | bytes 61448 | tf_op jit(solution)/shard_map/ppermute | solution.py:32
  30.5 5.6 %collective-permute-start.9 = (bf16[40,256]{1,0:T(8,128)(2,1)S(1)}, bf16[40,256]{1,0:T(8,128)(2,1)S(1)}, u32[]{:S(2)}, u32[]{:S(2)}) collective-permute-start(bf16[40,256]{1,0:T(8,128)(2,1)S(1)} %get-tuple-element.75.refs_0_), channel_id=1, source_target_pairs={{0,6},{1,7},{2,4},{3,5},{4,2},{5,3},{6,0},{7,1},{8,14},{9,15},{10,... | collective-permute-start | bytes 61448 | tf_op jit(solution)/shard_map/ppermute | solution.py:32
  32.3 5.2 %copy-start.3 = (bf16[2048,512]{1,0:T(8,128)(2,1)S(1)}, bf16[2048,512]{1,0:T(8,128)(2,1)}, u32[]{:S(2)}) copy-start(bf16[2048,512]{1,0:T(8,128)(2,1)} %refs_4_.4) | copy-start | bytes 6291460
  32.3 5.2 %copy-start.9 = (bf16[40,512]{1,0:T(8,128)(2,1)S(1)}, bf16[40,512]{1,0:T(8,128)(2,1)}, u32[]{:S(2)}) copy-start(bf16[40,512]{1,0:T(8,128)(2,1)} %refs_5_.4) | copy-start | bytes 122884
  36.1 1.4 %collective-permute-start.11 = (bf16[120,256]{1,0:T(8,128)(2,1)S(1)}, bf16[120,256]{1,0:T(8,128)(2,1)S(1)}, u32[]{:S(2)}, u32[]{:S(2)}) collective-permute-start(bf16[120,256]{1,0:T(8,128)(2,1)S(1)} %constant_dynamic-update-slice_fusion.2.refs_1_), channel_id=1, source_target_pairs={{0,1},{1,0},{2,3},{3,2},{4,5},{5,4},{6,7},{7,6},{8,9},{9,8},{10,11... | collective-permute-start | bytes 184328 | tf_op jit(solution)/shard_map/ppermute | solution.py:25
  36.2 1.3 %collective-permute-start.10 = (bf16[40,256]{1,0:T(8,128)(2,1)S(1)}, bf16[40,256]{1,0:T(8,128)(2,1)S(1)}, u32[]{:S(2)}, u32[]{:S(2)}) collective-permute-start(bf16[40,256]{1,0:T(8,128)(2,1)S(1)} %get-tuple-element.75.refs_0_), channel_id=1, source_target_pairs={{0,1},{1,0},{2,3},{3,2},{4,5},{5,4},{6,7},{7,6},{8,9},{9,8},{10,11... | collective-permute-start | bytes 61448 | tf_op jit(solution)/shard_map/ppermute | solution.py:25
  38.1 6.2 %collective-permute-start.12 = (bf16[10,640]{1,0:T(8,128)(2,1)S(1)}, bf16[10,640]{1,0:T(8,128)(2,1)S(1)}, u32[]{:S(2)}, u32[]{:S(2)}) collective-permute-start(bf16[10,640]{1,0:T(8,128)(2,1)S(1)} %get-tuple-element.89), channel_id=1, source_target_pairs={{0,8},{8,0},{16,24},{24,16},{1,9},{9,1},{17,25},{25,17},{2,10},{10... | collective-permute-start | bytes 38408 | tf_op jit(solution)/shard_map/ppermute | solution.py:40
  39.9 4.4 %collective-permute-start.13 = (bf16[10,640]{1,0:T(8,128)(2,1)S(1)}, bf16[10,640]{1,0:T(8,128)(2,1)S(1)}, u32[]{:S(2)}, u32[]{:S(2)}) collective-permute-start(bf16[10,640]{1,0:T(8,128)(2,1)S(1)} %get-tuple-element.90), channel_id=1, source_target_pairs={{0,16},{8,24},{16,0},{24,8},{1,17},{9,25},{17,1},{25,9},{2,18},{10... | collective-permute-start | bytes 38408 | tf_op jit(solution)/shard_map/ppermute | solution.py:40
  40.9 4.7 %collective-permute-start.14 = (bf16[10,640]{1,0:T(8,128)(2,1)S(1)}, bf16[10,640]{1,0:T(8,128)(2,1)S(1)}, u32[]{:S(2)}, u32[]{:S(2)}) collective-permute-start(bf16[10,640]{1,0:T(8,128)(2,1)S(1)} %get-tuple-element.91), channel_id=1, source_target_pairs={{0,24},{8,16},{16,8},{24,0},{1,25},{9,17},{17,9},{25,1},{2,26},{10... | collective-permute-start | bytes 38408 | tf_op jit(solution)/shard_map/ppermute | solution.py:40
  41.7 12.5 %copy-start = (bf16[2,4096,256]{2,1,0:T(8,128)(2,1)S(1)}, bf16[2,4096,256]{2,1,0:T(8,128)(2,1)}, u32[]{:S(2)}) copy-start(bf16[2,4096,256]{2,1,0:T(8,128)(2,1)} %refs_5_.5) | copy-start | bytes 12582916
  41.7 12.5 %copy-start.1 = (bf16[2,4096,256]{2,1,0:T(8,128)(2,1)S(1)}, bf16[2,4096,256]{2,1,0:T(8,128)(2,1)}, u32[]{:S(2)}) copy-start(bf16[2,4096,256]{2,1,0:T(8,128)(2,1)} %refs_6_.1) | copy-start | bytes 12582916
  41.7 12.5 %copy-start.11 = (f32[4096]{0:T(1024)S(1)}, f32[4096]{0:T(1024)}, u32[]{:S(2)}) copy-start(f32[4096]{0:T(1024)} %param.26) | copy-start | bytes 49156
  45.7 4.5 %collective-permute-start.15 = (bf16[40,512]{1,0:T(8,128)(2,1)S(1)}, bf16[40,512]{1,0:T(8,128)(2,1)S(1)}, u32[]{:S(2)}, u32[]{:S(2)}) collective-permute-start(bf16[40,512]{1,0:T(8,128)(2,1)S(1)} %pad_maximum_fusion.refs_0_), channel_id=1, source_target_pairs={{0,2},{1,3},{2,0},{3,1},{4,6},{5,7},{6,4},{7,5},{8,10},{9,11},{10,... | collective-permute-start | bytes 122888 | tf_op jit(solution)/shard_map/ppermute | solution.py:32
  45.8 5.3 %collective-permute-start.16 = (bf16[40,512]{1,0:T(8,128)(2,1)S(1)}, bf16[40,512]{1,0:T(8,128)(2,1)S(1)}, u32[]{:S(2)}, u32[]{:S(2)}) collective-permute-start(bf16[40,512]{1,0:T(8,128)(2,1)S(1)} %pad_maximum_fusion.refs_0_), channel_id=1, source_target_pairs={{0,4},{1,5},{2,6},{3,7},{4,0},{5,1},{6,2},{7,3},{8,12},{9,13},{10,... | collective-permute-start | bytes 122888 | tf_op jit(solution)/shard_map/ppermute | solution.py:32
  47.0 5.8 %collective-permute-start.17 = (bf16[40,512]{1,0:T(8,128)(2,1)S(1)}, bf16[40,512]{1,0:T(8,128)(2,1)S(1)}, u32[]{:S(2)}, u32[]{:S(2)}) collective-permute-start(bf16[40,512]{1,0:T(8,128)(2,1)S(1)} %pad_maximum_fusion.refs_0_), channel_id=1, source_target_pairs={{0,6},{1,7},{2,4},{3,5},{4,2},{5,3},{6,0},{7,1},{8,14},{9,15},{10,... | collective-permute-start | bytes 122888 | tf_op jit(solution)/shard_map/ppermute | solution.py:32
  52.8 1.4 %collective-permute-start.19 = (bf16[120,512]{1,0:T(8,128)(2,1)S(1)}, bf16[120,512]{1,0:T(8,128)(2,1)S(1)}, u32[]{:S(2)}, u32[]{:S(2)}) collective-permute-start(bf16[120,512]{1,0:T(8,128)(2,1)S(1)} %constant_dynamic-update-slice_fusion.5.refs_1_), channel_id=1, source_target_pairs={{0,1},{1,0},{2,3},{3,2},{4,5},{5,4},{6,7},{7,6},{8,9},{9,8},{10,11... | collective-permute-start | bytes 368648 | tf_op jit(solution)/shard_map/ppermute | solution.py:25
  52.8 1.4 %collective-permute-start.18 = (bf16[40,512]{1,0:T(8,128)(2,1)S(1)}, bf16[40,512]{1,0:T(8,128)(2,1)S(1)}, u32[]{:S(2)}, u32[]{:S(2)}) collective-permute-start(bf16[40,512]{1,0:T(8,128)(2,1)S(1)} %pad_maximum_fusion.refs_0_), channel_id=1, source_target_pairs={{0,1},{1,0},{2,3},{3,2},{4,5},{5,4},{6,7},{7,6},{8,9},{9,8},{10,11... | collective-permute-start | bytes 122888 | tf_op jit(solution)/shard_map/ppermute | solution.py:25
  54.2 12.7 %copy-start.2 = (bf16[2,2048,512]{2,1,0:T(8,128)(2,1)S(1)}, bf16[2,2048,512]{2,1,0:T(8,128)(2,1)}, u32[]{:S(2)}) copy-start(bf16[2,2048,512]{2,1,0:T(8,128)(2,1)} %refs_4_.5) | copy-start | bytes 12582916
  55.9 4.5 %collective-permute-start.20 = (bf16[2,40,256]{2,1,0:T(8,128)(2,1)S(1)}, bf16[2,40,256]{2,1,0:T(8,128)(2,1)S(1)}, u32[]{:S(2)}, u32[]{:S(2)}) collective-permute-start(bf16[2,40,256]{2,1,0:T(8,128)(2,1)S(1)} %lift.1.refs_0_), channel_id=1, source_target_pairs={{0,2},{1,3},{2,0},{3,1},{4,6},{5,7},{6,4},{7,5},{8,10},{9,11},{10,... | collective-permute-start | bytes 122888 | tf_op jit(solution)/shard_map/ppermute | solution.py:32
  56.0 6.6 %collective-permute-start.21 = (bf16[2,40,256]{2,1,0:T(8,128)(2,1)S(1)}, bf16[2,40,256]{2,1,0:T(8,128)(2,1)S(1)}, u32[]{:S(2)}, u32[]{:S(2)}) collective-permute-start(bf16[2,40,256]{2,1,0:T(8,128)(2,1)S(1)} %lift.1.refs_0_), channel_id=1, source_target_pairs={{0,4},{1,5},{2,6},{3,7},{4,0},{5,1},{6,2},{7,3},{8,12},{9,13},{10,... | collective-permute-start | bytes 122888 | tf_op jit(solution)/shard_map/ppermute | solution.py:32
  59.7 5.8 %collective-permute-start.22 = (bf16[2,40,256]{2,1,0:T(8,128)(2,1)S(1)}, bf16[2,40,256]{2,1,0:T(8,128)(2,1)S(1)}, u32[]{:S(2)}, u32[]{:S(2)}) collective-permute-start(bf16[2,40,256]{2,1,0:T(8,128)(2,1)S(1)} %lift.1.refs_0_), channel_id=1, source_target_pairs={{0,6},{1,7},{2,4},{3,5},{4,2},{5,3},{6,0},{7,1},{8,14},{9,15},{10,... | collective-permute-start | bytes 122888 | tf_op jit(solution)/shard_map/ppermute | solution.py:32
  65.5 1.4 %collective-permute-start.24 = (bf16[2,120,256]{2,1,0:T(8,128)(2,1)S(1)}, bf16[2,120,256]{2,1,0:T(8,128)(2,1)S(1)}, u32[]{:S(2)}, u32[]{:S(2)}) collective-permute-start(bf16[2,120,256]{2,1,0:T(8,128)(2,1)S(1)} %constant_dynamic-update-slice_fusion.8.refs_1_), channel_id=1, source_target_pairs={{0,1},{1,0},{2,3},{3,2},{4,5},{5,4},{6,7},{7,6},{8,9},{9,8},{10,11... | collective-permute-start | bytes 368648 | tf_op jit(solution)/shard_map/ppermute | solution.py:25
  65.5 1.4 %collective-permute-start.23 = (bf16[2,40,256]{2,1,0:T(8,128)(2,1)S(1)}, bf16[2,40,256]{2,1,0:T(8,128)(2,1)S(1)}, u32[]{:S(2)}, u32[]{:S(2)}) collective-permute-start(bf16[2,40,256]{2,1,0:T(8,128)(2,1)S(1)} %lift.1.refs_0_), channel_id=1, source_target_pairs={{0,1},{1,0},{2,3},{3,2},{4,5},{5,4},{6,7},{7,6},{8,9},{9,8},{10,11... | collective-permute-start | bytes 122888 | tf_op jit(solution)/shard_map/ppermute | solution.py:25
  67.7 3.8 %collective-permute-start.25 = (bf16[10,512]{1,0:T(8,128)(2,1)S(1)}, bf16[10,512]{1,0:T(8,128)(2,1)S(1)}, u32[]{:S(2)}, u32[]{:S(2)}) collective-permute-start(bf16[10,512]{1,0:T(8,128)(2,1)S(1)} %get-tuple-element.98), channel_id=1, source_target_pairs={{0,8},{8,0},{16,24},{24,16},{1,9},{9,1},{17,25},{25,17},{2,10},{10... | collective-permute-start | bytes 30728 | tf_op jit(solution)/shard_map/ppermute | solution.py:40
  68.5 3.7 %collective-permute-start.26 = (bf16[10,512]{1,0:T(8,128)(2,1)S(1)}, bf16[10,512]{1,0:T(8,128)(2,1)S(1)}, u32[]{:S(2)}, u32[]{:S(2)}) collective-permute-start(bf16[10,512]{1,0:T(8,128)(2,1)S(1)} %get-tuple-element.99), channel_id=1, source_target_pairs={{0,16},{8,24},{16,0},{24,8},{1,17},{9,25},{17,1},{25,9},{2,18},{10... | collective-permute-start | bytes 30728 | tf_op jit(solution)/shard_map/ppermute | solution.py:40
  69.3 4.6 %collective-permute-start.27 = (bf16[10,512]{1,0:T(8,128)(2,1)S(1)}, bf16[10,512]{1,0:T(8,128)(2,1)S(1)}, u32[]{:S(2)}, u32[]{:S(2)}) collective-permute-start(bf16[10,512]{1,0:T(8,128)(2,1)S(1)} %get-tuple-element.100), channel_id=1, source_target_pairs={{0,24},{8,16},{16,8},{24,0},{1,25},{9,17},{17,9},{25,1},{2,26},{10... | collective-permute-start | bytes 30728 | tf_op jit(solution)/shard_map/ppermute | solution.py:40

commit v2 on v1

--- a/solution.py
+++ b/solution.py
@@ -175,7 +175,7 @@
 
 
 def turns_of(peers):
-    return [(peers - 1 - turn, turn) for turn in range(peers // CORES)]
+    return [(peers - 1 - turn, turn) for turn in reversed(range(peers // CORES))]
 
 
 def project_kernel(peers, rows, gain_ref, *refs):
@@ -246,10 +246,14 @@
     return (lane // HEAD == row).astype(f32)
 
 
-def columns_times(rows, table):
+def split_of(rows):
     high = rows.astype(bf16).astype(f32)
     mid = (rows - high).astype(bf16).astype(f32)
-    split = jnp.concatenate([high, mid, rows - high - mid], axis=0).astype(bf16)
+    return jnp.concatenate([high, mid, rows - high - mid], axis=0).astype(bf16)
+
+
+def columns_times(rows, table):
+    split = split_of(rows)
     return lax.dot_general(split, table, (((0,), (0,)), ((), ())), preferred_element_type=f32)
 
 
@@ -294,26 +298,27 @@
         key_ref[:, cut] = two
         own.append(jnp.sum(one * two, axis=-1, keepdims=True) * value[:, cut])
     block = 8
-    mask = blocks_of(block)
-    ones = jnp.concatenate([mask] * 3, axis=0).astype(bf16)
+    line = lax.broadcasted_iota(jnp.int32, (block, HEAD), 0)
 
     def some(number, carry):
         start = pl.multiple_of(number * block, block)
         for head in range(heads):
             cut = slice(head * HEAD, (head + 1) * HEAD)
-            spread = columns_times(query_ref[pl.ds(start, block), cut], ones)
-            found = [
-                jnp.sum(
-                    spread[:, row * HEAD : (row + 1) * HEAD] * state_ref[start + row, head],
-                    axis=0,
-                    keepdims=True,
-                )
-                for row in range(block)
-            ]
-            read_ref[pl.ds(start, block), cut] = jnp.concatenate(found, axis=0)
+            split = split_of(query_ref[pl.ds(start, block), cut])
+            split = jnp.concatenate([split, split], axis=1)
+            found = jnp.zeros((block, HEAD), f32)
+            for row in range(block):
+                state = state_ref[start + row, head]
+                high = state.astype(bf16)
+                low = (state - high.astype(f32)).astype(bf16)
+                both = jnp.concatenate([high, low], axis=0)
+                part = jnp.dot(split, both, preferred_element_type=f32)
+                part = part[:block] + part[block : 2 * block] + part[2 * block :]
+                found = jnp.where(line == row, part, found)
+            read_ref[pl.ds(start, block), cut] = found
         return carry
 
-    lax.fori_loop(0, rows // block, some, 0)
+    lax.fori_loop(0, rows // block, some, 0, unroll=True)
     for head in range(heads):
         cut = slice(head * HEAD, (head + 1) * HEAD)
         read = decay_of(head, heads) * read_ref[:, cut] + own[head]

time: 75 us -> 73.1 us (0.975)
  waiting for transfers between devices: 25.4 us -> 24.3 us
  Pallas kernels: 11.2 us -> 10.3 us
    pallas_call x1, Pallas kernels: 2.13 us -> 1.18 us  [read_state(): pl.pallas_call(functools.partial(read_kernel, len(parts), heads, width_mo...]
    ppermute x2, starting transfers between devices: 8.4 us -> 9.16 us  [layer(): came.append(lax.ppermute(joined, ('ep', 'tp'), route))]
where the time goes in v2:
time: 73.1 us; the launch traced here: 72.9 us
  starting transfers between devices  36.1 us (49%)
  waiting for transfers between devices  24.3 us (33%)
  Pallas kernels  10.3 us (14%)
  between operations  0.96 us (1%)
  local copies, waits for them, and re-layouts  0.92 us (1%)
    ppermute x9, starting transfers between devices, along_z(): lax.ppermute(array, 'tp', [(i, i ^ CORES * k) for i in range(size)])  13.3 us
    ppermute x9, starting transfers between devices, to_peers(): lax.ppermute(arrays[k], 'ep', [(i, i ^ k) for i in range(size)])  11.5 us
    ppermute x9, waiting for transfers between devices, along_z(): lax.ppermute(array, 'tp', [(i, i ^ CORES * k) for i in range(size)])  9.61 us
    ppermute x2, starting transfers between devices, layer(): came.append(lax.ppermute(joined, ('ep', 'tp'), route))  9.16 us
    ppermute x9, waiting for transfers between devices, to_peers(): lax.ppermute(arrays[k], 'ep', [(i, i ^ k) for i in range(size)])  8.77 us
    ppermute x8, waiting for transfers between devices, swap_cores(): return lax.ppermute(array, 'tp', [(i, i ^ 1) for i in range(size)])  4.25 us
    pallas_call x2, Pallas kernels, update_state(): pl.pallas_call(functools.partial(update_kernel, heads, first), grid=(last...  4.25 us
    ppermute x8, starting transfers between devices, swap_cores(): return lax.ppermute(array, 'tp', [(i, i ^ 1) for i in range(size)])  2.22 us
  transfers between devices with their start and end apart: 28, of which 17 were waited for; matrix products, arithmetic and copies ran while one was open for 0% of the time, Pallas kernels for 6%

profile of v2, /device:TPU:0, one launch (start us, length us, event | category | flops | bytes accessed | tf_op | source)
XLA Modules:
  0.0 72.9 jit_solution(13124047484306274946)
XLA Ops:
  0.6 0.6 collective-permute-start
  1.2 0.8 %copy-done.8 = bf16[40,512]{1,0:T(8,128)(2,1)S(1)} copy-done((bf16[40,512]{1,0:T(8,128)(2,1)S(1)}, bf16[40,512]{1,0:T(8,128)(2,1)}, u32[]{:S(2)}) %copy-start.8) | copy-done | bytes 40984
  2.0 0.0 copy-start.12
  2.0 0.0 copy-start.13
  2.0 0.3 collective-permute-done.other_ref
  2.3 3.9 %collective-permute-start.1 = (bf16[40,1024]{1,0:T(8,128)(2,1)S(1)}, bf16[40,1024]{1,0:T(8,128)(2,1)S(1)}, u32[]{:S(2)}, u32[]{:S(2)}) collective-permute-start(bf16[40,1024]{1,0:T(8,128)(2,1)S(1)} %join.1), channel_id=1, source_target_pairs={{0,4},{1,3},{2,12},{3,11},{4,20},{5,19},{6,28},{7,27},{8,6},{9,1},... | collective-permute-start | bytes 245768 | tf_op jit(solution)/shard_map/ppermute | solution.py:611
  6.2 5.2 %collective-permute-start.2 = (bf16[40,1024]{1,0:T(8,128)(2,1)S(1)}, bf16[40,1024]{1,0:T(8,128)(2,1)S(1)}, u32[]{:S(2)}, u32[]{:S(2)}) collective-permute-start(bf16[40,1024]{1,0:T(8,128)(2,1)S(1)} %join.1), channel_id=1, source_target_pairs={{0,6},{1,1},{2,14},{3,9},{4,22},{5,17},{6,30},{7,25},{8,4},{9,3},{... | collective-permute-start | bytes 245768 | tf_op jit(solution)/shard_map/ppermute | solution.py:611
  11.5 0.0 copy-start.4
  11.5 0.0 copy-start.5
  11.5 0.0 copy-start.7
  11.5 0.0 copy-start.10
  11.5 0.0 slice-start
  11.6 0.3 prepare.1
  11.8 0.2 fusion
  12.0 0.1 pad_maximum_fusion.1
  12.1 1.7 %collective-permute-done.2 = bf16[40,1024]{1,0:T(8,128)(2,1)S(1)} collective-permute-done((bf16[40,1024]{1,0:T(8,128)(2,1)S(1)}, bf16[40,1024]{1,0:T(8,128)(2,1)S(1)}, u32[]{:S(2)}, u32[]{:S(2)}) %collective-permute-start.2) | collective-permute-done | bytes 81952 | tf_op jit(solution)/shard_map/ppermute | solution.py:611
  13.8 0.1 collective-permute-start.3
  13.9 1.4 %collective-permute-done.3.refs_1_ = bf16[80,1024]{1,0:T(8,128)(2,1)S(1)} collective-permute-done((bf16[80,1024]{1,0:T(8,128)(2,1)S(1)}, bf16[80,1024]{1,0:T(8,128)(2,1)S(1)}, u32[]{:S(2)}, u32[]{:S(2)}) %collective-permute-start.3) | collective-permute-done | bytes 163872 | tf_op jit(solution)/shard_map/ppermute | solution.py:25
  15.3 0.0 copy-start.14
  15.3 0.6 project.1
  15.9 2.8 %collective-permute-start.4 = (bf16[40,1152]{1,0:T(8,128)(2,1)S(1)}, bf16[40,1152]{1,0:T(8,128)(2,1)S(1)}, u32[]{:S(2)}, u32[]{:S(2)}) collective-permute-start(bf16[40,1152]{1,0:T(8,128)(2,1)S(1)} %get-tuple-element.69), channel_id=1, source_target_pairs={{0,8},{8,0},{16,24},{24,16},{1,9},{9,1},{17,25},{25,17},{2,10},{10... | collective-permute-start | bytes 276488 | tf_op jit(solution)/shard_map/ppermute | solution.py:40
  18.7 0.9 %collective-permute-start.5 = (bf16[40,1152]{1,0:T(8,128)(2,1)S(1)}, bf16[40,1152]{1,0:T(8,128)(2,1)S(1)}, u32[]{:S(2)}, u32[]{:S(2)}) collective-permute-start(bf16[40,1152]{1,0:T(8,128)(2,1)S(1)} %get-tuple-element.70), channel_id=1, source_target_pairs={{0,16},{8,24},{16,0},{24,8},{1,17},{9,25},{17,1},{25,9},{2,18},{10... | collective-permute-start | bytes 276488 | tf_op jit(solution)/shard_map/ppermute | solution.py:40
  19.7 0.6 collective-permute-start.6
  20.3 1.4 %collective-permute-done.4.refs_4_ = bf16[40,1152]{1,0:T(8,128)(2,1)S(1)} collective-permute-done((bf16[40,1152]{1,0:T(8,128)(2,1)S(1)}, bf16[40,1152]{1,0:T(8,128)(2,1)S(1)}, u32[]{:S(2)}, u32[]{:S(2)}) %collective-permute-start.4) | collective-permute-done | bytes 92192 | tf_op jit(solution)/shard_map/ppermute | solution.py:40
  21.7 3.6 %collective-permute-done.5.refs_5_ = bf16[40,1152]{1,0:T(8,128)(2,1)S(1)} collective-permute-done((bf16[40,1152]{1,0:T(8,128)(2,1)S(1)}, bf16[40,1152]{1,0:T(8,128)(2,1)S(1)}, u32[]{:S(2)}, u32[]{:S(2)}) %collective-permute-start.5) | collective-permute-done | bytes 92192 | tf_op jit(solution)/shard_map/ppermute | solution.py:40
  25.3 1.2 %read_state.1 = (bf16[40,256]{1,0:T(8,128)(2,1)S(1)}, f32[40,256]{1,0:T(8,128)S(1)}, f32[40,256]{1,0:T(8,128)S(1)}) custom-call(f32[40,128]{1,0:T(8,128)S(1)} %get-tuple-element.64.refs_0_, f32[40,128]{1,0:T(8,128)S(1)} %get-tuple-element.65.refs_1_, f32[1,256]{1,0:T(1,128)S(1)} %bitcast.11, f32[40,1152]{1,0:T(8,128)S(1)} %get-tuple-element.68.refs_3_, ...), custom_call_target="tpu_custom_call" | custom-call | flops 5000000000 | bytes 30000000 | tf_op jit(solution)/shard_map/read_state/pallas_call | solution.py:335
  26.5 0.6 collective-permute-start.7
  27.1 1.7 %collective-permute-start.8 = (bf16[40,256]{1,0:T(8,128)(2,1)S(1)}, bf16[40,256]{1,0:T(8,128)(2,1)S(1)}, u32[]{:S(2)}, u32[]{:S(2)}) collective-permute-start(bf16[40,256]{1,0:T(8,128)(2,1)S(1)} %get-tuple-element.75.refs_0_), channel_id=1, source_target_pairs={{0,4},{1,5},{2,6},{3,7},{4,0},{5,1},{6,2},{7,3},{8,12},{9,13},{10,... | collective-permute-start | bytes 61448 | tf_op jit(solution)/shard_map/ppermute | solution.py:32
  28.8 2.1 %collective-permute-start.9 = (bf16[40,256]{1,0:T(8,128)(2,1)S(1)}, bf16[40,256]{1,0:T(8,128)(2,1)S(1)}, u32[]{:S(2)}, u32[]{:S(2)}) collective-permute-start(bf16[40,256]{1,0:T(8,128)(2,1)S(1)} %get-tuple-element.75.refs_0_), channel_id=1, source_target_pairs={{0,6},{1,7},{2,4},{3,5},{4,2},{5,3},{6,0},{7,1},{8,14},{9,15},{10,... | collective-permute-start | bytes 61448 | tf_op jit(solution)/shard_map/ppermute | solution.py:32
  30.9 1.6 %update_state.2.refs_4_ = f32[40,2,128,128]{3,2,1,0:T(8,128)} custom-call(f32[40,256]{1,0:T(8,128)S(1)} %get-tuple-element.73.refs_0_, f32[40,256]{1,0:T(8,128)S(1)} %get-tuple-element.74.refs_1_, f32[40,2,128,128]{3,2,1,0:T(8,128)S(1)} %bitcast.6), custom_call_target="tpu_custom_call" | custom-call | flops 5000000000 | bytes 30000000 | tf_op jit(solution)/shard_map/update_state/pallas_call | solution.py:379
  32.5 1.9 %collective-permute-done.9 = bf16[40,256]{1,0:T(8,128)(2,1)S(1)} collective-permute-done((bf16[40,256]{1,0:T(8,128)(2,1)S(1)}, bf16[40,256]{1,0:T(8,128)(2,1)S(1)}, u32[]{:S(2)}, u32[]{:S(2)}) %collective-permute-start.9) | collective-permute-done | bytes 20512 | tf_op jit(solution)/shard_map/ppermute | solution.py:32
  34.4 0.1 collective-permute-start.11
  34.5 0.5 collective-permute-start.10
  35.0 0.8 %collective-permute-done.10.refs_2_ = bf16[40,256]{1,0:T(8,128)(2,1)S(1)} collective-permute-done((bf16[40,256]{1,0:T(8,128)(2,1)S(1)}, bf16[40,256]{1,0:T(8,128)(2,1)S(1)}, u32[]{:S(2)}, u32[]{:S(2)}) %collective-permute-start.10) | collective-permute-done | bytes 20512 | tf_op jit(solution)/shard_map/ppermute | solution.py:25
  35.8 0.6 out_project.1
  36.5 1.6 %collective-permute-start.12 = (bf16[10,640]{1,0:T(8,128)(2,1)S(1)}, bf16[10,640]{1,0:T(8,128)(2,1)S(1)}, u32[]{:S(2)}, u32[]{:S(2)}) collective-permute-start(bf16[10,640]{1,0:T(8,128)(2,1)S(1)} %get-tuple-element.89), channel_id=1, source_target_pairs={{0,8},{8,0},{16,24},{24,16},{1,9},{9,1},{17,25},{25,17},{2,10},{10... | collective-permute-start | bytes 38408 | tf_op jit(solution)/shard_map/ppermute | solution.py:40
  38.1 0.9 %collective-permute-start.13 = (bf16[10,640]{1,0:T(8,128)(2,1)S(1)}, bf16[10,640]{1,0:T(8,128)(2,1)S(1)}, u32[]{:S(2)}, u32[]{:S(2)}) collective-permute-start(bf16[10,640]{1,0:T(8,128)(2,1)S(1)} %get-tuple-element.90), channel_id=1, source_target_pairs={{0,16},{8,24},{16,0},{24,8},{1,17},{9,25},{17,1},{25,9},{2,18},{10... | collective-permute-start | bytes 38408 | tf_op jit(solution)/shard_map/ppermute | solution.py:40
  38.9 1.1 %collective-permute-start.14 = (bf16[10,640]{1,0:T(8,128)(2,1)S(1)}, bf16[10,640]{1,0:T(8,128)(2,1)S(1)}, u32[]{:S(2)}, u32[]{:S(2)}) collective-permute-start(bf16[10,640]{1,0:T(8,128)(2,1)S(1)} %get-tuple-element.91), channel_id=1, source_target_pairs={{0,24},{8,16},{16,8},{24,0},{1,25},{9,17},{17,9},{25,1},{2,26},{10... | collective-permute-start | bytes 38408 | tf_op jit(solution)/shard_map/ppermute | solution.py:40
  40.0 2.6 %update_state.3 = f32[40,2,128,128]{3,2,1,0:T(8,128)} custom-call(f32[40,256]{1,0:T(8,128)S(1)} %get-tuple-element.73.refs_0_, f32[40,256]{1,0:T(8,128)S(1)} %get-tuple-element.74.refs_1_, f32[40,2,128,128]{3,2,1,0:T(8,128)S(1)} %bitcast.6, bf16[40,512]{1,0:T(8,128)(2,1)S(1)} %get-tuple-element.87.refs_3_.refs_0_, ...), custom_call_target="tpu_custom_call", output_to_operand_aliasing={{}: (4, {})} | custom-call | flops 5000000000 | bytes 30000000 | tf_op jit(solution)/shard_map/update_state/pallas_call | solution.py:379
  42.6 1.0 %collective-permute-done.14.refs_8_ = bf16[10,640]{1,0:T(8,128)(2,1)S(1)} collective-permute-done((bf16[10,640]{1,0:T(8,128)(2,1)S(1)}, bf16[10,640]{1,0:T(8,128)(2,1)S(1)}, u32[]{:S(2)}, u32[]{:S(2)}) %collective-permute-start.14) | collective-permute-done | bytes 12832 | tf_op jit(solution)/shard_map/ppermute | solution.py:40
  43.7 0.1 collective-permute-start.15
  43.8 1.8 %collective-permute-start.16 = (bf16[40,512]{1,0:T(8,128)(2,1)S(1)}, bf16[40,512]{1,0:T(8,128)(2,1)S(1)}, u32[]{:S(2)}, u32[]{:S(2)}) collective-permute-start(bf16[40,512]{1,0:T(8,128)(2,1)S(1)} %pad_maximum_fusion.refs_0_), channel_id=1, source_target_pairs={{0,4},{1,5},{2,6},{3,7},{4,0},{5,1},{6,2},{7,3},{8,12},{9,13},{10,... | collective-permute-start | bytes 122888 | tf_op jit(solution)/shard_map/ppermute | solution.py:32
  45.6 2.6 %collective-permute-start.17 = (bf16[40,512]{1,0:T(8,128)(2,1)S(1)}, bf16[40,512]{1,0:T(8,128)(2,1)S(1)}, u32[]{:S(2)}, u32[]{:S(2)}) collective-permute-start(bf16[40,512]{1,0:T(8,128)(2,1)S(1)} %pad_maximum_fusion.refs_0_), channel_id=1, source_target_pairs={{0,6},{1,7},{2,4},{3,5},{4,2},{5,3},{6,0},{7,1},{8,14},{9,15},{10,... | collective-permute-start | bytes 122888 | tf_op jit(solution)/shard_map/ppermute | solution.py:32
  48.1 0.6 collective-permute-done.16
  48.7 2.6 %collective-permute-done.17 = bf16[40,512]{1,0:T(8,128)(2,1)S(1)} collective-permute-done((bf16[40,512]{1,0:T(8,128)(2,1)S(1)}, bf16[40,512]{1,0:T(8,128)(2,1)S(1)}, u32[]{:S(2)}, u32[]{:S(2)}) %collective-permute-start.17) | collective-permute-done | bytes 40992 | tf_op jit(solution)/shard_map/ppermute | solution.py:32
  51.4 0.5 collective-permute-start.18
  51.9 0.9 %collective-permute-done.18.refs_2_ = bf16[40,512]{1,0:T(8,128)(2,1)S(1)} collective-permute-done((bf16[40,512]{1,0:T(8,128)(2,1)S(1)}, bf16[40,512]{1,0:T(8,128)(2,1)S(1)}, u32[]{:S(2)}, u32[]{:S(2)}) %collective-permute-start.18) | collective-permute-done | bytes 40992 | tf_op jit(solution)/shard_map/ppermute | solution.py:25
  52.8 0.0 copy-start.2
  52.8 1.7 %lift.1.refs_0_ = bf16[2,40,256]{2,1,0:T(8,128)(2,1)S(1)} custom-call(bf16[40,512]{1,0:T(8,128)(2,1)S(1)} %pad_maximum_fusion.refs_0_, bf16[120,512]{1,0:T(8,128)(2,1)S(1)} %constant_dynamic-update-slice_fusion.5.refs_1_, bf16[40,512]{1,0:T(8,128)(2,1)S(1)} %collective-permute-done.18.refs_2_, bf16[120,512]{1,0:T(8,128)(2,1)S(1)} %collective-permute-done.19.refs_3_, ...), custom_call_target="tpu_custom_call" | custom-call | flops 7500000256 | bytes 45000000 | tf_op jit(solution)/shard_map/lift/pallas_call | solution.py:464
  54.5 0.1 collective-permute-start.20
  54.6 3.1 %collective-permute-start.21 = (bf16[2,40,256]{2,1,0:T(8,128)(2,1)S(1)}, bf16[2,40,256]{2,1,0:T(8,128)(2,1)S(1)}, u32[]{:S(2)}, u32[]{:S(2)}) collective-permute-start(bf16[2,40,256]{2,1,0:T(8,128)(2,1)S(1)} %lift.1.refs_0_), channel_id=1, source_target_pairs={{0,4},{1,5},{2,6},{3,7},{4,0},{5,1},{6,2},{7,3},{8,12},{9,13},{10,... | collective-permute-start | bytes 122888 | tf_op jit(solution)/shard_map/ppermute | solution.py:32
  57.7 1.3 %collective-permute-start.22 = (bf16[2,40,256]{2,1,0:T(8,128)(2,1)S(1)}, bf16[2,40,256]{2,1,0:T(8,128)(2,1)S(1)}, u32[]{:S(2)}, u32[]{:S(2)}) collective-permute-start(bf16[2,40,256]{2,1,0:T(8,128)(2,1)S(1)} %lift.1.refs_0_), channel_id=1, source_target_pairs={{0,6},{1,7},{2,4},{3,5},{4,2},{5,3},{6,0},{7,1},{8,14},{9,15},{10,... | collective-permute-start | bytes 122888 | tf_op jit(solution)/shard_map/ppermute | solution.py:32
  58.9 0.7 collective-permute-done.21
  59.7 3.8 %collective-permute-done.22 = bf16[2,40,256]{2,1,0:T(8,128)(2,1)S(1)} collective-permute-done((bf16[2,40,256]{2,1,0:T(8,128)(2,1)S(1)}, bf16[2,40,256]{2,1,0:T(8,128)(2,1)S(1)}, u32[]{:S(2)}, u32[]{:S(2)}) %collective-permute-start.22) | collective-permute-done | bytes 40992 | tf_op jit(solution)/shard_map/ppermute | solution.py:32
  63.5 0.5 collective-permute-start.23
  64.0 0.9 %collective-permute-done.23.refs_2_ = bf16[2,40,256]{2,1,0:T(8,128)(2,1)S(1)} collective-permute-done((bf16[2,40,256]{2,1,0:T(8,128)(2,1)S(1)}, bf16[2,40,256]{2,1,0:T(8,128)(2,1)S(1)}, u32[]{:S(2)}, u32[]{:S(2)}) %collective-permute-start.23) | collective-permute-done | bytes 40992 | tf_op jit(solution)/shard_map/ppermute | solution.py:25
  64.9 0.9 %lower.1 = (bf16[10,512]{1,0:T(8,128)(2,1)S(1)}, bf16[10,512]{1,0:T(8,128)(2,1)S(1)}, bf16[10,512]{1,0:T(8,128)(2,1)S(1)}, bf16[10,512]{1,0:T(8,128)(2,1)S(1)}) custom-call(bf16[2,40,256]{2,1,0:T(8,128)(2,1)S(1)} %lift.1.refs_0_, bf16[2,120,256]{2,1,0:T(8,128)(2,1)S(1)} %constant_dynamic-update-slice_fusion.8.refs_1_, ...), custom_call_target="tpu_custom_call" | custom-call | flops 5000000000 | bytes 30000000 | tf_op jit(solution)/shard_map/lower/pallas_call | solution.py:512
  65.7 0.9 %collective-permute-start.25 = (bf16[10,512]{1,0:T(8,128)(2,1)S(1)}, bf16[10,512]{1,0:T(8,128)(2,1)S(1)}, u32[]{:S(2)}, u32[]{:S(2)}) collective-permute-start(bf16[10,512]{1,0:T(8,128)(2,1)S(1)} %get-tuple-element.98), channel_id=1, source_target_pairs={{0,8},{8,0},{16,24},{24,16},{1,9},{9,1},{17,25},{25,17},{2,10},{10... | collective-permute-start | bytes 30728 | tf_op jit(solution)/shard_map/ppermute | solution.py:40
  66.7 0.8 %collective-permute-start.26 = (bf16[10,512]{1,0:T(8,128)(2,1)S(1)}, bf16[10,512]{1,0:T(8,128)(2,1)S(1)}, u32[]{:S(2)}, u32[]{:S(2)}) collective-permute-start(bf16[10,512]{1,0:T(8,128)(2,1)S(1)} %get-tuple-element.99), channel_id=1, source_target_pairs={{0,16},{8,24},{16,0},{24,8},{1,17},{9,25},{17,1},{25,9},{2,18},{10... | collective-permute-start | bytes 30728 | tf_op jit(solution)/shard_map/ppermute | solution.py:40
  67.4 1.9 %collective-permute-start.27 = (bf16[10,512]{1,0:T(8,128)(2,1)S(1)}, bf16[10,512]{1,0:T(8,128)(2,1)S(1)}, u32[]{:S(2)}, u32[]{:S(2)}) collective-permute-start(bf16[10,512]{1,0:T(8,128)(2,1)S(1)} %get-tuple-element.100), channel_id=1, source_target_pairs={{0,24},{8,16},{16,8},{24,0},{1,25},{9,17},{17,9},{25,1},{2,26},{10... | collective-permute-start | bytes 30728 | tf_op jit(solution)/shard_map/ppermute | solution.py:40
  69.3 0.2 collective-permute-done.25.refs_6_
  69.5 0.9 %collective-permute-done.26.refs_7_ = bf16[10,512]{1,0:T(8,128)(2,1)S(1)} collective-permute-done((bf16[10,512]{1,0:T(8,128)(2,1)S(1)}, bf16[10,512]{1,0:T(8,128)(2,1)S(1)}, u32[]{:S(2)}, u32[]{:S(2)}) %collective-permute-start.26) | collective-permute-done | bytes 10272 | tf_op jit(solution)/shard_map/ppermute | solution.py:40
  70.4 1.7 %collective-permute-done.27.refs_8_ = bf16[10,512]{1,0:T(8,128)(2,1)S(1)} collective-permute-done((bf16[10,512]{1,0:T(8,128)(2,1)S(1)}, bf16[10,512]{1,0:T(8,128)(2,1)S(1)}, u32[]{:S(2)}, u32[]{:S(2)}) %collective-permute-start.27) | collective-permute-done | bytes 10272 | tf_op jit(solution)/shard_map/ppermute | solution.py:40
  72.1 0.8 %finish.1 = bf16[40,512]{1,0:T(8,128)(2,1)} custom-call(bf16[40,512]{1,0:T(8,128)(2,1)S(1)} %get-tuple-element.87.refs_3_.refs_0_, bf16[10,40]{1,0:T(8,128)(2,1)S(1)} %get-tuple-element.79.refs_6_.refs_1_, bf16[10,40]{1,0:T(8,128)(2,1)S(1)} %get-tuple-element.80.refs_7_.refs_2_, bf16[10,40]{1,0:T(8,128)(2,1)S(1)} %get-tuple-element.81.refs_8_.refs_3_, ...), custom_call_target="tpu_custom_call" | custom-call | flops 2500000000 | bytes 15000000 | tf_op jit(solution)/shard_map/finish/pallas_call | solution.py:542
  (60 shorter events, 0.2 us)
Async XLA Ops:
  0.6 1.6 %collective-permute-start = (bf16[40,512]{1,0:T(8,128)(2,1)}, bf16[40,512]{1,0:T(8,128)(2,1)S(1)}, u32[]{:S(2)}, u32[]{:S(2)}) collective-permute-start(bf16[40,512]{1,0:T(8,128)(2,1)} %refs_5_.4), channel_id=1, source_target_pairs={{0,1},{1,0},{2,3},{3,2},{4,5},{5,4},{6,7},{7,6},{8,9},{9,8},{10,11... | collective-permute-start | bytes 122888 | tf_op jit(solution)/shard_map/ppermute | solution.py:25
  1.2 0.8 %copy-start.8 = (bf16[40,512]{1,0:T(8,128)(2,1)S(1)}, bf16[40,512]{1,0:T(8,128)(2,1)}, u32[]{:S(2)}) copy-start(bf16[40,512]{1,0:T(8,128)(2,1)} %refs_5_.4) | copy-start | bytes 122884
  2.0 9.5 %copy-start.15 = (s32[40]{0:T(128)S(1)}, s32[40]{0:T(128)}, u32[]{:S(2)}) copy-start(s32[40]{0:T(128)} %param.17) | copy-start | bytes 484
  2.0 9.5 %copy-start.12 = (s32[40,2]{0,1:T(2,128)S(1)}, s32[40,2]{0,1:T(2,128)}, u32[]{:S(2)}) copy-start(s32[40,2]{0,1:T(2,128)} %param.30) | copy-start | bytes 964
  2.0 9.5 %copy-start.13 = (f32[40,2]{0,1:T(2,128)S(1)}, f32[40,2]{0,1:T(2,128)}, u32[]{:S(2)}) copy-start(f32[40,2]{0,1:T(2,128)} %param.31) | copy-start | bytes 964
  2.3 9.8 %collective-permute-start.1 = (bf16[40,1024]{1,0:T(8,128)(2,1)S(1)}, bf16[40,1024]{1,0:T(8,128)(2,1)S(1)}, u32[]{:S(2)}, u32[]{:S(2)}) collective-permute-start(bf16[40,1024]{1,0:T(8,128)(2,1)S(1)} %join.1), channel_id=1, source_target_pairs={{0,4},{1,3},{2,12},{3,11},{4,20},{5,19},{6,28},{7,27},{8,6},{9,1},... | collective-permute-start | bytes 245768 | tf_op jit(solution)/shard_map/ppermute | solution.py:611
  6.2 7.6 %collective-permute-start.2 = (bf16[40,1024]{1,0:T(8,128)(2,1)S(1)}, bf16[40,1024]{1,0:T(8,128)(2,1)S(1)}, u32[]{:S(2)}, u32[]{:S(2)}) collective-permute-start(bf16[40,1024]{1,0:T(8,128)(2,1)S(1)} %join.1), channel_id=1, source_target_pairs={{0,6},{1,1},{2,14},{3,9},{4,22},{5,17},{6,30},{7,25},{8,4},{9,3},{... | collective-permute-start | bytes 245768 | tf_op jit(solution)/shard_map/ppermute | solution.py:611
  11.5 3.8 %copy-start.4 = (bf16[1024,256]{1,0:T(8,128)(2,1)S(1)}, bf16[1024,256]{1,0:T(8,128)(2,1)}, u32[]{:S(2)}) copy-start(bf16[1024,256]{1,0:T(8,128)(2,1)} %refs_2_.3) | copy-start | bytes 1572868
  11.5 3.8 %copy-start.5 = (bf16[1024,256]{1,0:T(8,128)(2,1)S(1)}, bf16[1024,256]{1,0:T(8,128)(2,1)}, u32[]{:S(2)}) copy-start(bf16[1024,256]{1,0:T(8,128)(2,1)} %refs_3_.1) | copy-start | bytes 1572868
  11.5 3.8 %copy-start.6 = (bf16[1024,256]{1,0:T(8,128)(2,1)S(1)}, bf16[1024,256]{1,0:T(8,128)(2,1)}, u32[]{:S(2)}) copy-start(bf16[1024,256]{1,0:T(8,128)(2,1)} %refs_4_.3) | copy-start | bytes 1572868
  11.5 3.8 %copy-start.7 = (bf16[1024,256]{1,0:T(8,128)(2,1)S(1)}, bf16[1024,256]{1,0:T(8,128)(2,1)}, u32[]{:S(2)}) copy-start(bf16[1024,256]{1,0:T(8,128)(2,1)} %refs_5_.3) | copy-start | bytes 1572868
  11.5 3.8 %copy-start.10 = (f32[4096]{0:T(1024)S(1)}, f32[4096]{0:T(1024)}, u32[]{:S(2)}) copy-start(f32[4096]{0:T(1024)} %param.25) | copy-start | bytes 49156
  11.5 13.7 %slice-start = ((s8[5242880]{0:T(1024)(128)(4,1)}), s8[4194304]{0:T(1024)(128)(4,1)S(1)}, s32[]{:S(2)}) async-start(s8[5242880]{0:T(1024)(128)(4,1)} %bitcast.5), calls=%async_computation | async-start | bytes 8388608
  13.8 11.5 %slice-start.1 = ((s8[5242880]{0:T(1024)(128)(4,1)}), s8[1048576]{0:T(1024)(128)(4,1)S(1)}, s32[]{:S(2)}) async-start(s8[5242880]{0:T(1024)(128)(4,1)} %bitcast.5), calls=%async_computation.1 | async-start | bytes 2097152
  13.8 1.5 %collective-permute-start.3 = (bf16[80,1024]{1,0:T(8,128)(2,1)S(1)}, bf16[80,1024]{1,0:T(8,128)(2,1)S(1)}, u32[]{:S(2)}, u32[]{:S(2)}) collective-permute-start(bf16[80,1024]{1,0:T(8,128)(2,1)S(1)} %constant_dynamic-update-slice_fusion.refs_0_), channel_id=1, source_target_pairs={{0,1},{1,0},{2,3},{3,2},{4,5},{5,4},{6,7},{7,6},{8,9},{9,8},{10,11... | collective-permute-start | bytes 491528 | tf_op jit(solution)/shard_map/ppermute | solution.py:25
  15.3 10.0 %copy-start.14 = (f32[256]{0:T(256)S(1)}, f32[256]{0:T(256)}, u32[]{:S(2)}) copy-start(f32[256]{0:T(256)} %param.23) | copy-start | bytes 3076
  15.9 5.8 %collective-permute-start.4 = (bf16[40,1152]{1,0:T(8,128)(2,1)S(1)}, bf16[40,1152]{1,0:T(8,128)(2,1)S(1)}, u32[]{:S(2)}, u32[]{:S(2)}) collective-permute-start(bf16[40,1152]{1,0:T(8,128)(2,1)S(1)} %get-tuple-element.69), channel_id=1, source_target_pairs={{0,8},{8,0},{16,24},{24,16},{1,9},{9,1},{17,25},{25,17},{2,10},{10... | collective-permute-start | bytes 276488 | tf_op jit(solution)/shard_map/ppermute | solution.py:40
  18.7 6.5 %collective-permute-start.5 = (bf16[40,1152]{1,0:T(8,128)(2,1)S(1)}, bf16[40,1152]{1,0:T(8,128)(2,1)S(1)}, u32[]{:S(2)}, u32[]{:S(2)}) collective-permute-start(bf16[40,1152]{1,0:T(8,128)(2,1)S(1)} %get-tuple-element.70), channel_id=1, source_target_pairs={{0,16},{8,24},{16,0},{24,8},{1,17},{9,25},{17,1},{25,9},{2,18},{10... | collective-permute-start | bytes 276488 | tf_op jit(solution)/shard_map/ppermute | solution.py:40
  19.7 5.6 %collective-permute-start.6 = (bf16[40,1152]{1,0:T(8,128)(2,1)S(1)}, bf16[40,1152]{1,0:T(8,128)(2,1)S(1)}, u32[]{:S(2)}, u32[]{:S(2)}) collective-permute-start(bf16[40,1152]{1,0:T(8,128)(2,1)S(1)} %get-tuple-element.71), channel_id=1, source_target_pairs={{0,24},{8,16},{16,8},{24,0},{1,25},{9,17},{17,9},{25,1},{2,26},{10... | collective-permute-start | bytes 276488 | tf_op jit(solution)/shard_map/ppermute | solution.py:40
  26.5 6.1 %collective-permute-start.7 = (bf16[40,256]{1,0:T(8,128)(2,1)S(1)}, bf16[40,256]{1,0:T(8,128)(2,1)S(1)}, u32[]{:S(2)}, u32[]{:S(2)}) collective-permute-start(bf16[40,256]{1,0:T(8,128)(2,1)S(1)} %get-tuple-element.75.refs_0_), channel_id=1, source_target_pairs={{0,2},{1,3},{2,0},{3,1},{4,6},{5,7},{6,4},{7,5},{8,10},{9,11},{10,... | collective-permute-start | bytes 61448 | tf_op jit(solution)/shard_map/ppermute | solution.py:32
  27.1 5.4 %collective-permute-start.8 = (bf16[40,256]{1,0:T(8,128)(2,1)S(1)}, bf16[40,256]{1,0:T(8,128)(2,1)S(1)}, u32[]{:S(2)}, u32[]{:S(2)}) collective-permute-start(bf16[40,256]{1,0:T(8,128)(2,1)S(1)} %get-tuple-element.75.refs_0_), channel_id=1, source_target_pairs={{0,4},{1,5},{2,6},{3,7},{4,0},{5,1},{6,2},{7,3},{8,12},{9,13},{10,... | collective-permute-start | bytes 61448 | tf_op jit(solution)/shard_map/ppermute | solution.py:32
  28.8 5.6 %collective-permute-start.9 = (bf16[40,256]{1,0:T(8,128)(2,1)S(1)}, bf16[40,256]{1,0:T(8,128)(2,1)S(1)}, u32[]{:S(2)}, u32[]{:S(2)}) collective-permute-start(bf16[40,256]{1,0:T(8,128)(2,1)S(1)} %get-tuple-element.75.refs_0_), channel_id=1, source_target_pairs={{0,6},{1,7},{2,4},{3,5},{4,2},{5,3},{6,0},{7,1},{8,14},{9,15},{10,... | collective-permute-start | bytes 61448 | tf_op jit(solution)/shard_map/ppermute | solution.py:32
  30.9 4.9 %copy-start.3 = (bf16[2048,512]{1,0:T(8,128)(2,1)S(1)}, bf16[2048,512]{1,0:T(8,128)(2,1)}, u32[]{:S(2)}) copy-start(bf16[2048,512]{1,0:T(8,128)(2,1)} %refs_4_.4) | copy-start | bytes 6291460
  30.9 4.9 %copy-start.9 = (bf16[40,512]{1,0:T(8,128)(2,1)S(1)}, bf16[40,512]{1,0:T(8,128)(2,1)}, u32[]{:S(2)}) copy-start(bf16[40,512]{1,0:T(8,128)(2,1)} %refs_5_.4) | copy-start | bytes 122884
  34.4 1.4 %collective-permute-start.11 = (bf16[120,256]{1,0:T(8,128)(2,1)S(1)}, bf16[120,256]{1,0:T(8,128)(2,1)S(1)}, u32[]{:S(2)}, u32[]{:S(2)}) collective-permute-start(bf16[120,256]{1,0:T(8,128)(2,1)S(1)} %constant_dynamic-update-slice_fusion.2.refs_1_), channel_id=1, source_target_pairs={{0,1},{1,0},{2,3},{3,2},{4,5},{5,4},{6,7},{7,6},{8,9},{9,8},{10,11... | collective-permute-start | bytes 184328 | tf_op jit(solution)/shard_map/ppermute | solution.py:25
  34.5 1.3 %collective-permute-start.10 = (bf16[40,256]{1,0:T(8,128)(2,1)S(1)}, bf16[40,256]{1,0:T(8,128)(2,1)S(1)}, u32[]{:S(2)}, u32[]{:S(2)}) collective-permute-start(bf16[40,256]{1,0:T(8,128)(2,1)S(1)} %get-tuple-element.75.refs_0_), channel_id=1, source_target_pairs={{0,1},{1,0},{2,3},{3,2},{4,5},{5,4},{6,7},{7,6},{8,9},{9,8},{10,11... | collective-permute-start | bytes 61448 | tf_op jit(solution)/shard_map/ppermute | solution.py:25
  36.5 6.2 %collective-permute-start.12 = (bf16[10,640]{1,0:T(8,128)(2,1)S(1)}, bf16[10,640]{1,0:T(8,128)(2,1)S(1)}, u32[]{:S(2)}, u32[]{:S(2)}) collective-permute-start(bf16[10,640]{1,0:T(8,128)(2,1)S(1)} %get-tuple-element.89), channel_id=1, source_target_pairs={{0,8},{8,0},{16,24},{24,16},{1,9},{9,1},{17,25},{25,17},{2,10},{10... | collective-permute-start | bytes 38408 | tf_op jit(solution)/shard_map/ppermute | solution.py:40
  38.1 4.6 %collective-permute-start.13 = (bf16[10,640]{1,0:T(8,128)(2,1)S(1)}, bf16[10,640]{1,0:T(8,128)(2,1)S(1)}, u32[]{:S(2)}, u32[]{:S(2)}) collective-permute-start(bf16[10,640]{1,0:T(8,128)(2,1)S(1)} %get-tuple-element.90), channel_id=1, source_target_pairs={{0,16},{8,24},{16,0},{24,8},{1,17},{9,25},{17,1},{25,9},{2,18},{10... | collective-permute-start | bytes 38408 | tf_op jit(solution)/shard_map/ppermute | solution.py:40
  38.9 4.7 %collective-permute-start.14 = (bf16[10,640]{1,0:T(8,128)(2,1)S(1)}, bf16[10,640]{1,0:T(8,128)(2,1)S(1)}, u32[]{:S(2)}, u32[]{:S(2)}) collective-permute-start(bf16[10,640]{1,0:T(8,128)(2,1)S(1)} %get-tuple-element.91), channel_id=1, source_target_pairs={{0,24},{8,16},{16,8},{24,0},{1,25},{9,17},{17,9},{25,1},{2,26},{10... | collective-permute-start | bytes 38408 | tf_op jit(solution)/shard_map/ppermute | solution.py:40
  40.0 12.8 %copy-start = (bf16[2,4096,256]{2,1,0:T(8,128)(2,1)S(1)}, bf16[2,4096,256]{2,1,0:T(8,128)(2,1)}, u32[]{:S(2)}) copy-start(bf16[2,4096,256]{2,1,0:T(8,128)(2,1)} %refs_5_.5) | copy-start | bytes 12582916
  40.0 12.8 %copy-start.1 = (bf16[2,4096,256]{2,1,0:T(8,128)(2,1)S(1)}, bf16[2,4096,256]{2,1,0:T(8,128)(2,1)}, u32[]{:S(2)}) copy-start(bf16[2,4096,256]{2,1,0:T(8,128)(2,1)} %refs_6_.1) | copy-start | bytes 12582916
  40.0 12.8 %copy-start.11 = (f32[4096]{0:T(1024)S(1)}, f32[4096]{0:T(1024)}, u32[]{:S(2)}) copy-start(f32[4096]{0:T(1024)} %param.26) | copy-start | bytes 49156
  43.7 4.5 %collective-permute-start.15 = (bf16[40,512]{1,0:T(8,128)(2,1)S(1)}, bf16[40,512]{1,0:T(8,128)(2,1)S(1)}, u32[]{:S(2)}, u32[]{:S(2)}) collective-permute-start(bf16[40,512]{1,0:T(8,128)(2,1)S(1)} %pad_maximum_fusion.refs_0_), channel_id=1, source_target_pairs={{0,2},{1,3},{2,0},{3,1},{4,6},{5,7},{6,4},{7,5},{8,10},{9,11},{10,... | collective-permute-start | bytes 122888 | tf_op jit(solution)/shard_map/ppermute | solution.py:32
  43.8 5.0 %collective-permute-start.16 = (bf16[40,512]{1,0:T(8,128)(2,1)S(1)}, bf16[40,512]{1,0:T(8,128)(2,1)S(1)}, u32[]{:S(2)}, u32[]{:S(2)}) collective-permute-start(bf16[40,512]{1,0:T(8,128)(2,1)S(1)} %pad_maximum_fusion.refs_0_), channel_id=1, source_target_pairs={{0,4},{1,5},{2,6},{3,7},{4,0},{5,1},{6,2},{7,3},{8,12},{9,13},{10,... | collective-permute-start | bytes 122888 | tf_op jit(solution)/shard_map/ppermute | solution.py:32
  45.6 5.8 %collective-permute-start.17 = (bf16[40,512]{1,0:T(8,128)(2,1)S(1)}, bf16[40,512]{1,0:T(8,128)(2,1)S(1)}, u32[]{:S(2)}, u32[]{:S(2)}) collective-permute-start(bf16[40,512]{1,0:T(8,128)(2,1)S(1)} %pad_maximum_fusion.refs_0_), channel_id=1, source_target_pairs={{0,6},{1,7},{2,4},{3,5},{4,2},{5,3},{6,0},{7,1},{8,14},{9,15},{10,... | collective-permute-start | bytes 122888 | tf_op jit(solution)/shard_map/ppermute | solution.py:32
  51.4 1.4 %collective-permute-start.19 = (bf16[120,512]{1,0:T(8,128)(2,1)S(1)}, bf16[120,512]{1,0:T(8,128)(2,1)S(1)}, u32[]{:S(2)}, u32[]{:S(2)}) collective-permute-start(bf16[120,512]{1,0:T(8,128)(2,1)S(1)} %constant_dynamic-update-slice_fusion.5.refs_1_), channel_id=1, source_target_pairs={{0,1},{1,0},{2,3},{3,2},{4,5},{5,4},{6,7},{7,6},{8,9},{9,8},{10,11... | collective-permute-start | bytes 368648 | tf_op jit(solution)/shard_map/ppermute | solution.py:25
  51.4 1.4 %collective-permute-start.18 = (bf16[40,512]{1,0:T(8,128)(2,1)S(1)}, bf16[40,512]{1,0:T(8,128)(2,1)S(1)}, u32[]{:S(2)}, u32[]{:S(2)}) collective-permute-start(bf16[40,512]{1,0:T(8,128)(2,1)S(1)} %pad_maximum_fusion.refs_0_), channel_id=1, source_target_pairs={{0,1},{1,0},{2,3},{3,2},{4,5},{5,4},{6,7},{7,6},{8,9},{9,8},{10,11... | collective-permute-start | bytes 122888 | tf_op jit(solution)/shard_map/ppermute | solution.py:25
  52.8 12.1 %copy-start.2 = (bf16[2,2048,512]{2,1,0:T(8,128)(2,1)S(1)}, bf16[2,2048,512]{2,1,0:T(8,128)(2,1)}, u32[]{:S(2)}) copy-start(bf16[2,2048,512]{2,1,0:T(8,128)(2,1)} %refs_4_.5) | copy-start | bytes 12582916
  54.5 4.5 %collective-permute-start.20 = (bf16[2,40,256]{2,1,0:T(8,128)(2,1)S(1)}, bf16[2,40,256]{2,1,0:T(8,128)(2,1)S(1)}, u32[]{:S(2)}, u32[]{:S(2)}) collective-permute-start(bf16[2,40,256]{2,1,0:T(8,128)(2,1)S(1)} %lift.1.refs_0_), channel_id=1, source_target_pairs={{0,2},{1,3},{2,0},{3,1},{4,6},{5,7},{6,4},{7,5},{8,10},{9,11},{10,... | collective-permute-start | bytes 122888 | tf_op jit(solution)/shard_map/ppermute | solution.py:32
  54.6 5.1 %collective-permute-start.21 = (bf16[2,40,256]{2,1,0:T(8,128)(2,1)S(1)}, bf16[2,40,256]{2,1,0:T(8,128)(2,1)S(1)}, u32[]{:S(2)}, u32[]{:S(2)}) collective-permute-start(bf16[2,40,256]{2,1,0:T(8,128)(2,1)S(1)} %lift.1.refs_0_), channel_id=1, source_target_pairs={{0,4},{1,5},{2,6},{3,7},{4,0},{5,1},{6,2},{7,3},{8,12},{9,13},{10,... | collective-permute-start | bytes 122888 | tf_op jit(solution)/shard_map/ppermute | solution.py:32
  57.7 5.8 %collective-permute-start.22 = (bf16[2,40,256]{2,1,0:T(8,128)(2,1)S(1)}, bf16[2,40,256]{2,1,0:T(8,128)(2,1)S(1)}, u32[]{:S(2)}, u32[]{:S(2)}) collective-permute-start(bf16[2,40,256]{2,1,0:T(8,128)(2,1)S(1)} %lift.1.refs_0_), channel_id=1, source_target_pairs={{0,6},{1,7},{2,4},{3,5},{4,2},{5,3},{6,0},{7,1},{8,14},{9,15},{10,... | collective-permute-start | bytes 122888 | tf_op jit(solution)/shard_map/ppermute | solution.py:32
  63.5 1.4 %collective-permute-start.24 = (bf16[2,120,256]{2,1,0:T(8,128)(2,1)S(1)}, bf16[2,120,256]{2,1,0:T(8,128)(2,1)S(1)}, u32[]{:S(2)}, u32[]{:S(2)}) collective-permute-start(bf16[2,120,256]{2,1,0:T(8,128)(2,1)S(1)} %constant_dynamic-update-slice_fusion.8.refs_1_), channel_id=1, source_target_pairs={{0,1},{1,0},{2,3},{3,2},{4,5},{5,4},{6,7},{7,6},{8,9},{9,8},{10,11... | collective-permute-start | bytes 368648 | tf_op jit(solution)/shard_map/ppermute | solution.py:25
  63.5 1.4 %collective-permute-start.23 = (bf16[2,40,256]{2,1,0:T(8,128)(2,1)S(1)}, bf16[2,40,256]{2,1,0:T(8,128)(2,1)S(1)}, u32[]{:S(2)}, u32[]{:S(2)}) collective-permute-start(bf16[2,40,256]{2,1,0:T(8,128)(2,1)S(1)} %lift.1.refs_0_), channel_id=1, source_target_pairs={{0,1},{1,0},{2,3},{3,2},{4,5},{5,4},{6,7},{7,6},{8,9},{9,8},{10,11... | collective-permute-start | bytes 122888 | tf_op jit(solution)/shard_map/ppermute | solution.py:25
  65.7 3.8 %collective-permute-start.25 = (bf16[10,512]{1,0:T(8,128)(2,1)S(1)}, bf16[10,512]{1,0:T(8,128)(2,1)S(1)}, u32[]{:S(2)}, u32[]{:S(2)}) collective-permute-start(bf16[10,512]{1,0:T(8,128)(2,1)S(1)} %get-tuple-element.98), channel_id=1, source_target_pairs={{0,8},{8,0},{16,24},{24,16},{1,9},{9,1},{17,25},{25,17},{2,10},{10... | collective-permute-start | bytes 30728 | tf_op jit(solution)/shard_map/ppermute | solution.py:40
  66.7 3.7 %collective-permute-start.26 = (bf16[10,512]{1,0:T(8,128)(2,1)S(1)}, bf16[10,512]{1,0:T(8,128)(2,1)S(1)}, u32[]{:S(2)}, u32[]{:S(2)}) collective-permute-start(bf16[10,512]{1,0:T(8,128)(2,1)S(1)} %get-tuple-element.99), channel_id=1, source_target_pairs={{0,16},{8,24},{16,0},{24,8},{1,17},{9,25},{17,1},{25,9},{2,18},{10... | collective-permute-start | bytes 30728 | tf_op jit(solution)/shard_map/ppermute | solution.py:40
  67.4 4.6 %collective-permute-start.27 = (bf16[10,512]{1,0:T(8,128)(2,1)S(1)}, bf16[10,512]{1,0:T(8,128)(2,1)S(1)}, u32[]{:S(2)}, u32[]{:S(2)}) collective-permute-start(bf16[10,512]{1,0:T(8,128)(2,1)S(1)} %get-tuple-element.100), channel_id=1, source_target_pairs={{0,24},{8,16},{16,8},{24,0},{1,25},{9,17},{17,9},{25,1},{2,26},{10... | collective-permute-start | bytes 30728 | tf_op jit(solution)/shard_map/ppermute | solution.py:40

commit v3 on v2

--- a/solution.py
+++ b/solution.py
@@ -41,14 +41,22 @@
     return found
 
 
-def split_pieces(refs, levels):
-    own, rest, other, others = refs
-    rows = own.shape[-2]
-    found = []
-    for one, many in ((own, rest), (other, others)):
-        found.append(one)
-        found += [many.at[..., pl.ds(k * rows, rows), :] for k in range(levels - 1)]
-    return found
+def pieces_of(one, many, levels):
+    rows = one.shape[-2]
+    return [one] + [many.at[..., pl.ds(k * rows, rows), :] for k in range(levels - 1)]
+
+
+def call(kernel, outs, operands, microseconds, scratch=()):
+    specs = [held()] * len(outs)
+    return pl.pallas_call(
+        kernel,
+        out_shape=outs,
+        in_specs=[held()] * len(operands),
+        out_specs=specs,
+        scratch_shapes=list(scratch),
+        compiler_params=limit(6),
+        cost_estimate=cost(microseconds),
+    )(*[near(array) for array in operands])
 
 
 def spots(count, width):
@@ -389,20 +397,26 @@
     )(*operands)
 
 
-def out_kernel(count, peers, *refs):
-    pieces = split_pieces(refs[:4], count // CORES)
-    weight_ref, hidden_ref = refs[4:6]
-    placing = refs[6 : 6 + peers]
-    shares = refs[6 + peers : 6 + 2 * peers]
-    after_ref = refs[6 + 2 * peers]
-    outs = refs[7 + 2 * peers :]
+def out_sum(pieces, places, weight_ref, total):
     width = pieces[0].shape[1]
-    places = spots(count, width)
+    for piece, place in zip(pieces, places):
+        block = weight_ref[pl.ds(place, width), :]
+        total = total + jnp.dot(piece[...], block, preferred_element_type=f32)
+    return total
+
+
+def out_first(levels, own, rest, weight_ref, hidden_ref, total_ref):
+    places = spots(CORES * levels, own.shape[1])[:levels]
     total = hidden_ref[...].astype(f32)
-    for number in range(count):
-        block = weight_ref[pl.ds(places[number], width), :]
-        total = total + jnp.dot(pieces[number][...], block, preferred_element_type=f32)
-    after = total.astype(bf16)
+    total_ref[...] = out_sum(pieces_of(own, rest, levels), places, weight_ref, total)
+
+
+def out_last(levels, peers, other, others, weight_ref, total_ref, *refs):
+    placing, shares = refs[:peers], refs[peers : 2 * peers]
+    after_ref, outs = refs[2 * peers], refs[2 * peers + 1 :]
+    places = spots(CORES * levels, other.shape[1])[levels:]
+    pieces = pieces_of(other, others, levels)
+    after = out_sum(pieces, places, weight_ref, total_ref[...]).astype(bf16)
     after_ref[...] = after
     cut = after.shape[1]
     for peer in range(peers):
@@ -412,81 +426,124 @@
 
 
 def out_project(pieces, weight, hidden, placing, shares):
+    own, rest, other, others = pieces
     rows, width = hidden.shape
-    slots = placing[0].shape[0]
-    peers = len(placing)
-    operands = [near(array) for array in (*pieces, weight, hidden, *placing, *shares)]
-    return pl.pallas_call(
-        functools.partial(out_kernel, weight.shape[0] // pieces[0].shape[1], peers),
-        out_shape=[near_shape((rows, width), bf16)]
-        + [near_shape((slots, width + HEAD), bf16)] * peers,
-        in_specs=[held()] * len(operands),
-        out_specs=[held()] * (1 + peers),
-        compiler_params=limit(8),
-        cost_estimate=cost(2),
-        name="out_project",
-    )(*operands)
-
-
-def lift_kernel(count, depth, *refs):
-    pieces = split_pieces(refs[:4], count // CORES)
-    gain_ref, gate_ref, up_ref, active_ref = refs[4:]
+    slots, peers = placing[0].shape[0], len(placing)
+    levels = 1 + rest.shape[0] // rows
+    (total,) = call(
+        functools.partial(out_first, levels),
+        [near_shape((rows, width), f32)],
+        (own, rest, weight, hidden),
+        1,
+    )
+    return call(
+        functools.partial(out_last, levels, peers),
+        [near_shape((rows, width), bf16)] + [near_shape((slots, width + HEAD), bf16)] * peers,
+        (other, others, weight, total, *placing, *shares),
+        2,
+    )
+
+
+def lift_sum(pieces, places, gain_ref, gate_ref, up_ref, squares, gates, ups):
     width = pieces[0].shape[1]
-    places = spots(count, width)
-    squares = None
-    for piece in pieces:
+    for piece, place in zip(pieces, places):
         values = piece[...].astype(f32)
-        here = jnp.sum(values * values, axis=-1, keepdims=True)
-        squares = here if squares is None else squares + here
+        squares = squares + jnp.sum(values * values, axis=-1, keepdims=True)
+        scaled = (values * gain_ref[:, pl.ds(place, width)]).astype(bf16)
+        for expert in range(gate_ref.shape[0]):
+            one = gate_ref[expert, pl.ds(place, width), :]
+            two = up_ref[expert, pl.ds(place, width), :]
+            gates[expert] = gates[expert] + jnp.dot(scaled, one, preferred_element_type=f32)
+            ups[expert] = ups[expert] + jnp.dot(scaled, two, preferred_element_type=f32)
+    return squares, gates, ups
+
+
+def lift_first(levels, own, rest, gain_ref, gate_ref, up_ref, gates_ref, ups_ref, squares_ref):
+    experts, rows, width = gates_ref.shape
+    places = spots(CORES * levels, own.shape[1])[:levels]
+    zeros = [jnp.zeros((rows, width), f32)] * experts
+    squares, gates, ups = lift_sum(
+        pieces_of(own, rest, levels),
+        places,
+        gain_ref,
+        gate_ref,
+        up_ref,
+        jnp.zeros((rows, 1), f32),
+        list(zeros),
+        list(zeros),
+    )
+    squares_ref[...] = jnp.broadcast_to(squares, squares_ref.shape)
+    for expert in range(experts):
+        gates_ref[expert] = gates[expert]
+        ups_ref[expert] = ups[expert]
+
+
+def lift_last(
+    levels, depth, other, others, gain_ref, gate_ref, up_ref, gates_ref, ups_ref, squares_ref, active_ref
+):
+    experts = gates_ref.shape[0]
+    places = spots(CORES * levels, other.shape[1])[levels:]
+    squares, gates, ups = lift_sum(
+        pieces_of(other, others, levels),
+        places,
+        gain_ref,
+        gate_ref,
+        up_ref,
+        squares_ref[:, :1],
+        [gates_ref[expert] for expert in range(experts)],
+        [ups_ref[expert] for expert in range(experts)],
+    )
     factor = lax.rsqrt(squares * (1.0 / depth) + epsilon)
-    experts = gate_ref.shape[0]
-    gates, ups = [None] * experts, [None] * experts
-    for number in range(count):
-        start = places[number]
-        gain = gain_ref[:, pl.ds(start, width)]
-        scaled = (pieces[number][...].astype(f32) * factor * gain).astype(bf16)
-        for expert in range(experts):
-            one = gate_ref[expert, pl.ds(start, width), :]
-            two = up_ref[expert, pl.ds(start, width), :]
-            gate = jnp.dot(scaled, one, preferred_element_type=f32)
-            up = jnp.dot(scaled, two, preferred_element_type=f32)
-            gates[expert] = gate if number == 0 else gates[expert] + gate
-            ups[expert] = up if number == 0 else ups[expert] + up
     for expert in range(experts):
-        gate = gates[expert]
-        active_ref[expert] = (gate * jax.nn.sigmoid(gate) * ups[expert]).astype(bf16)
+        gate = gates[expert] * factor
+        active_ref[expert] = (gate * jax.nn.sigmoid(gate) * (ups[expert] * factor)).astype(bf16)
 
 
 def lift(pieces, gain, expert_gate, expert_up):
+    own, rest, other, others = pieces
     experts, depth, width = expert_gate.shape
-    rows = pieces[0].shape[0]
-    operands = [near(array) for array in (*pieces, gain, expert_gate, expert_up)]
-    return pl.pallas_call(
-        functools.partial(lift_kernel, depth // pieces[0].shape[1], depth),
-        out_shape=near_shape((experts, rows, width), bf16),
-        in_specs=[held()] * len(operands),
-        out_specs=held(),
-        compiler_params=limit(8),
-        cost_estimate=cost(3),
-        name="lift",
-    )(*operands)
-
-
-def lower_kernel(count, peers, slots, *refs):
-    pieces = split_pieces(refs[:4], count // CORES)
-    down_ref = refs[4]
-    tables = refs[5 : 5 + peers]
-    outs = refs[5 + peers : 5 + 2 * peers]
-    mean_ref = refs[-1]
-    experts, _, width = pieces[0].shape
-    places = spots(count, width)
-    totals = [None] * experts
-    for number in range(count):
-        start = places[number]
-        for expert in range(experts):
-            block = down_ref[expert, pl.ds(start, width), :]
-            product = jnp.dot(pieces[number][expert], block, preferred_element_type=f32)
-            totals[expert] = product if number == 0 else totals[expert] + product
+    rows = own.shape[0]
+    levels = 1 + rest.shape[0] // rows
+    sums = call(
+        functools.partial(lift_first, levels),
+        [near_shape((experts, rows, width), f32)] * 2 + [near_shape((rows, HEAD), f32)],
+        (own, rest, gain, expert_gate, expert_up),
+        2,
+    )
+    (active,) = call(
+        functools.partial(lift_last, levels, depth),
+        [near_shape((experts, rows, width), bf16)],
+        (other, others, gain, expert_gate, expert_up, *sums),
+        2,
+    )
+    return active
+
+
+def lower_sum(pieces, places, down_ref, totals):
+    width = pieces[0].shape[-1]
+    for piece, place in zip(pieces, places):
+        for expert in range(down_ref.shape[0]):
+            block = down_ref[expert, pl.ds(place, width), :]
+            product = jnp.dot(piece[expert], block, preferred_element_type=f32)
+            totals[expert] = product if totals[expert] is None else totals[expert] + product
+    return totals
+
+
+def lower_first(levels, own, rest, down_ref, totals_ref):
+    experts = down_ref.shape[0]
+    places = spots(CORES * levels, own.shape[2])[:levels]
+    totals = lower_sum(pieces_of(own, rest, levels), places, down_ref, [None] * experts)
+    for expert in range(experts):
+        totals_ref[expert] = totals[expert]
+
+
+def lower_last(levels, peers, other, others, down_ref, totals_ref, *refs):
+    tables, outs, mean_ref = refs[:peers], refs[peers : 2 * peers], refs[-1]
+    experts, _ = totals_ref.shape[:2]
+    slots = tables[0].shape[0]
+    places = spots(CORES * levels, other.shape[2])[levels:]
+    totals = [totals_ref[expert] for expert in range(experts)]
+    totals = lower_sum(pieces_of(other, others, levels), places, down_ref, totals)
     for expert in range(experts):
         mean_ref[expert] = totals[expert].astype(bf16).astype(f32)
     cut = tables[0].shape[1] - HEAD
@@ -505,20 +562,24 @@
 
 
 def lower(pieces, expert_down, tables):
-    experts, depth, width = expert_down.shape
-    rows = pieces[0].shape[1]
+    own, rest, other, others = pieces
+    experts, _, width = expert_down.shape
+    rows = own.shape[1]
+    levels = 1 + rest.shape[1] // rows
     peers, slots = len(tables), tables[0].shape[0]
-    operands = [near(array) for array in (*pieces, expert_down, *tables)]
-    return pl.pallas_call(
-        functools.partial(lower_kernel, depth // pieces[0].shape[2], peers, slots),
-        out_shape=[near_shape((slots, width), bf16)] * peers,
-        in_specs=[held()] * len(operands),
-        out_specs=[held()] * peers,
-        scratch_shapes=[pltpu.VMEM((experts, rows, width), f32)],
-        compiler_params=limit(8),
-        cost_estimate=cost(2),
-        name="lower",
-    )(*operands)
+    (totals,) = call(
+        functools.partial(lower_first, levels),
+        [near_shape((experts, rows, width), f32)],
+        (own, rest, expert_down),
+        1,
+    )
+    return call(
+        functools.partial(lower_last, levels, peers),
+        [near_shape((slots, width), bf16)] * peers,
+        (other, others, expert_down, totals, *tables),
+        2,
+        [pltpu.VMEM((experts, rows, width), f32)],
+    )
 
 
 def finish_kernel(peers, *refs):

time: 73.1 us -> 71.6 us (0.979)
  starting transfers between devices: 36.1 us -> 35.1 us
    ppermute x8, starting transfers between devices: 2.22 us -> 1.27 us  [swap_cores(): return lax.ppermute(array, 'tp', [(i, i ^ 1) for i in range(size)])]
    pallas_call x3 -> x6, Pallas kernels: 3.14 us -> 3.36 us  [call(): pl.pallas_call(kernel, out_shape=outs, in_specs=[held()] * len(operands),...]
  transfers between devices with their start and end apart: 28 -> 28, of which waited for: 17 -> 18; matrix products, arithmetic and copies ran while one was open for 0% -> 0% of each run, Pallas kernels for 6% -> 9%
where the time goes in v3:
time: 71.6 us; the launch traced here: 71.4 us
  starting transfers between devices  35.1 us (49%)
  waiting for transfers between devices  23.6 us (33%)
  Pallas kernels  10.5 us (15%)
  between operations  0.98 us (1%)
  local copies, waits for them, and re-layouts  0.92 us (1%)
    ppermute x9, starting transfers between devices, along_z(): lax.ppermute(array, 'tp', [(i, i ^ CORES * k) for i in range(size)])  13.2 us
    ppermute x9, starting transfers between devices, to_peers(): lax.ppermute(arrays[k], 'ep', [(i, i ^ k) for i in range(size)])  11.5 us
    ppermute x9, waiting for transfers between devices, along_z(): lax.ppermute(array, 'tp', [(i, i ^ CORES * k) for i in range(size)])  9.62 us
    ppermute x2, starting transfers between devices, layer(): came.append(lax.ppermute(joined, ('ep', 'tp'), route))  9.16 us
    ppermute x9, waiting for transfers between devices, to_peers(): lax.ppermute(arrays[k], 'ep', [(i, i ^ k) for i in range(size)])  8.77 us
    pallas_call x2, Pallas kernels, update_state(): pl.pallas_call(functools.partial(update_kernel, heads, first), grid=(last...  4.24 us
    ppermute x8, waiting for transfers between devices, swap_cores(): return lax.ppermute(array, 'tp', [(i, i ^ 1) for i in range(size)])  3.53 us
    pallas_call x6, Pallas kernels, call(): pl.pallas_call(kernel, out_shape=outs, in_specs=[held()] * len(operands),...  3.36 us
  transfers between devices with their start and end apart: 28, of which 18 were waited for; matrix products, arithmetic and copies ran while one was open for 0% of the time, Pallas kernels for 9%

profile of v3, /device:TPU:0, one launch (start us, length us, event | category | flops | bytes accessed | tf_op | source)
XLA Modules:
  0.0 71.4 jit_solution(3918755315709564489)
XLA Ops:
  0.6 0.6 collective-permute-start
  1.2 0.8 %copy-done.8 = bf16[40,512]{1,0:T(8,128)(2,1)S(1)} copy-done((bf16[40,512]{1,0:T(8,128)(2,1)S(1)}, bf16[40,512]{1,0:T(8,128)(2,1)}, u32[]{:S(2)}) %copy-start.8) | copy-done | bytes 40984
  2.0 0.0 copy-start.12
  2.0 0.0 copy-start.13
  2.0 0.3 collective-permute-done.other_ref
  2.3 3.9 %collective-permute-start.1 = (bf16[40,1024]{1,0:T(8,128)(2,1)S(1)}, bf16[40,1024]{1,0:T(8,128)(2,1)S(1)}, u32[]{:S(2)}, u32[]{:S(2)}) collective-permute-start(bf16[40,1024]{1,0:T(8,128)(2,1)S(1)} %join.1), channel_id=1, source_target_pairs={{0,4},{1,3},{2,12},{3,11},{4,20},{5,19},{6,28},{7,27},{8,6},{9,1},... | collective-permute-start | bytes 245768 | tf_op jit(solution)/shard_map/ppermute | solution.py:672
  6.2 5.2 %collective-permute-start.2 = (bf16[40,1024]{1,0:T(8,128)(2,1)S(1)}, bf16[40,1024]{1,0:T(8,128)(2,1)S(1)}, u32[]{:S(2)}, u32[]{:S(2)}) collective-permute-start(bf16[40,1024]{1,0:T(8,128)(2,1)S(1)} %join.1), channel_id=1, source_target_pairs={{0,6},{1,1},{2,14},{3,9},{4,22},{5,17},{6,30},{7,25},{8,4},{9,3},{... | collective-permute-start | bytes 245768 | tf_op jit(solution)/shard_map/ppermute | solution.py:672
  11.5 0.0 copy-start.4
  11.5 0.0 copy-start.7
  11.5 0.0 copy-start.10
  11.5 0.0 slice-start
  11.6 0.3 prepare.1
  11.8 0.2 fusion
  12.0 0.1 pad_maximum_fusion.1
  12.1 1.7 %collective-permute-done.2 = bf16[40,1024]{1,0:T(8,128)(2,1)S(1)} collective-permute-done((bf16[40,1024]{1,0:T(8,128)(2,1)S(1)}, bf16[40,1024]{1,0:T(8,128)(2,1)S(1)}, u32[]{:S(2)}, u32[]{:S(2)}) %collective-permute-start.2) | collective-permute-done | bytes 81952 | tf_op jit(solution)/shard_map/ppermute | solution.py:672
  13.8 0.1 collective-permute-start.3
  13.9 1.4 %collective-permute-done.3.refs_1_ = bf16[80,1024]{1,0:T(8,128)(2,1)S(1)} collective-permute-done((bf16[80,1024]{1,0:T(8,128)(2,1)S(1)}, bf16[80,1024]{1,0:T(8,128)(2,1)S(1)}, u32[]{:S(2)}, u32[]{:S(2)}) %collective-permute-start.3) | collective-permute-done | bytes 163872 | tf_op jit(solution)/shard_map/ppermute | solution.py:25
  15.3 0.6 project.1
  15.9 2.8 %collective-permute-start.4 = (bf16[40,1152]{1,0:T(8,128)(2,1)S(1)}, bf16[40,1152]{1,0:T(8,128)(2,1)S(1)}, u32[]{:S(2)}, u32[]{:S(2)}) collective-permute-start(bf16[40,1152]{1,0:T(8,128)(2,1)S(1)} %get-tuple-element.72), channel_id=1, source_target_pairs={{0,8},{8,0},{16,24},{24,16},{1,9},{9,1},{17,25},{25,17},{2,10},{10... | collective-permute-start | bytes 276488 | tf_op jit(solution)/shard_map/ppermute | solution.py:40
  18.7 0.9 %collective-permute-start.5 = (bf16[40,1152]{1,0:T(8,128)(2,1)S(1)}, bf16[40,1152]{1,0:T(8,128)(2,1)S(1)}, u32[]{:S(2)}, u32[]{:S(2)}) collective-permute-start(bf16[40,1152]{1,0:T(8,128)(2,1)S(1)} %get-tuple-element.73), channel_id=1, source_target_pairs={{0,16},{8,24},{16,0},{24,8},{1,17},{9,25},{17,1},{25,9},{2,18},{10... | collective-permute-start | bytes 276488 | tf_op jit(solution)/shard_map/ppermute | solution.py:40
  19.7 0.6 collective-permute-start.6
  20.2 1.4 %collective-permute-done.4.refs_4_ = bf16[40,1152]{1,0:T(8,128)(2,1)S(1)} collective-permute-done((bf16[40,1152]{1,0:T(8,128)(2,1)S(1)}, bf16[40,1152]{1,0:T(8,128)(2,1)S(1)}, u32[]{:S(2)}, u32[]{:S(2)}) %collective-permute-start.4) | collective-permute-done | bytes 92192 | tf_op jit(solution)/shard_map/ppermute | solution.py:40
  21.7 3.6 %collective-permute-done.5.refs_5_ = bf16[40,1152]{1,0:T(8,128)(2,1)S(1)} collective-permute-done((bf16[40,1152]{1,0:T(8,128)(2,1)S(1)}, bf16[40,1152]{1,0:T(8,128)(2,1)S(1)}, u32[]{:S(2)}, u32[]{:S(2)}) %collective-permute-start.5) | collective-permute-done | bytes 92192 | tf_op jit(solution)/shard_map/ppermute | solution.py:40
  25.3 1.2 %read_state.1 = (bf16[40,256]{1,0:T(8,128)(2,1)S(1)}, f32[40,256]{1,0:T(8,128)S(1)}, f32[40,256]{1,0:T(8,128)S(1)}) custom-call(f32[40,128]{1,0:T(8,128)S(1)} %get-tuple-element.67.refs_0_, f32[40,128]{1,0:T(8,128)S(1)} %get-tuple-element.68.refs_1_, f32[1,256]{1,0:T(1,128)S(1)} %bitcast.12, f32[40,1152]{1,0:T(8,128)S(1)} %get-tuple-element.71.refs_3_, ...), custom_call_target="tpu_custom_call" | custom-call | flops 5000000000 | bytes 30000000 | tf_op jit(solution)/shard_map/read_state/pallas_call | solution.py:343
  26.4 0.6 collective-permute-start.7
  27.0 1.7 %collective-permute-start.8 = (bf16[40,256]{1,0:T(8,128)(2,1)S(1)}, bf16[40,256]{1,0:T(8,128)(2,1)S(1)}, u32[]{:S(2)}, u32[]{:S(2)}) collective-permute-start(bf16[40,256]{1,0:T(8,128)(2,1)S(1)} %get-tuple-element.78.own), channel_id=1, source_target_pairs={{0,4},{1,5},{2,6},{3,7},{4,0},{5,1},{6,2},{7,3},{8,12},{9,13},{10,... | collective-permute-start | bytes 61448 | tf_op jit(solution)/shard_map/ppermute | solution.py:32
  28.8 2.1 %collective-permute-start.9 = (bf16[40,256]{1,0:T(8,128)(2,1)S(1)}, bf16[40,256]{1,0:T(8,128)(2,1)S(1)}, u32[]{:S(2)}, u32[]{:S(2)}) collective-permute-start(bf16[40,256]{1,0:T(8,128)(2,1)S(1)} %get-tuple-element.78.own), channel_id=1, source_target_pairs={{0,6},{1,7},{2,4},{3,5},{4,2},{5,3},{6,0},{7,1},{8,14},{9,15},{10,... | collective-permute-start | bytes 61448 | tf_op jit(solution)/shard_map/ppermute | solution.py:32
  30.8 1.6 %update_state.2.refs_4_ = f32[40,2,128,128]{3,2,1,0:T(8,128)} custom-call(f32[40,256]{1,0:T(8,128)S(1)} %get-tuple-element.76.refs_0_, f32[40,256]{1,0:T(8,128)S(1)} %get-tuple-element.77.refs_1_, f32[40,2,128,128]{3,2,1,0:T(8,128)S(1)} %bitcast.6), custom_call_target="tpu_custom_call" | custom-call | flops 5000000000 | bytes 30000000 | tf_op jit(solution)/shard_map/update_state/pallas_call | solution.py:387
  32.5 1.9 %collective-permute-done.9 = bf16[40,256]{1,0:T(8,128)(2,1)S(1)} collective-permute-done((bf16[40,256]{1,0:T(8,128)(2,1)S(1)}, bf16[40,256]{1,0:T(8,128)(2,1)S(1)}, u32[]{:S(2)}, u32[]{:S(2)}) %collective-permute-start.9) | collective-permute-done | bytes 20512 | tf_op jit(solution)/shard_map/ppermute | solution.py:32
  34.4 0.6 collective-permute-start.11
  34.9 0.3 shard_map.167.total_ref
  35.2 0.3 collective-permute-done.10.other
  35.5 0.3 collective-permute-done.11.others
  35.8 0.4 shard_map.168
  36.3 1.6 %collective-permute-start.12 = (bf16[10,640]{1,0:T(8,128)(2,1)S(1)}, bf16[10,640]{1,0:T(8,128)(2,1)S(1)}, u32[]{:S(2)}, u32[]{:S(2)}) collective-permute-start(bf16[10,640]{1,0:T(8,128)(2,1)S(1)} %get-tuple-element.92), channel_id=1, source_target_pairs={{0,8},{8,0},{16,24},{24,16},{1,9},{9,1},{17,25},{25,17},{2,10},{10... | collective-permute-start | bytes 38408 | tf_op jit(solution)/shard_map/ppermute | solution.py:40
  37.9 0.9 %collective-permute-start.13 = (bf16[10,640]{1,0:T(8,128)(2,1)S(1)}, bf16[10,640]{1,0:T(8,128)(2,1)S(1)}, u32[]{:S(2)}, u32[]{:S(2)}) collective-permute-start(bf16[10,640]{1,0:T(8,128)(2,1)S(1)} %get-tuple-element.93), channel_id=1, source_target_pairs={{0,16},{8,24},{16,0},{24,8},{1,17},{9,25},{17,1},{25,9},{2,18},{10... | collective-permute-start | bytes 38408 | tf_op jit(solution)/shard_map/ppermute | solution.py:40
  38.8 1.1 %collective-permute-start.14 = (bf16[10,640]{1,0:T(8,128)(2,1)S(1)}, bf16[10,640]{1,0:T(8,128)(2,1)S(1)}, u32[]{:S(2)}, u32[]{:S(2)}) collective-permute-start(bf16[10,640]{1,0:T(8,128)(2,1)S(1)} %get-tuple-element.94), channel_id=1, source_target_pairs={{0,24},{8,16},{16,8},{24,0},{1,25},{9,17},{17,9},{25,1},{2,26},{10... | collective-permute-start | bytes 38408 | tf_op jit(solution)/shard_map/ppermute | solution.py:40
  39.8 2.6 %update_state.3 = f32[40,2,128,128]{3,2,1,0:T(8,128)} custom-call(f32[40,256]{1,0:T(8,128)S(1)} %get-tuple-element.76.refs_0_, f32[40,256]{1,0:T(8,128)S(1)} %get-tuple-element.77.refs_1_, f32[40,2,128,128]{3,2,1,0:T(8,128)S(1)} %bitcast.6, bf16[40,512]{1,0:T(8,128)(2,1)S(1)} %get-tuple-element.90.refs_3_.refs_0_, ...), custom_call_target="tpu_custom_call", output_to_operand_aliasing={{}: (4, {})} | custom-call | flops 5000000000 | bytes 30000000 | tf_op jit(solution)/shard_map/update_state/pallas_call | solution.py:387
  42.4 1.0 %collective-permute-done.14.refs_3_ = bf16[10,640]{1,0:T(8,128)(2,1)S(1)} collective-permute-done((bf16[10,640]{1,0:T(8,128)(2,1)S(1)}, bf16[10,640]{1,0:T(8,128)(2,1)S(1)}, u32[]{:S(2)}, u32[]{:S(2)}) %collective-permute-start.14) | collective-permute-done | bytes 12832 | tf_op jit(solution)/shard_map/ppermute | solution.py:40
  43.5 0.1 collective-permute-start.16
  43.6 0.1 collective-permute-start.15
  43.7 1.7 %collective-permute-start.17 = (bf16[40,512]{1,0:T(8,128)(2,1)S(1)}, bf16[40,512]{1,0:T(8,128)(2,1)S(1)}, u32[]{:S(2)}, u32[]{:S(2)}) collective-permute-start(bf16[40,512]{1,0:T(8,128)(2,1)S(1)} %pad_maximum_fusion.own), channel_id=1, source_target_pairs={{0,4},{1,5},{2,6},{3,7},{4,0},{5,1},{6,2},{7,3},{8,12},{9,13},{10,... | collective-permute-start | bytes 122888 | tf_op jit(solution)/shard_map/ppermute | solution.py:32
  45.4 2.6 %collective-permute-start.18 = (bf16[40,512]{1,0:T(8,128)(2,1)S(1)}, bf16[40,512]{1,0:T(8,128)(2,1)S(1)}, u32[]{:S(2)}, u32[]{:S(2)}) collective-permute-start(bf16[40,512]{1,0:T(8,128)(2,1)S(1)} %pad_maximum_fusion.own), channel_id=1, source_target_pairs={{0,6},{1,7},{2,4},{3,5},{4,2},{5,3},{6,0},{7,1},{8,14},{9,15},{10,... | collective-permute-start | bytes 122888 | tf_op jit(solution)/shard_map/ppermute | solution.py:32
  48.0 1.0 %collective-permute-done.17 = bf16[40,512]{1,0:T(8,128)(2,1)S(1)} collective-permute-done((bf16[40,512]{1,0:T(8,128)(2,1)S(1)}, bf16[40,512]{1,0:T(8,128)(2,1)S(1)}, u32[]{:S(2)}, u32[]{:S(2)}) %collective-permute-start.17) | collective-permute-done | bytes 40992 | tf_op jit(solution)/shard_map/ppermute | solution.py:32
  49.0 2.2 %collective-permute-done.18 = bf16[40,512]{1,0:T(8,128)(2,1)S(1)} collective-permute-done((bf16[40,512]{1,0:T(8,128)(2,1)S(1)}, bf16[40,512]{1,0:T(8,128)(2,1)S(1)}, u32[]{:S(2)}, u32[]{:S(2)}) %collective-permute-start.18) | collective-permute-done | bytes 40992 | tf_op jit(solution)/shard_map/ppermute | solution.py:32
  51.2 0.9 %shard_map.169 = (f32[2,40,256]{2,1,0:T(8,128)S(1)}, f32[2,40,256]{2,1,0:T(8,128)S(1)}, f32[40,128]{1,0:T(8,128)S(1)}) custom-call(bf16[40,512]{1,0:T(8,128)(2,1)S(1)} %pad_maximum_fusion.own, bf16[120,512]{1,0:T(8,128)(2,1)S(1)} %constant_dynamic-update-slice_fusion.5.rest, f32[1,4096]{1,0:T(1,128)S(1)} %bitcast.8, bf16[2,4096,256]{2,1,0:T(8,128)(2,1)S(1)} %copy-done, ...), custom_call_target="tpu_custom_call" | custom-call | flops 5000000000 | bytes 30000000 | tf_op jit(solution)/shard_map/pallas_call | solution.py:51
  52.1 0.4 collective-permute-done.19.others
  52.5 0.9 %shard_map.170.own = bf16[2,40,256]{2,1,0:T(8,128)(2,1)S(1)} custom-call(bf16[40,512]{1,0:T(8,128)(2,1)S(1)} %collective-permute-done.15.other, bf16[120,512]{1,0:T(8,128)(2,1)S(1)} %collective-permute-done.19.others, f32[1,4096]{1,0:T(1,128)S(1)} %bitcast.9, bf16[2,4096,256]{2,1,0:T(8,128)(2,1)S(1)} %copy-done, bf16[2,4096,256]{2,1,0:T(8,128)(2,1)S(1)} %copy-done.1, ...), custom_call_target="tpu_custom_call" | custom-call | flops 5000000000 | bytes 30000000 | tf_op jit(solution)/shard_map/pallas_call | solution.py:51
  53.4 0.7 collective-permute-start.21
  54.0 2.5 %collective-permute-start.22 = (bf16[2,40,256]{2,1,0:T(8,128)(2,1)S(1)}, bf16[2,40,256]{2,1,0:T(8,128)(2,1)S(1)}, u32[]{:S(2)}, u32[]{:S(2)}) collective-permute-start(bf16[2,40,256]{2,1,0:T(8,128)(2,1)S(1)} %shard_map.170.own), channel_id=1, source_target_pairs={{0,4},{1,5},{2,6},{3,7},{4,0},{5,1},{6,2},{7,3},{8,12},{9,13},{10,... | collective-permute-start | bytes 122888 | tf_op jit(solution)/shard_map/ppermute | solution.py:32
  56.6 1.3 %collective-permute-start.23 = (bf16[2,40,256]{2,1,0:T(8,128)(2,1)S(1)}, bf16[2,40,256]{2,1,0:T(8,128)(2,1)S(1)}, u32[]{:S(2)}, u32[]{:S(2)}) collective-permute-start(bf16[2,40,256]{2,1,0:T(8,128)(2,1)S(1)} %shard_map.170.own), channel_id=1, source_target_pairs={{0,6},{1,7},{2,4},{3,5},{4,2},{5,3},{6,0},{7,1},{8,14},{9,15},{10,... | collective-permute-start | bytes 122888 | tf_op jit(solution)/shard_map/ppermute | solution.py:32
  57.8 1.1 %collective-permute-done.22 = bf16[2,40,256]{2,1,0:T(8,128)(2,1)S(1)} collective-permute-done((bf16[2,40,256]{2,1,0:T(8,128)(2,1)S(1)}, bf16[2,40,256]{2,1,0:T(8,128)(2,1)S(1)}, u32[]{:S(2)}, u32[]{:S(2)}) %collective-permute-start.22) | collective-permute-done | bytes 40992 | tf_op jit(solution)/shard_map/ppermute | solution.py:32
  59.0 3.4 %collective-permute-done.23 = bf16[2,40,256]{2,1,0:T(8,128)(2,1)S(1)} collective-permute-done((bf16[2,40,256]{2,1,0:T(8,128)(2,1)S(1)}, bf16[2,40,256]{2,1,0:T(8,128)(2,1)S(1)}, u32[]{:S(2)}, u32[]{:S(2)}) %collective-permute-start.23) | collective-permute-done | bytes 40992 | tf_op jit(solution)/shard_map/ppermute | solution.py:32
  62.4 0.5 shard_map.171.totals_ref
  62.9 0.0 collective-permute-done.20.other
  62.9 0.8 %collective-permute-done.24.others = bf16[2,120,256]{2,1,0:T(8,128)(2,1)S(1)} collective-permute-done((bf16[2,120,256]{2,1,0:T(8,128)(2,1)S(1)}, bf16[2,120,256]{2,1,0:T(8,128)(2,1)S(1)}, u32[]{:S(2)}, u32[]{:S(2)}) %collective-permute-start.24) | collective-permute-done | bytes 122912 | tf_op jit(solution)/shard_map/ppermute | solution.py:25
  63.7 0.5 shard_map.172
  64.2 0.9 %collective-permute-start.25 = (bf16[10,512]{1,0:T(8,128)(2,1)S(1)}, bf16[10,512]{1,0:T(8,128)(2,1)S(1)}, u32[]{:S(2)}, u32[]{:S(2)}) collective-permute-start(bf16[10,512]{1,0:T(8,128)(2,1)S(1)} %get-tuple-element.104), channel_id=1, source_target_pairs={{0,8},{8,0},{16,24},{24,16},{1,9},{9,1},{17,25},{25,17},{2,10},{10... | collective-permute-start | bytes 30728 | tf_op jit(solution)/shard_map/ppermute | solution.py:40
  65.1 0.8 %collective-permute-start.26 = (bf16[10,512]{1,0:T(8,128)(2,1)S(1)}, bf16[10,512]{1,0:T(8,128)(2,1)S(1)}, u32[]{:S(2)}, u32[]{:S(2)}) collective-permute-start(bf16[10,512]{1,0:T(8,128)(2,1)S(1)} %get-tuple-element.105), channel_id=1, source_target_pairs={{0,16},{8,24},{16,0},{24,8},{1,17},{9,25},{17,1},{25,9},{2,18},{10... | collective-permute-start | bytes 30728 | tf_op jit(solution)/shard_map/ppermute | solution.py:40
  65.9 1.9 %collective-permute-start.27 = (bf16[10,512]{1,0:T(8,128)(2,1)S(1)}, bf16[10,512]{1,0:T(8,128)(2,1)S(1)}, u32[]{:S(2)}, u32[]{:S(2)}) collective-permute-start(bf16[10,512]{1,0:T(8,128)(2,1)S(1)} %get-tuple-element.106), channel_id=1, source_target_pairs={{0,24},{8,16},{16,8},{24,0},{1,25},{9,17},{17,9},{25,1},{2,26},{10... | collective-permute-start | bytes 30728 | tf_op jit(solution)/shard_map/ppermute | solution.py:40
  67.8 0.2 collective-permute-done.25.refs_6_
  68.0 0.8 %collective-permute-done.26.refs_7_ = bf16[10,512]{1,0:T(8,128)(2,1)S(1)} collective-permute-done((bf16[10,512]{1,0:T(8,128)(2,1)S(1)}, bf16[10,512]{1,0:T(8,128)(2,1)S(1)}, u32[]{:S(2)}, u32[]{:S(2)}) %collective-permute-start.26) | collective-permute-done | bytes 10272 | tf_op jit(solution)/shard_map/ppermute | solution.py:40
  68.9 1.7 %collective-permute-done.27.refs_8_ = bf16[10,512]{1,0:T(8,128)(2,1)S(1)} collective-permute-done((bf16[10,512]{1,0:T(8,128)(2,1)S(1)}, bf16[10,512]{1,0:T(8,128)(2,1)S(1)}, u32[]{:S(2)}, u32[]{:S(2)}) %collective-permute-start.27) | collective-permute-done | bytes 10272 | tf_op jit(solution)/shard_map/ppermute | solution.py:40
  70.6 0.9 %finish.1 = bf16[40,512]{1,0:T(8,128)(2,1)} custom-call(bf16[40,512]{1,0:T(8,128)(2,1)S(1)} %get-tuple-element.90.refs_3_.refs_0_, bf16[10,40]{1,0:T(8,128)(2,1)S(1)} %get-tuple-element.82.refs_0_.refs_1_, bf16[10,40]{1,0:T(8,128)(2,1)S(1)} %get-tuple-element.83.refs_1_.refs_2_, bf16[10,40]{1,0:T(8,128)(2,1)S(1)} %get-tuple-element.84.refs_2_.refs_3_, ...), custom_call_target="tpu_custom_call" | custom-call | flops 2500000000 | bytes 15000000 | tf_op jit(solution)/shard_map/finish/pallas_call | solution.py:603
  (63 shorter events, 0.2 us)
Async XLA Ops:
  0.6 1.6 %collective-permute-start = (bf16[40,512]{1,0:T(8,128)(2,1)}, bf16[40,512]{1,0:T(8,128)(2,1)S(1)}, u32[]{:S(2)}, u32[]{:S(2)}) collective-permute-start(bf16[40,512]{1,0:T(8,128)(2,1)} %hidden_ref.1), channel_id=1, source_target_pairs={{0,1},{1,0},{2,3},{3,2},{4,5},{5,4},{6,7},{7,6},{8,9},{9,8},{10,11... | collective-permute-start | bytes 122888 | tf_op jit(solution)/shard_map/ppermute | solution.py:25
  1.2 0.8 %copy-start.8 = (bf16[40,512]{1,0:T(8,128)(2,1)S(1)}, bf16[40,512]{1,0:T(8,128)(2,1)}, u32[]{:S(2)}) copy-start(bf16[40,512]{1,0:T(8,128)(2,1)} %hidden_ref.1) | copy-start | bytes 122884
  2.0 9.5 %copy-start.15 = (s32[40]{0:T(128)S(1)}, s32[40]{0:T(128)}, u32[]{:S(2)}) copy-start(s32[40]{0:T(128)} %param.17) | copy-start | bytes 484
  2.0 9.5 %copy-start.12 = (s32[40,2]{0,1:T(2,128)S(1)}, s32[40,2]{0,1:T(2,128)}, u32[]{:S(2)}) copy-start(s32[40,2]{0,1:T(2,128)} %param.30) | copy-start | bytes 964
  2.0 9.5 %copy-start.13 = (f32[40,2]{0,1:T(2,128)S(1)}, f32[40,2]{0,1:T(2,128)}, u32[]{:S(2)}) copy-start(f32[40,2]{0,1:T(2,128)} %param.31) | copy-start | bytes 964
  2.3 9.8 %collective-permute-start.1 = (bf16[40,1024]{1,0:T(8,128)(2,1)S(1)}, bf16[40,1024]{1,0:T(8,128)(2,1)S(1)}, u32[]{:S(2)}, u32[]{:S(2)}) collective-permute-start(bf16[40,1024]{1,0:T(8,128)(2,1)S(1)} %join.1), channel_id=1, source_target_pairs={{0,4},{1,3},{2,12},{3,11},{4,20},{5,19},{6,28},{7,27},{8,6},{9,1},... | collective-permute-start | bytes 245768 | tf_op jit(solution)/shard_map/ppermute | solution.py:672
  6.2 7.6 %collective-permute-start.2 = (bf16[40,1024]{1,0:T(8,128)(2,1)S(1)}, bf16[40,1024]{1,0:T(8,128)(2,1)S(1)}, u32[]{:S(2)}, u32[]{:S(2)}) collective-permute-start(bf16[40,1024]{1,0:T(8,128)(2,1)S(1)} %join.1), channel_id=1, source_target_pairs={{0,6},{1,1},{2,14},{3,9},{4,22},{5,17},{6,30},{7,25},{8,4},{9,3},{... | collective-permute-start | bytes 245768 | tf_op jit(solution)/shard_map/ppermute | solution.py:672
  11.5 3.8 %copy-start.4 = (bf16[1024,256]{1,0:T(8,128)(2,1)S(1)}, bf16[1024,256]{1,0:T(8,128)(2,1)}, u32[]{:S(2)}) copy-start(bf16[1024,256]{1,0:T(8,128)(2,1)} %refs_2_.3) | copy-start | bytes 1572868
  11.5 3.8 %copy-start.5 = (bf16[1024,256]{1,0:T(8,128)(2,1)S(1)}, bf16[1024,256]{1,0:T(8,128)(2,1)}, u32[]{:S(2)}) copy-start(bf16[1024,256]{1,0:T(8,128)(2,1)} %refs_3_.1) | copy-start | bytes 1572868
  11.5 3.8 %copy-start.6 = (bf16[1024,256]{1,0:T(8,128)(2,1)S(1)}, bf16[1024,256]{1,0:T(8,128)(2,1)}, u32[]{:S(2)}) copy-start(bf16[1024,256]{1,0:T(8,128)(2,1)} %refs_4_.1) | copy-start | bytes 1572868
  11.5 3.8 %copy-start.7 = (bf16[1024,256]{1,0:T(8,128)(2,1)S(1)}, bf16[1024,256]{1,0:T(8,128)(2,1)}, u32[]{:S(2)}) copy-start(bf16[1024,256]{1,0:T(8,128)(2,1)} %refs_5_.1) | copy-start | bytes 1572868
  11.5 3.8 %copy-start.10 = (f32[4096]{0:T(1024)S(1)}, f32[4096]{0:T(1024)}, u32[]{:S(2)}) copy-start(f32[4096]{0:T(1024)} %param.25) | copy-start | bytes 49156
  11.5 13.7 %slice-start = ((s8[5242880]{0:T(1024)(128)(4,1)}), s8[4194304]{0:T(1024)(128)(4,1)S(1)}, s32[]{:S(2)}) async-start(s8[5242880]{0:T(1024)(128)(4,1)} %bitcast.5), calls=%async_computation | async-start | bytes 8388608
  13.8 11.5 %slice-start.1 = ((s8[5242880]{0:T(1024)(128)(4,1)}), s8[1048576]{0:T(1024)(128)(4,1)S(1)}, s32[]{:S(2)}) async-start(s8[5242880]{0:T(1024)(128)(4,1)} %bitcast.5), calls=%async_computation.1 | async-start | bytes 2097152
  13.8 1.5 %collective-permute-start.3 = (bf16[80,1024]{1,0:T(8,128)(2,1)S(1)}, bf16[80,1024]{1,0:T(8,128)(2,1)S(1)}, u32[]{:S(2)}, u32[]{:S(2)}) collective-permute-start(bf16[80,1024]{1,0:T(8,128)(2,1)S(1)} %constant_dynamic-update-slice_fusion.refs_0_), channel_id=1, source_target_pairs={{0,1},{1,0},{2,3},{3,2},{4,5},{5,4},{6,7},{7,6},{8,9},{9,8},{10,11... | collective-permute-start | bytes 491528 | tf_op jit(solution)/shard_map/ppermute | solution.py:25
  15.3 9.9 %copy-start.14 = (f32[256]{0:T(256)S(1)}, f32[256]{0:T(256)}, u32[]{:S(2)}) copy-start(f32[256]{0:T(256)} %param.23) | copy-start | bytes 3076
  15.9 5.8 %collective-permute-start.4 = (bf16[40,1152]{1,0:T(8,128)(2,1)S(1)}, bf16[40,1152]{1,0:T(8,128)(2,1)S(1)}, u32[]{:S(2)}, u32[]{:S(2)}) collective-permute-start(bf16[40,1152]{1,0:T(8,128)(2,1)S(1)} %get-tuple-element.72), channel_id=1, source_target_pairs={{0,8},{8,0},{16,24},{24,16},{1,9},{9,1},{17,25},{25,17},{2,10},{10... | collective-permute-start | bytes 276488 | tf_op jit(solution)/shard_map/ppermute | solution.py:40
  18.7 6.5 %collective-permute-start.5 = (bf16[40,1152]{1,0:T(8,128)(2,1)S(1)}, bf16[40,1152]{1,0:T(8,128)(2,1)S(1)}, u32[]{:S(2)}, u32[]{:S(2)}) collective-permute-start(bf16[40,1152]{1,0:T(8,128)(2,1)S(1)} %get-tuple-element.73), channel_id=1, source_target_pairs={{0,16},{8,24},{16,0},{24,8},{1,17},{9,25},{17,1},{25,9},{2,18},{10... | collective-permute-start | bytes 276488 | tf_op jit(solution)/shard_map/ppermute | solution.py:40
  19.7 5.6 %collective-permute-start.6 = (bf16[40,1152]{1,0:T(8,128)(2,1)S(1)}, bf16[40,1152]{1,0:T(8,128)(2,1)S(1)}, u32[]{:S(2)}, u32[]{:S(2)}) collective-permute-start(bf16[40,1152]{1,0:T(8,128)(2,1)S(1)} %get-tuple-element.74), channel_id=1, source_target_pairs={{0,24},{8,16},{16,8},{24,0},{1,25},{9,17},{17,9},{25,1},{2,26},{10... | collective-permute-start | bytes 276488 | tf_op jit(solution)/shard_map/ppermute | solution.py:40
  26.4 6.1 %collective-permute-start.7 = (bf16[40,256]{1,0:T(8,128)(2,1)S(1)}, bf16[40,256]{1,0:T(8,128)(2,1)S(1)}, u32[]{:S(2)}, u32[]{:S(2)}) collective-permute-start(bf16[40,256]{1,0:T(8,128)(2,1)S(1)} %get-tuple-element.78.own), channel_id=1, source_target_pairs={{0,2},{1,3},{2,0},{3,1},{4,6},{5,7},{6,4},{7,5},{8,10},{9,11},{10,... | collective-permute-start | bytes 61448 | tf_op jit(solution)/shard_map/ppermute | solution.py:32
  27.0 5.4 %collective-permute-start.8 = (bf16[40,256]{1,0:T(8,128)(2,1)S(1)}, bf16[40,256]{1,0:T(8,128)(2,1)S(1)}, u32[]{:S(2)}, u32[]{:S(2)}) collective-permute-start(bf16[40,256]{1,0:T(8,128)(2,1)S(1)} %get-tuple-element.78.own), channel_id=1, source_target_pairs={{0,4},{1,5},{2,6},{3,7},{4,0},{5,1},{6,2},{7,3},{8,12},{9,13},{10,... | collective-permute-start | bytes 61448 | tf_op jit(solution)/shard_map/ppermute | solution.py:32
  28.8 5.6 %collective-permute-start.9 = (bf16[40,256]{1,0:T(8,128)(2,1)S(1)}, bf16[40,256]{1,0:T(8,128)(2,1)S(1)}, u32[]{:S(2)}, u32[]{:S(2)}) collective-permute-start(bf16[40,256]{1,0:T(8,128)(2,1)S(1)} %get-tuple-element.78.own), channel_id=1, source_target_pairs={{0,6},{1,7},{2,4},{3,5},{4,2},{5,3},{6,0},{7,1},{8,14},{9,15},{10,... | collective-permute-start | bytes 61448 | tf_op jit(solution)/shard_map/ppermute | solution.py:32
  30.8 4.1 %copy-start.3 = (bf16[2048,512]{1,0:T(8,128)(2,1)S(1)}, bf16[2048,512]{1,0:T(8,128)(2,1)}, u32[]{:S(2)}) copy-start(bf16[2048,512]{1,0:T(8,128)(2,1)} %weight_ref.3) | copy-start | bytes 6291460
  30.8 4.1 %copy-start.9 = (bf16[40,512]{1,0:T(8,128)(2,1)S(1)}, bf16[40,512]{1,0:T(8,128)(2,1)}, u32[]{:S(2)}) copy-start(bf16[40,512]{1,0:T(8,128)(2,1)} %hidden_ref.1) | copy-start | bytes 122884
  34.4 1.2 %collective-permute-start.10 = (bf16[40,256]{1,0:T(8,128)(2,1)S(1)}, bf16[40,256]{1,0:T(8,128)(2,1)S(1)}, u32[]{:S(2)}, u32[]{:S(2)}) collective-permute-start(bf16[40,256]{1,0:T(8,128)(2,1)S(1)} %get-tuple-element.78.own), channel_id=1, source_target_pairs={{0,1},{1,0},{2,3},{3,2},{4,5},{5,4},{6,7},{7,6},{8,9},{9,8},{10,11... | collective-permute-start | bytes 61448 | tf_op jit(solution)/shard_map/ppermute | solution.py:25
  34.4 1.5 %collective-permute-start.11 = (bf16[120,256]{1,0:T(8,128)(2,1)S(1)}, bf16[120,256]{1,0:T(8,128)(2,1)S(1)}, u32[]{:S(2)}, u32[]{:S(2)}) collective-permute-start(bf16[120,256]{1,0:T(8,128)(2,1)S(1)} %constant_dynamic-update-slice_fusion.2.rest), channel_id=1, source_target_pairs={{0,1},{1,0},{2,3},{3,2},{4,5},{5,4},{6,7},{7,6},{8,9},{9,8},{10,11... | collective-permute-start | bytes 184328 | tf_op jit(solution)/shard_map/ppermute | solution.py:25
  36.3 6.2 %collective-permute-start.12 = (bf16[10,640]{1,0:T(8,128)(2,1)S(1)}, bf16[10,640]{1,0:T(8,128)(2,1)S(1)}, u32[]{:S(2)}, u32[]{:S(2)}) collective-permute-start(bf16[10,640]{1,0:T(8,128)(2,1)S(1)} %get-tuple-element.92), channel_id=1, source_target_pairs={{0,8},{8,0},{16,24},{24,16},{1,9},{9,1},{17,25},{25,17},{2,10},{10... | collective-permute-start | bytes 38408 | tf_op jit(solution)/shard_map/ppermute | solution.py:40
  37.9 4.6 %collective-permute-start.13 = (bf16[10,640]{1,0:T(8,128)(2,1)S(1)}, bf16[10,640]{1,0:T(8,128)(2,1)S(1)}, u32[]{:S(2)}, u32[]{:S(2)}) collective-permute-start(bf16[10,640]{1,0:T(8,128)(2,1)S(1)} %get-tuple-element.93), channel_id=1, source_target_pairs={{0,16},{8,24},{16,0},{24,8},{1,17},{9,25},{17,1},{25,9},{2,18},{10... | collective-permute-start | bytes 38408 | tf_op jit(solution)/shard_map/ppermute | solution.py:40
  38.8 4.7 %collective-permute-start.14 = (bf16[10,640]{1,0:T(8,128)(2,1)S(1)}, bf16[10,640]{1,0:T(8,128)(2,1)S(1)}, u32[]{:S(2)}, u32[]{:S(2)}) collective-permute-start(bf16[10,640]{1,0:T(8,128)(2,1)S(1)} %get-tuple-element.94), channel_id=1, source_target_pairs={{0,24},{8,16},{16,8},{24,0},{1,25},{9,17},{17,9},{25,1},{2,26},{10... | collective-permute-start | bytes 38408 | tf_op jit(solution)/shard_map/ppermute | solution.py:40
  39.8 11.4 %copy-start = (bf16[2,4096,256]{2,1,0:T(8,128)(2,1)S(1)}, bf16[2,4096,256]{2,1,0:T(8,128)(2,1)}, u32[]{:S(2)}) copy-start(bf16[2,4096,256]{2,1,0:T(8,128)(2,1)} %gate_ref.3) | copy-start | bytes 12582916
  39.8 11.4 %copy-start.1 = (bf16[2,4096,256]{2,1,0:T(8,128)(2,1)S(1)}, bf16[2,4096,256]{2,1,0:T(8,128)(2,1)}, u32[]{:S(2)}) copy-start(bf16[2,4096,256]{2,1,0:T(8,128)(2,1)} %up_ref.3) | copy-start | bytes 12582916
  39.8 11.4 %copy-start.11 = (f32[4096]{0:T(1024)S(1)}, f32[4096]{0:T(1024)}, u32[]{:S(2)}) copy-start(f32[4096]{0:T(1024)} %param.26) | copy-start | bytes 49156
  43.5 4.5 %collective-permute-start.16 = (bf16[40,512]{1,0:T(8,128)(2,1)S(1)}, bf16[40,512]{1,0:T(8,128)(2,1)S(1)}, u32[]{:S(2)}, u32[]{:S(2)}) collective-permute-start(bf16[40,512]{1,0:T(8,128)(2,1)S(1)} %pad_maximum_fusion.own), channel_id=1, source_target_pairs={{0,2},{1,3},{2,0},{3,1},{4,6},{5,7},{6,4},{7,5},{8,10},{9,11},{10,... | collective-permute-start | bytes 122888 | tf_op jit(solution)/shard_map/ppermute | solution.py:32
  43.6 8.5 %collective-permute-start.15 = (bf16[40,512]{1,0:T(8,128)(2,1)S(1)}, bf16[40,512]{1,0:T(8,128)(2,1)S(1)}, u32[]{:S(2)}, u32[]{:S(2)}) collective-permute-start(bf16[40,512]{1,0:T(8,128)(2,1)S(1)} %pad_maximum_fusion.own), channel_id=1, source_target_pairs={{0,1},{1,0},{2,3},{3,2},{4,5},{5,4},{6,7},{7,6},{8,9},{9,8},{10,11... | collective-permute-start | bytes 122888 | tf_op jit(solution)/shard_map/ppermute | solution.py:25
  43.7 5.4 %collective-permute-start.17 = (bf16[40,512]{1,0:T(8,128)(2,1)S(1)}, bf16[40,512]{1,0:T(8,128)(2,1)S(1)}, u32[]{:S(2)}, u32[]{:S(2)}) collective-permute-start(bf16[40,512]{1,0:T(8,128)(2,1)S(1)} %pad_maximum_fusion.own), channel_id=1, source_target_pairs={{0,4},{1,5},{2,6},{3,7},{4,0},{5,1},{6,2},{7,3},{8,12},{9,13},{10,... | collective-permute-start | bytes 122888 | tf_op jit(solution)/shard_map/ppermute | solution.py:32
  45.4 5.8 %collective-permute-start.18 = (bf16[40,512]{1,0:T(8,128)(2,1)S(1)}, bf16[40,512]{1,0:T(8,128)(2,1)S(1)}, u32[]{:S(2)}, u32[]{:S(2)}) collective-permute-start(bf16[40,512]{1,0:T(8,128)(2,1)S(1)} %pad_maximum_fusion.own), channel_id=1, source_target_pairs={{0,6},{1,7},{2,4},{3,5},{4,2},{5,3},{6,0},{7,1},{8,14},{9,15},{10,... | collective-permute-start | bytes 122888 | tf_op jit(solution)/shard_map/ppermute | solution.py:32
  51.2 1.3 %collective-permute-start.19 = (bf16[120,512]{1,0:T(8,128)(2,1)S(1)}, bf16[120,512]{1,0:T(8,128)(2,1)S(1)}, u32[]{:S(2)}, u32[]{:S(2)}) collective-permute-start(bf16[120,512]{1,0:T(8,128)(2,1)S(1)} %constant_dynamic-update-slice_fusion.5.rest), channel_id=1, source_target_pairs={{0,1},{1,0},{2,3},{3,2},{4,5},{5,4},{6,7},{7,6},{8,9},{9,8},{10,11... | collective-permute-start | bytes 368648 | tf_op jit(solution)/shard_map/ppermute | solution.py:25
  52.5 9.9 %copy-start.2 = (bf16[2,2048,512]{2,1,0:T(8,128)(2,1)S(1)}, bf16[2,2048,512]{2,1,0:T(8,128)(2,1)}, u32[]{:S(2)}) copy-start(bf16[2,2048,512]{2,1,0:T(8,128)(2,1)} %down_ref.3) | copy-start | bytes 12582916
  53.4 4.5 %collective-permute-start.21 = (bf16[2,40,256]{2,1,0:T(8,128)(2,1)S(1)}, bf16[2,40,256]{2,1,0:T(8,128)(2,1)S(1)}, u32[]{:S(2)}, u32[]{:S(2)}) collective-permute-start(bf16[2,40,256]{2,1,0:T(8,128)(2,1)S(1)} %shard_map.170.own), channel_id=1, source_target_pairs={{0,2},{1,3},{2,0},{3,1},{4,6},{5,7},{6,4},{7,5},{8,10},{9,11},{10,... | collective-permute-start | bytes 122888 | tf_op jit(solution)/shard_map/ppermute | solution.py:32
  54.0 8.8 %collective-permute-start.20 = (bf16[2,40,256]{2,1,0:T(8,128)(2,1)S(1)}, bf16[2,40,256]{2,1,0:T(8,128)(2,1)S(1)}, u32[]{:S(2)}, u32[]{:S(2)}) collective-permute-start(bf16[2,40,256]{2,1,0:T(8,128)(2,1)S(1)} %shard_map.170.own), channel_id=1, source_target_pairs={{0,1},{1,0},{2,3},{3,2},{4,5},{5,4},{6,7},{7,6},{8,9},{9,8},{10,11... | collective-permute-start | bytes 122888 | tf_op jit(solution)/shard_map/ppermute | solution.py:25
  54.0 4.9 %collective-permute-start.22 = (bf16[2,40,256]{2,1,0:T(8,128)(2,1)S(1)}, bf16[2,40,256]{2,1,0:T(8,128)(2,1)S(1)}, u32[]{:S(2)}, u32[]{:S(2)}) collective-permute-start(bf16[2,40,256]{2,1,0:T(8,128)(2,1)S(1)} %shard_map.170.own), channel_id=1, source_target_pairs={{0,4},{1,5},{2,6},{3,7},{4,0},{5,1},{6,2},{7,3},{8,12},{9,13},{10,... | collective-permute-start | bytes 122888 | tf_op jit(solution)/shard_map/ppermute | solution.py:32
  56.6 5.8 %collective-permute-start.23 = (bf16[2,40,256]{2,1,0:T(8,128)(2,1)S(1)}, bf16[2,40,256]{2,1,0:T(8,128)(2,1)S(1)}, u32[]{:S(2)}, u32[]{:S(2)}) collective-permute-start(bf16[2,40,256]{2,1,0:T(8,128)(2,1)S(1)} %shard_map.170.own), channel_id=1, source_target_pairs={{0,6},{1,7},{2,4},{3,5},{4,2},{5,3},{6,0},{7,1},{8,14},{9,15},{10,... | collective-permute-start | bytes 122888 | tf_op jit(solution)/shard_map/ppermute | solution.py:32
  62.4 1.3 %collective-permute-start.24 = (bf16[2,120,256]{2,1,0:T(8,128)(2,1)S(1)}, bf16[2,120,256]{2,1,0:T(8,128)(2,1)S(1)}, u32[]{:S(2)}, u32[]{:S(2)}) collective-permute-start(bf16[2,120,256]{2,1,0:T(8,128)(2,1)S(1)} %constant_dynamic-update-slice_fusion.8.rest), channel_id=1, source_target_pairs={{0,1},{1,0},{2,3},{3,2},{4,5},{5,4},{6,7},{7,6},{8,9},{9,8},{10,11... | collective-permute-start | bytes 368648 | tf_op jit(solution)/shard_map/ppermute | solution.py:25
  64.2 3.8 %collective-permute-start.25 = (bf16[10,512]{1,0:T(8,128)(2,1)S(1)}, bf16[10,512]{1,0:T(8,128)(2,1)S(1)}, u32[]{:S(2)}, u32[]{:S(2)}) collective-permute-start(bf16[10,512]{1,0:T(8,128)(2,1)S(1)} %get-tuple-element.104), channel_id=1, source_target_pairs={{0,8},{8,0},{16,24},{24,16},{1,9},{9,1},{17,25},{25,17},{2,10},{10... | collective-permute-start | bytes 30728 | tf_op jit(solution)/shard_map/ppermute | solution.py:40
  65.1 3.7 %collective-permute-start.26 = (bf16[10,512]{1,0:T(8,128)(2,1)S(1)}, bf16[10,512]{1,0:T(8,128)(2,1)S(1)}, u32[]{:S(2)}, u32[]{:S(2)}) collective-permute-start(bf16[10,512]{1,0:T(8,128)(2,1)S(1)} %get-tuple-element.105), channel_id=1, source_target_pairs={{0,16},{8,24},{16,0},{24,8},{1,17},{9,25},{17,1},{25,9},{2,18},{10... | collective-permute-start | bytes 30728 | tf_op jit(solution)/shard_map/ppermute | solution.py:40
  65.9 4.6 %collective-permute-start.27 = (bf16[10,512]{1,0:T(8,128)(2,1)S(1)}, bf16[10,512]{1,0:T(8,128)(2,1)S(1)}, u32[]{:S(2)}, u32[]{:S(2)}) collective-permute-start(bf16[10,512]{1,0:T(8,128)(2,1)S(1)} %get-tuple-element.106), channel_id=1, source_target_pairs={{0,24},{8,16},{16,8},{24,0},{1,25},{9,17},{17,9},{25,1},{2,26},{10... | collective-permute-start | bytes 30728 | tf_op jit(solution)/shard_map/ppermute | solution.py:40

commit v4 on v3

--- a/solution.py
+++ b/solution.py
@@ -41,9 +41,9 @@
     return found
 
 
-def pieces_of(one, many, levels):
-    rows = one.shape[-2]
-    return [one] + [many.at[..., pl.ds(k * rows, rows), :] for k in range(levels - 1)]
+def parts_of(many, levels):
+    rows = many.shape[-2] // (levels - 1)
+    return [many.at[..., pl.ds(k * rows, rows), :] for k in range(levels - 1)]
 
 
 def call(kernel, outs, operands, microseconds, scratch=()):
@@ -405,17 +405,17 @@
     return total
 
 
-def out_first(levels, own, rest, weight_ref, hidden_ref, total_ref):
-    places = spots(CORES * levels, own.shape[1])[:levels]
+def out_first(levels, own, rest, other, weight_ref, hidden_ref, total_ref):
+    places = spots(CORES * levels, own.shape[1])[: levels + 1]
     total = hidden_ref[...].astype(f32)
-    total_ref[...] = out_sum(pieces_of(own, rest, levels), places, weight_ref, total)
-
-
-def out_last(levels, peers, other, others, weight_ref, total_ref, *refs):
+    total_ref[...] = out_sum([own, *parts_of(rest, levels), other], places, weight_ref, total)
+
+
+def out_last(levels, peers, others, weight_ref, total_ref, *refs):
     placing, shares = refs[:peers], refs[peers : 2 * peers]
     after_ref, outs = refs[2 * peers], refs[2 * peers + 1 :]
-    places = spots(CORES * levels, other.shape[1])[levels:]
-    pieces = pieces_of(other, others, levels)
+    places = spots(CORES * levels, others.shape[1])[levels + 1 :]
+    pieces = parts_of(others, levels)
     after = out_sum(pieces, places, weight_ref, total_ref[...]).astype(bf16)
     after_ref[...] = after
     cut = after.shape[1]
@@ -433,13 +433,13 @@
     (total,) = call(
         functools.partial(out_first, levels),
         [near_shape((rows, width), f32)],
-        (own, rest, weight, hidden),
+        (own, rest, other, weight, hidden),
         1,
     )
     return call(
         functools.partial(out_last, levels, peers),
         [near_shape((rows, width), bf16)] + [near_shape((slots, width + HEAD), bf16)] * peers,
-        (other, others, weight, total, *placing, *shares),
+        (others, weight, total, *placing, *shares),
         2,
     )
 
@@ -458,12 +458,12 @@
     return squares, gates, ups
 
 
-def lift_first(levels, own, rest, gain_ref, gate_ref, up_ref, gates_ref, ups_ref, squares_ref):
+def lift_first(levels, own, rest, other, gain_ref, gate_ref, up_ref, gates_ref, ups_ref, squares_ref):
     experts, rows, width = gates_ref.shape
-    places = spots(CORES * levels, own.shape[1])[:levels]
+    places = spots(CORES * levels, own.shape[1])[: levels + 1]
     zeros = [jnp.zeros((rows, width), f32)] * experts
     squares, gates, ups = lift_sum(
-        pieces_of(own, rest, levels),
+        [own, *parts_of(rest, levels), other],
         places,
         gain_ref,
         gate_ref,
@@ -479,12 +479,12 @@
 
 
 def lift_last(
-    levels, depth, other, others, gain_ref, gate_ref, up_ref, gates_ref, ups_ref, squares_ref, active_ref
+    levels, depth, others, gain_ref, gate_ref, up_ref, gates_ref, ups_ref, squares_ref, active_ref
 ):
     experts = gates_ref.shape[0]
-    places = spots(CORES * levels, other.shape[1])[levels:]
+    places = spots(CORES * levels, others.shape[1])[levels + 1 :]
     squares, gates, ups = lift_sum(
-        pieces_of(other, others, levels),
+        parts_of(others, levels),
         places,
         gain_ref,
         gate_ref,
@@ -507,13 +507,13 @@
     sums = call(
         functools.partial(lift_first, levels),
         [near_shape((experts, rows, width), f32)] * 2 + [near_shape((rows, HEAD), f32)],
-        (own, rest, gain, expert_gate, expert_up),
+        (own, rest, other, gain, expert_gate, expert_up),
         2,
     )
     (active,) = call(
         functools.partial(lift_last, levels, depth),
         [near_shape((experts, rows, width), bf16)],
-        (other, others, gain, expert_gate, expert_up, *sums),
+        (others, gain, expert_gate, expert_up, *sums),
         2,
     )
     return active
@@ -529,21 +529,21 @@
     return totals
 
 
-def lower_first(levels, own, rest, down_ref, totals_ref):
+def lower_first(levels, own, rest, other, down_ref, totals_ref):
     experts = down_ref.shape[0]
-    places = spots(CORES * levels, own.shape[2])[:levels]
-    totals = lower_sum(pieces_of(own, rest, levels), places, down_ref, [None] * experts)
+    places = spots(CORES * levels, own.shape[2])[: levels + 1]
+    totals = lower_sum([own, *parts_of(rest, levels), other], places, down_ref, [None] * experts)
     for expert in range(experts):
         totals_ref[expert] = totals[expert]
 
 
-def lower_last(levels, peers, other, others, down_ref, totals_ref, *refs):
+def lower_last(levels, peers, others, down_ref, totals_ref, *refs):
     tables, outs, mean_ref = refs[:peers], refs[peers : 2 * peers], refs[-1]
     experts, _ = totals_ref.shape[:2]
     slots = tables[0].shape[0]
-    places = spots(CORES * levels, other.shape[2])[levels:]
+    places = spots(CORES * levels, others.shape[2])[levels + 1 :]
     totals = [totals_ref[expert] for expert in range(experts)]
-    totals = lower_sum(pieces_of(other, others, levels), places, down_ref, totals)
+    totals = lower_sum(parts_of(others, levels), places, down_ref, totals)
     for expert in range(experts):
         mean_ref[expert] = totals[expert].astype(bf16).astype(f32)
     cut = tables[0].shape[1] - HEAD
@@ -570,13 +570,13 @@
     (totals,) = call(
         functools.partial(lower_first, levels),
         [near_shape((experts, rows, width), f32)],
-        (own, rest, expert_down),
+        (own, rest, other, expert_down),
         1,
     )
     return call(
         functools.partial(lower_last, levels, peers),
         [near_shape((slots, width), bf16)] * peers,
-        (other, others, expert_down, totals, *tables),
+        (others, expert_down, totals, *tables),
         2,
         [pltpu.VMEM((experts, rows, width), f32)],
     )
@@ -611,9 +611,9 @@
     )(*operands)
 
 
-def shared(lines):
+def shared(piece, lines):
     rest = jnp.concatenate(lines[1:], axis=-2)
-    return [lines[0], rest, swap_cores(lines[0]), swap_cores(rest)]
+    return [piece, rest, swap_cores(piece), swap_cores(rest)]
 
 
 def layer(
@@ -693,17 +693,17 @@
     next_state = update_state(key, value, ret_state, 0, split, None, ())
 
     lines, next_state = lax.optimization_barrier((along_z(mixed), next_state))
-    pieces = shared(lines)
+    pieces = shared(mixed, lines)
     after, *packed = out_project(pieces, out_weight, hidden, placing, shares)
 
     next_state = update_state(key, value, ret_state, split, blocks, next_state, (after,))
     arrived = to_peers(packed)
     arrived, next_state = lax.optimization_barrier((arrived, next_state))
     rows = jnp.concatenate([table[:, :slice_width] for table in arrived], axis=0)
-    pieces = shared(along_z(rows))
+    pieces = shared(rows, along_z(rows))
     active = lift(pieces, ffn_gain.reshape(1, depth), expert_gate, expert_up)
 
-    pieces = shared(along_z(active))
+    pieces = shared(active, along_z(active))
     back = lower(pieces, expert_down, arrived)
     back = to_peers(back)
     return (finish(after, placing, back), next_state)

time: 71.6 us -> 71.1 us (level)
  transfers between devices with their start and end apart: 28 -> 28, of which waited for: 18 -> 17; matrix products, arithmetic and copies ran while one was open for 0% -> 0% of each run, Pallas kernels for 9% -> 9%
where the time goes in v4:
time: 71.1 us; the launch traced here: 70.9 us
  starting transfers between devices  34.6 us (49%)
  waiting for transfers between devices  23.6 us (33%)
  Pallas kernels  10.5 us (15%)
  between operations  1.01 us (1%)
  local copies, waits for them, and re-layouts  0.92 us (1%)
    ppermute x9, starting transfers between devices, along_z(): lax.ppermute(array, 'tp', [(i, i ^ CORES * k) for i in range(size)])  13.3 us
    ppermute x9, starting transfers between devices, to_peers(): lax.ppermute(arrays[k], 'ep', [(i, i ^ k) for i in range(size)])  11.5 us
    ppermute x9, waiting for transfers between devices, along_z(): lax.ppermute(array, 'tp', [(i, i ^ CORES * k) for i in range(size)])  9.58 us
    ppermute x2, starting transfers between devices, layer(): came.append(lax.ppermute(joined, ('ep', 'tp'), route))  9.16 us
    ppermute x9, waiting for transfers between devices, to_peers(): lax.ppermute(arrays[k], 'ep', [(i, i ^ k) for i in range(size)])  8.77 us
    pallas_call x2, Pallas kernels, update_state(): pl.pallas_call(functools.partial(update_kernel, heads, first), grid=(last...  4.26 us
    ppermute x8, waiting for transfers between devices, swap_cores(): return lax.ppermute(array, 'tp', [(i, i ^ 1) for i in range(size)])  3.51 us
    pallas_call x6, Pallas kernels, call(): pl.pallas_call(kernel, out_shape=outs, in_specs=[held()] * len(operands),...  3.38 us
  transfers between devices with their start and end apart: 28, of which 17 were waited for; matrix products, arithmetic and copies ran while one was open for 0% of the time, Pallas kernels for 9%

profile of v4, /device:TPU:0, one launch (start us, length us, event | category | flops | bytes accessed | tf_op | source)
XLA Modules:
  0.0 70.9 jit_solution(5194386513535457534)
XLA Ops:
  0.6 0.6 collective-permute-start
  1.2 0.8 %copy-done.8 = bf16[40,512]{1,0:T(8,128)(2,1)S(1)} copy-done((bf16[40,512]{1,0:T(8,128)(2,1)S(1)}, bf16[40,512]{1,0:T(8,128)(2,1)}, u32[]{:S(2)}) %copy-start.8) | copy-done | bytes 40984
  2.0 0.0 copy-start.12
  2.0 0.0 copy-start.13
  2.0 0.3 collective-permute-done.other_ref
  2.3 3.9 %collective-permute-start.1 = (bf16[40,1024]{1,0:T(8,128)(2,1)S(1)}, bf16[40,1024]{1,0:T(8,128)(2,1)S(1)}, u32[]{:S(2)}, u32[]{:S(2)}) collective-permute-start(bf16[40,1024]{1,0:T(8,128)(2,1)S(1)} %join.1), channel_id=1, source_target_pairs={{0,4},{1,3},{2,12},{3,11},{4,20},{5,19},{6,28},{7,27},{8,6},{9,1},... | collective-permute-start | bytes 245768 | tf_op jit(solution)/shard_map/ppermute | solution.py:672
  6.2 5.2 %collective-permute-start.2 = (bf16[40,1024]{1,0:T(8,128)(2,1)S(1)}, bf16[40,1024]{1,0:T(8,128)(2,1)S(1)}, u32[]{:S(2)}, u32[]{:S(2)}) collective-permute-start(bf16[40,1024]{1,0:T(8,128)(2,1)S(1)} %join.1), channel_id=1, source_target_pairs={{0,6},{1,1},{2,14},{3,9},{4,22},{5,17},{6,30},{7,25},{8,4},{9,3},{... | collective-permute-start | bytes 245768 | tf_op jit(solution)/shard_map/ppermute | solution.py:672
  11.5 0.0 copy-start.4
  11.5 0.0 copy-start.5
  11.5 0.0 copy-start.6
  11.5 0.0 copy-start.7
  11.5 0.0 copy-start.10
  11.5 0.0 slice-start
  11.6 0.3 prepare.1
  11.8 0.2 fusion
  12.0 0.1 pad_maximum_fusion.1
  12.1 1.7 %collective-permute-done.2 = bf16[40,1024]{1,0:T(8,128)(2,1)S(1)} collective-permute-done((bf16[40,1024]{1,0:T(8,128)(2,1)S(1)}, bf16[40,1024]{1,0:T(8,128)(2,1)S(1)}, u32[]{:S(2)}, u32[]{:S(2)}) %collective-permute-start.2) | collective-permute-done | bytes 81952 | tf_op jit(solution)/shard_map/ppermute | solution.py:672
  13.8 0.1 collective-permute-start.3
  13.9 1.4 %collective-permute-done.3.refs_1_ = bf16[80,1024]{1,0:T(8,128)(2,1)S(1)} collective-permute-done((bf16[80,1024]{1,0:T(8,128)(2,1)S(1)}, bf16[80,1024]{1,0:T(8,128)(2,1)S(1)}, u32[]{:S(2)}, u32[]{:S(2)}) %collective-permute-start.3) | collective-permute-done | bytes 163872 | tf_op jit(solution)/shard_map/ppermute | solution.py:25
  15.3 0.0 copy-start.14
  15.3 0.6 project.1
  15.9 2.8 %collective-permute-start.4 = (bf16[40,1152]{1,0:T(8,128)(2,1)S(1)}, bf16[40,1152]{1,0:T(8,128)(2,1)S(1)}, u32[]{:S(2)}, u32[]{:S(2)}) collective-permute-start(bf16[40,1152]{1,0:T(8,128)(2,1)S(1)} %get-tuple-element.71), channel_id=1, source_target_pairs={{0,8},{8,0},{16,24},{24,16},{1,9},{9,1},{17,25},{25,17},{2,10},{10... | collective-permute-start | bytes 276488 | tf_op jit(solution)/shard_map/ppermute | solution.py:40
  18.7 0.9 %collective-permute-start.5 = (bf16[40,1152]{1,0:T(8,128)(2,1)S(1)}, bf16[40,1152]{1,0:T(8,128)(2,1)S(1)}, u32[]{:S(2)}, u32[]{:S(2)}) collective-permute-start(bf16[40,1152]{1,0:T(8,128)(2,1)S(1)} %get-tuple-element.72), channel_id=1, source_target_pairs={{0,16},{8,24},{16,0},{24,8},{1,17},{9,25},{17,1},{25,9},{2,18},{10... | collective-permute-start | bytes 276488 | tf_op jit(solution)/shard_map/ppermute | solution.py:40
  19.7 0.6 collective-permute-start.6
  20.2 1.4 %collective-permute-done.4.refs_4_ = bf16[40,1152]{1,0:T(8,128)(2,1)S(1)} collective-permute-done((bf16[40,1152]{1,0:T(8,128)(2,1)S(1)}, bf16[40,1152]{1,0:T(8,128)(2,1)S(1)}, u32[]{:S(2)}, u32[]{:S(2)}) %collective-permute-start.4) | collective-permute-done | bytes 92192 | tf_op jit(solution)/shard_map/ppermute | solution.py:40
  21.7 3.6 %collective-permute-done.5.refs_5_ = bf16[40,1152]{1,0:T(8,128)(2,1)S(1)} collective-permute-done((bf16[40,1152]{1,0:T(8,128)(2,1)S(1)}, bf16[40,1152]{1,0:T(8,128)(2,1)S(1)}, u32[]{:S(2)}, u32[]{:S(2)}) %collective-permute-start.5) | collective-permute-done | bytes 92192 | tf_op jit(solution)/shard_map/ppermute | solution.py:40
  25.3 1.2 %read_state.1 = (bf16[40,256]{1,0:T(8,128)(2,1)S(1)}, f32[40,256]{1,0:T(8,128)S(1)}, f32[40,256]{1,0:T(8,128)S(1)}) custom-call(f32[40,128]{1,0:T(8,128)S(1)} %get-tuple-element.66.refs_0_, f32[40,128]{1,0:T(8,128)S(1)} %get-tuple-element.67.refs_1_, f32[1,256]{1,0:T(1,128)S(1)} %bitcast.12, f32[40,1152]{1,0:T(8,128)S(1)} %get-tuple-element.70.refs_3_, ...), custom_call_target="tpu_custom_call" | custom-call | flops 5000000000 | bytes 30000000 | tf_op jit(solution)/shard_map/read_state/pallas_call | solution.py:343
  26.4 0.6 collective-permute-start.7
  27.1 1.7 %collective-permute-start.8 = (bf16[40,256]{1,0:T(8,128)(2,1)S(1)}, bf16[40,256]{1,0:T(8,128)(2,1)S(1)}, u32[]{:S(2)}, u32[]{:S(2)}) collective-permute-start(bf16[40,256]{1,0:T(8,128)(2,1)S(1)} %get-tuple-element.74.own), channel_id=1, source_target_pairs={{0,4},{1,5},{2,6},{3,7},{4,0},{5,1},{6,2},{7,3},{8,12},{9,13},{10,... | collective-permute-start | bytes 61448 | tf_op jit(solution)/shard_map/ppermute | solution.py:32
  28.8 2.1 %collective-permute-start.9 = (bf16[40,256]{1,0:T(8,128)(2,1)S(1)}, bf16[40,256]{1,0:T(8,128)(2,1)S(1)}, u32[]{:S(2)}, u32[]{:S(2)}) collective-permute-start(bf16[40,256]{1,0:T(8,128)(2,1)S(1)} %get-tuple-element.74.own), channel_id=1, source_target_pairs={{0,6},{1,7},{2,4},{3,5},{4,2},{5,3},{6,0},{7,1},{8,14},{9,15},{10,... | collective-permute-start | bytes 61448 | tf_op jit(solution)/shard_map/ppermute | solution.py:32
  30.9 1.7 %update_state.2.refs_4_ = f32[40,2,128,128]{3,2,1,0:T(8,128)} custom-call(f32[40,256]{1,0:T(8,128)S(1)} %get-tuple-element.75.refs_0_, f32[40,256]{1,0:T(8,128)S(1)} %get-tuple-element.76.refs_1_, f32[40,2,128,128]{3,2,1,0:T(8,128)S(1)} %bitcast.6), custom_call_target="tpu_custom_call" | custom-call | flops 5000000000 | bytes 30000000 | tf_op jit(solution)/shard_map/update_state/pallas_call | solution.py:387
  32.5 1.8 %collective-permute-done.9 = bf16[40,256]{1,0:T(8,128)(2,1)S(1)} collective-permute-done((bf16[40,256]{1,0:T(8,128)(2,1)S(1)}, bf16[40,256]{1,0:T(8,128)(2,1)S(1)}, u32[]{:S(2)}, u32[]{:S(2)}) %collective-permute-start.9) | collective-permute-done | bytes 20512 | tf_op jit(solution)/shard_map/ppermute | solution.py:32
  34.4 0.1 collective-permute-start.10
  34.5 0.3 shard_map.167.total_ref
  34.8 0.8 %collective-permute-done.10.others = bf16[120,256]{1,0:T(8,128)(2,1)S(1)} collective-permute-done((bf16[120,256]{1,0:T(8,128)(2,1)S(1)}, bf16[120,256]{1,0:T(8,128)(2,1)S(1)}, u32[]{:S(2)}, u32[]{:S(2)}) %collective-permute-start.10) | collective-permute-done | bytes 61472 | tf_op jit(solution)/shard_map/ppermute | solution.py:25
  35.7 0.4 shard_map.168
  36.1 1.6 %collective-permute-start.12 = (bf16[10,640]{1,0:T(8,128)(2,1)S(1)}, bf16[10,640]{1,0:T(8,128)(2,1)S(1)}, u32[]{:S(2)}, u32[]{:S(2)}) collective-permute-start(bf16[10,640]{1,0:T(8,128)(2,1)S(1)} %get-tuple-element.90), channel_id=1, source_target_pairs={{0,8},{8,0},{16,24},{24,16},{1,9},{9,1},{17,25},{25,17},{2,10},{10... | collective-permute-start | bytes 38408 | tf_op jit(solution)/shard_map/ppermute | solution.py:40
  37.7 0.9 %collective-permute-start.13 = (bf16[10,640]{1,0:T(8,128)(2,1)S(1)}, bf16[10,640]{1,0:T(8,128)(2,1)S(1)}, u32[]{:S(2)}, u32[]{:S(2)}) collective-permute-start(bf16[10,640]{1,0:T(8,128)(2,1)S(1)} %get-tuple-element.91), channel_id=1, source_target_pairs={{0,16},{8,24},{16,0},{24,8},{1,17},{9,25},{17,1},{25,9},{2,18},{10... | collective-permute-start | bytes 38408 | tf_op jit(solution)/shard_map/ppermute | solution.py:40
  38.6 1.1 %collective-permute-start.14 = (bf16[10,640]{1,0:T(8,128)(2,1)S(1)}, bf16[10,640]{1,0:T(8,128)(2,1)S(1)}, u32[]{:S(2)}, u32[]{:S(2)}) collective-permute-start(bf16[10,640]{1,0:T(8,128)(2,1)S(1)} %get-tuple-element.92), channel_id=1, source_target_pairs={{0,24},{8,16},{16,8},{24,0},{1,25},{9,17},{17,9},{25,1},{2,26},{10... | collective-permute-start | bytes 38408 | tf_op jit(solution)/shard_map/ppermute | solution.py:40
  39.6 2.6 %update_state.3 = f32[40,2,128,128]{3,2,1,0:T(8,128)} custom-call(f32[40,256]{1,0:T(8,128)S(1)} %get-tuple-element.75.refs_0_, f32[40,256]{1,0:T(8,128)S(1)} %get-tuple-element.76.refs_1_, f32[40,2,128,128]{3,2,1,0:T(8,128)S(1)} %bitcast.6, bf16[40,512]{1,0:T(8,128)(2,1)S(1)} %get-tuple-element.88.refs_3_.refs_0_, ...), custom_call_target="tpu_custom_call", output_to_operand_aliasing={{}: (4, {})} | custom-call | flops 5000000000 | bytes 30000000 | tf_op jit(solution)/shard_map/update_state/pallas_call | solution.py:387
  42.2 1.0 %collective-permute-done.14.refs_3_ = bf16[10,640]{1,0:T(8,128)(2,1)S(1)} collective-permute-done((bf16[10,640]{1,0:T(8,128)(2,1)S(1)}, bf16[10,640]{1,0:T(8,128)(2,1)S(1)}, u32[]{:S(2)}, u32[]{:S(2)}) %collective-permute-start.14) | collective-permute-done | bytes 12832 | tf_op jit(solution)/shard_map/ppermute | solution.py:40
  43.3 0.1 collective-permute-start.15
  43.4 1.8 %collective-permute-start.16 = (bf16[40,512]{1,0:T(8,128)(2,1)S(1)}, bf16[40,512]{1,0:T(8,128)(2,1)S(1)}, u32[]{:S(2)}, u32[]{:S(2)}) collective-permute-start(bf16[40,512]{1,0:T(8,128)(2,1)S(1)} %pad_maximum_fusion.own), channel_id=1, source_target_pairs={{0,4},{1,5},{2,6},{3,7},{4,0},{5,1},{6,2},{7,3},{8,12},{9,13},{10,... | collective-permute-start | bytes 122888 | tf_op jit(solution)/shard_map/ppermute | solution.py:32
  45.2 2.6 %collective-permute-start.17 = (bf16[40,512]{1,0:T(8,128)(2,1)S(1)}, bf16[40,512]{1,0:T(8,128)(2,1)S(1)}, u32[]{:S(2)}, u32[]{:S(2)}) collective-permute-start(bf16[40,512]{1,0:T(8,128)(2,1)S(1)} %pad_maximum_fusion.own), channel_id=1, source_target_pairs={{0,6},{1,7},{2,4},{3,5},{4,2},{5,3},{6,0},{7,1},{8,14},{9,15},{10,... | collective-permute-start | bytes 122888 | tf_op jit(solution)/shard_map/ppermute | solution.py:32
  47.8 1.0 %collective-permute-done.16 = bf16[40,512]{1,0:T(8,128)(2,1)S(1)} collective-permute-done((bf16[40,512]{1,0:T(8,128)(2,1)S(1)}, bf16[40,512]{1,0:T(8,128)(2,1)S(1)}, u32[]{:S(2)}, u32[]{:S(2)}) %collective-permute-start.16) | collective-permute-done | bytes 40992 | tf_op jit(solution)/shard_map/ppermute | solution.py:32
  48.8 2.2 %collective-permute-done.17 = bf16[40,512]{1,0:T(8,128)(2,1)S(1)} collective-permute-done((bf16[40,512]{1,0:T(8,128)(2,1)S(1)}, bf16[40,512]{1,0:T(8,128)(2,1)S(1)}, u32[]{:S(2)}, u32[]{:S(2)}) %collective-permute-start.17) | collective-permute-done | bytes 40992 | tf_op jit(solution)/shard_map/ppermute | solution.py:32
  51.0 1.0 %shard_map.169 = (f32[2,40,256]{2,1,0:T(8,128)S(1)}, f32[2,40,256]{2,1,0:T(8,128)S(1)}, f32[40,128]{1,0:T(8,128)S(1)}) custom-call(bf16[40,512]{1,0:T(8,128)(2,1)S(1)} %pad_maximum_fusion.own, bf16[120,512]{1,0:T(8,128)(2,1)S(1)} %constant_dynamic-update-slice_fusion.5.rest, bf16[40,512]{1,0:T(8,128)(2,1)S(1)} %collective-permute-done.19.other, ...), custom_call_target="tpu_custom_call" | custom-call | flops 5000000000 | bytes 30000000 | tf_op jit(solution)/shard_map/pallas_call | solution.py:51
  52.1 0.3 collective-permute-done.18.others
  52.3 0.7 shard_map.170.own
  53.0 0.1 collective-permute-start.20
  53.1 3.1 %collective-permute-start.21 = (bf16[2,40,256]{2,1,0:T(8,128)(2,1)S(1)}, bf16[2,40,256]{2,1,0:T(8,128)(2,1)S(1)}, u32[]{:S(2)}, u32[]{:S(2)}) collective-permute-start(bf16[2,40,256]{2,1,0:T(8,128)(2,1)S(1)} %shard_map.170.own), channel_id=1, source_target_pairs={{0,4},{1,5},{2,6},{3,7},{4,0},{5,1},{6,2},{7,3},{8,12},{9,13},{10,... | collective-permute-start | bytes 122888 | tf_op jit(solution)/shard_map/ppermute | solution.py:32
  56.2 1.2 %collective-permute-start.22 = (bf16[2,40,256]{2,1,0:T(8,128)(2,1)S(1)}, bf16[2,40,256]{2,1,0:T(8,128)(2,1)S(1)}, u32[]{:S(2)}, u32[]{:S(2)}) collective-permute-start(bf16[2,40,256]{2,1,0:T(8,128)(2,1)S(1)} %shard_map.170.own), channel_id=1, source_target_pairs={{0,6},{1,7},{2,4},{3,5},{4,2},{5,3},{6,0},{7,1},{8,14},{9,15},{10,... | collective-permute-start | bytes 122888 | tf_op jit(solution)/shard_map/ppermute | solution.py:32
  57.5 1.2 %collective-permute-done.21 = bf16[2,40,256]{2,1,0:T(8,128)(2,1)S(1)} collective-permute-done((bf16[2,40,256]{2,1,0:T(8,128)(2,1)S(1)}, bf16[2,40,256]{2,1,0:T(8,128)(2,1)S(1)}, u32[]{:S(2)}, u32[]{:S(2)}) %collective-permute-start.21) | collective-permute-done | bytes 40992 | tf_op jit(solution)/shard_map/ppermute | solution.py:32
  58.7 3.3 %collective-permute-done.22 = bf16[2,40,256]{2,1,0:T(8,128)(2,1)S(1)} collective-permute-done((bf16[2,40,256]{2,1,0:T(8,128)(2,1)S(1)}, bf16[2,40,256]{2,1,0:T(8,128)(2,1)S(1)}, u32[]{:S(2)}, u32[]{:S(2)}) %collective-permute-start.22) | collective-permute-done | bytes 40992 | tf_op jit(solution)/shard_map/ppermute | solution.py:32
  62.0 0.6 shard_map.171.totals_ref
  62.6 0.8 %collective-permute-done.23.others = bf16[2,120,256]{2,1,0:T(8,128)(2,1)S(1)} collective-permute-done((bf16[2,120,256]{2,1,0:T(8,128)(2,1)S(1)}, bf16[2,120,256]{2,1,0:T(8,128)(2,1)S(1)}, u32[]{:S(2)}, u32[]{:S(2)}) %collective-permute-start.23) | collective-permute-done | bytes 122912 | tf_op jit(solution)/shard_map/ppermute | solution.py:25
  63.3 0.4 shard_map.172
  63.7 0.9 %collective-permute-start.25 = (bf16[10,512]{1,0:T(8,128)(2,1)S(1)}, bf16[10,512]{1,0:T(8,128)(2,1)S(1)}, u32[]{:S(2)}, u32[]{:S(2)}) collective-permute-start(bf16[10,512]{1,0:T(8,128)(2,1)S(1)} %get-tuple-element.102), channel_id=1, source_target_pairs={{0,8},{8,0},{16,24},{24,16},{1,9},{9,1},{17,25},{25,17},{2,10},{10... | collective-permute-start | bytes 30728 | tf_op jit(solution)/shard_map/ppermute | solution.py:40
  64.7 0.8 %collective-permute-start.26 = (bf16[10,512]{1,0:T(8,128)(2,1)S(1)}, bf16[10,512]{1,0:T(8,128)(2,1)S(1)}, u32[]{:S(2)}, u32[]{:S(2)}) collective-permute-start(bf16[10,512]{1,0:T(8,128)(2,1)S(1)} %get-tuple-element.103), channel_id=1, source_target_pairs={{0,16},{8,24},{16,0},{24,8},{1,17},{9,25},{17,1},{25,9},{2,18},{10... | collective-permute-start | bytes 30728 | tf_op jit(solution)/shard_map/ppermute | solution.py:40
  65.4 1.9 %collective-permute-start.27 = (bf16[10,512]{1,0:T(8,128)(2,1)S(1)}, bf16[10,512]{1,0:T(8,128)(2,1)S(1)}, u32[]{:S(2)}, u32[]{:S(2)}) collective-permute-start(bf16[10,512]{1,0:T(8,128)(2,1)S(1)} %get-tuple-element.104), channel_id=1, source_target_pairs={{0,24},{8,16},{16,8},{24,0},{1,25},{9,17},{17,9},{25,1},{2,26},{10... | collective-permute-start | bytes 30728 | tf_op jit(solution)/shard_map/ppermute | solution.py:40
  67.3 0.2 collective-permute-done.25.refs_6_
  67.6 0.8 %collective-permute-done.26.refs_7_ = bf16[10,512]{1,0:T(8,128)(2,1)S(1)} collective-permute-done((bf16[10,512]{1,0:T(8,128)(2,1)S(1)}, bf16[10,512]{1,0:T(8,128)(2,1)S(1)}, u32[]{:S(2)}, u32[]{:S(2)}) %collective-permute-start.26) | collective-permute-done | bytes 10272 | tf_op jit(solution)/shard_map/ppermute | solution.py:40
  68.4 1.7 %collective-permute-done.27.refs_8_ = bf16[10,512]{1,0:T(8,128)(2,1)S(1)} collective-permute-done((bf16[10,512]{1,0:T(8,128)(2,1)S(1)}, bf16[10,512]{1,0:T(8,128)(2,1)S(1)}, u32[]{:S(2)}, u32[]{:S(2)}) %collective-permute-start.27) | collective-permute-done | bytes 10272 | tf_op jit(solution)/shard_map/ppermute | solution.py:40
  70.1 0.9 %finish.1 = bf16[40,512]{1,0:T(8,128)(2,1)} custom-call(bf16[40,512]{1,0:T(8,128)(2,1)S(1)} %get-tuple-element.88.refs_3_.refs_0_, bf16[10,40]{1,0:T(8,128)(2,1)S(1)} %get-tuple-element.80.refs_0_.refs_1_, bf16[10,40]{1,0:T(8,128)(2,1)S(1)} %get-tuple-element.81.refs_1_.refs_2_, bf16[10,40]{1,0:T(8,128)(2,1)S(1)} %get-tuple-element.82.refs_2_.refs_3_, ...), custom_call_target="tpu_custom_call" | custom-call | flops 2500000000 | bytes 15000000 | tf_op jit(solution)/shard_map/finish/pallas_call | solution.py:603
  (63 shorter events, 0.2 us)
Async XLA Ops:
  0.6 1.6 %collective-permute-start = (bf16[40,512]{1,0:T(8,128)(2,1)}, bf16[40,512]{1,0:T(8,128)(2,1)S(1)}, u32[]{:S(2)}, u32[]{:S(2)}) collective-permute-start(bf16[40,512]{1,0:T(8,128)(2,1)} %hidden_ref.1), channel_id=1, source_target_pairs={{0,1},{1,0},{2,3},{3,2},{4,5},{5,4},{6,7},{7,6},{8,9},{9,8},{10,11... | collective-permute-start | bytes 122888 | tf_op jit(solution)/shard_map/ppermute | solution.py:25
  1.2 0.8 %copy-start.8 = (bf16[40,512]{1,0:T(8,128)(2,1)S(1)}, bf16[40,512]{1,0:T(8,128)(2,1)}, u32[]{:S(2)}) copy-start(bf16[40,512]{1,0:T(8,128)(2,1)} %hidden_ref.1) | copy-start | bytes 122884
  2.0 9.5 %copy-start.15 = (s32[40]{0:T(128)S(1)}, s32[40]{0:T(128)}, u32[]{:S(2)}) copy-start(s32[40]{0:T(128)} %param.17) | copy-start | bytes 484
  2.0 9.5 %copy-start.12 = (s32[40,2]{0,1:T(2,128)S(1)}, s32[40,2]{0,1:T(2,128)}, u32[]{:S(2)}) copy-start(s32[40,2]{0,1:T(2,128)} %param.30) | copy-start | bytes 964
  2.0 9.5 %copy-start.13 = (f32[40,2]{0,1:T(2,128)S(1)}, f32[40,2]{0,1:T(2,128)}, u32[]{:S(2)}) copy-start(f32[40,2]{0,1:T(2,128)} %param.31) | copy-start | bytes 964
  2.3 9.8 %collective-permute-start.1 = (bf16[40,1024]{1,0:T(8,128)(2,1)S(1)}, bf16[40,1024]{1,0:T(8,128)(2,1)S(1)}, u32[]{:S(2)}, u32[]{:S(2)}) collective-permute-start(bf16[40,1024]{1,0:T(8,128)(2,1)S(1)} %join.1), channel_id=1, source_target_pairs={{0,4},{1,3},{2,12},{3,11},{4,20},{5,19},{6,28},{7,27},{8,6},{9,1},... | collective-permute-start | bytes 245768 | tf_op jit(solution)/shard_map/ppermute | solution.py:672
  6.2 7.6 %collective-permute-start.2 = (bf16[40,1024]{1,0:T(8,128)(2,1)S(1)}, bf16[40,1024]{1,0:T(8,128)(2,1)S(1)}, u32[]{:S(2)}, u32[]{:S(2)}) collective-permute-start(bf16[40,1024]{1,0:T(8,128)(2,1)S(1)} %join.1), channel_id=1, source_target_pairs={{0,6},{1,1},{2,14},{3,9},{4,22},{5,17},{6,30},{7,25},{8,4},{9,3},{... | collective-permute-start | bytes 245768 | tf_op jit(solution)/shard_map/ppermute | solution.py:672
  11.5 3.8 %copy-start.4 = (bf16[1024,256]{1,0:T(8,128)(2,1)S(1)}, bf16[1024,256]{1,0:T(8,128)(2,1)}, u32[]{:S(2)}) copy-start(bf16[1024,256]{1,0:T(8,128)(2,1)} %refs_2_.3) | copy-start | bytes 1572868
  11.5 3.8 %copy-start.5 = (bf16[1024,256]{1,0:T(8,128)(2,1)S(1)}, bf16[1024,256]{1,0:T(8,128)(2,1)}, u32[]{:S(2)}) copy-start(bf16[1024,256]{1,0:T(8,128)(2,1)} %refs_3_.1) | copy-start | bytes 1572868
  11.5 3.8 %copy-start.6 = (bf16[1024,256]{1,0:T(8,128)(2,1)S(1)}, bf16[1024,256]{1,0:T(8,128)(2,1)}, u32[]{:S(2)}) copy-start(bf16[1024,256]{1,0:T(8,128)(2,1)} %refs_4_.1) | copy-start | bytes 1572868
  11.5 3.8 %copy-start.7 = (bf16[1024,256]{1,0:T(8,128)(2,1)S(1)}, bf16[1024,256]{1,0:T(8,128)(2,1)}, u32[]{:S(2)}) copy-start(bf16[1024,256]{1,0:T(8,128)(2,1)} %refs_5_.1) | copy-start | bytes 1572868
  11.5 3.8 %copy-start.10 = (f32[4096]{0:T(1024)S(1)}, f32[4096]{0:T(1024)}, u32[]{:S(2)}) copy-start(f32[4096]{0:T(1024)} %param.25) | copy-start | bytes 49156
  11.5 13.7 %slice-start = ((s8[5242880]{0:T(1024)(128)(4,1)}), s8[4194304]{0:T(1024)(128)(4,1)S(1)}, s32[]{:S(2)}) async-start(s8[5242880]{0:T(1024)(128)(4,1)} %bitcast.5), calls=%async_computation | async-start | bytes 8388608
  13.8 11.5 %slice-start.1 = ((s8[5242880]{0:T(1024)(128)(4,1)}), s8[1048576]{0:T(1024)(128)(4,1)S(1)}, s32[]{:S(2)}) async-start(s8[5242880]{0:T(1024)(128)(4,1)} %bitcast.5), calls=%async_computation.1 | async-start | bytes 2097152
  13.8 1.5 %collective-permute-start.3 = (bf16[80,1024]{1,0:T(8,128)(2,1)S(1)}, bf16[80,1024]{1,0:T(8,128)(2,1)S(1)}, u32[]{:S(2)}, u32[]{:S(2)}) collective-permute-start(bf16[80,1024]{1,0:T(8,128)(2,1)S(1)} %constant_dynamic-update-slice_fusion.refs_0_), channel_id=1, source_target_pairs={{0,1},{1,0},{2,3},{3,2},{4,5},{5,4},{6,7},{7,6},{8,9},{9,8},{10,11... | collective-permute-start | bytes 491528 | tf_op jit(solution)/shard_map/ppermute | solution.py:25
  15.3 9.9 %copy-start.14 = (f32[256]{0:T(256)S(1)}, f32[256]{0:T(256)}, u32[]{:S(2)}) copy-start(f32[256]{0:T(256)} %param.23) | copy-start | bytes 3076
  15.9 5.8 %collective-permute-start.4 = (bf16[40,1152]{1,0:T(8,128)(2,1)S(1)}, bf16[40,1152]{1,0:T(8,128)(2,1)S(1)}, u32[]{:S(2)}, u32[]{:S(2)}) collective-permute-start(bf16[40,1152]{1,0:T(8,128)(2,1)S(1)} %get-tuple-element.71), channel_id=1, source_target_pairs={{0,8},{8,0},{16,24},{24,16},{1,9},{9,1},{17,25},{25,17},{2,10},{10... | collective-permute-start | bytes 276488 | tf_op jit(solution)/shard_map/ppermute | solution.py:40
  18.7 6.5 %collective-permute-start.5 = (bf16[40,1152]{1,0:T(8,128)(2,1)S(1)}, bf16[40,1152]{1,0:T(8,128)(2,1)S(1)}, u32[]{:S(2)}, u32[]{:S(2)}) collective-permute-start(bf16[40,1152]{1,0:T(8,128)(2,1)S(1)} %get-tuple-element.72), channel_id=1, source_target_pairs={{0,16},{8,24},{16,0},{24,8},{1,17},{9,25},{17,1},{25,9},{2,18},{10... | collective-permute-start | bytes 276488 | tf_op jit(solution)/shard_map/ppermute | solution.py:40
  19.7 5.6 %collective-permute-start.6 = (bf16[40,1152]{1,0:T(8,128)(2,1)S(1)}, bf16[40,1152]{1,0:T(8,128)(2,1)S(1)}, u32[]{:S(2)}, u32[]{:S(2)}) collective-permute-start(bf16[40,1152]{1,0:T(8,128)(2,1)S(1)} %get-tuple-element.73), channel_id=1, source_target_pairs={{0,24},{8,16},{16,8},{24,0},{1,25},{9,17},{17,9},{25,1},{2,26},{10... | collective-permute-start | bytes 276488 | tf_op jit(solution)/shard_map/ppermute | solution.py:40
  26.4 6.1 %collective-permute-start.7 = (bf16[40,256]{1,0:T(8,128)(2,1)S(1)}, bf16[40,256]{1,0:T(8,128)(2,1)S(1)}, u32[]{:S(2)}, u32[]{:S(2)}) collective-permute-start(bf16[40,256]{1,0:T(8,128)(2,1)S(1)} %get-tuple-element.74.own), channel_id=1, source_target_pairs={{0,2},{1,3},{2,0},{3,1},{4,6},{5,7},{6,4},{7,5},{8,10},{9,11},{10,... | collective-permute-start | bytes 61448 | tf_op jit(solution)/shard_map/ppermute | solution.py:32
  27.1 5.5 %collective-permute-start.8 = (bf16[40,256]{1,0:T(8,128)(2,1)S(1)}, bf16[40,256]{1,0:T(8,128)(2,1)S(1)}, u32[]{:S(2)}, u32[]{:S(2)}) collective-permute-start(bf16[40,256]{1,0:T(8,128)(2,1)S(1)} %get-tuple-element.74.own), channel_id=1, source_target_pairs={{0,4},{1,5},{2,6},{3,7},{4,0},{5,1},{6,2},{7,3},{8,12},{9,13},{10,... | collective-permute-start | bytes 61448 | tf_op jit(solution)/shard_map/ppermute | solution.py:32
  28.8 5.6 %collective-permute-start.9 = (bf16[40,256]{1,0:T(8,128)(2,1)S(1)}, bf16[40,256]{1,0:T(8,128)(2,1)S(1)}, u32[]{:S(2)}, u32[]{:S(2)}) collective-permute-start(bf16[40,256]{1,0:T(8,128)(2,1)S(1)} %get-tuple-element.74.own), channel_id=1, source_target_pairs={{0,6},{1,7},{2,4},{3,5},{4,2},{5,3},{6,0},{7,1},{8,14},{9,15},{10,... | collective-permute-start | bytes 61448 | tf_op jit(solution)/shard_map/ppermute | solution.py:32
  30.8 3.6 %collective-permute-start.11 = (bf16[40,256]{1,0:T(8,128)(2,1)S(1)}, bf16[40,256]{1,0:T(8,128)(2,1)S(1)}, u32[]{:S(2)}, u32[]{:S(2)}) collective-permute-start(bf16[40,256]{1,0:T(8,128)(2,1)S(1)} %get-tuple-element.74.own), channel_id=1, source_target_pairs={{0,1},{1,0},{2,3},{3,2},{4,5},{5,4},{6,7},{7,6},{8,9},{9,8},{10,11... | collective-permute-start | bytes 61448 | tf_op jit(solution)/shard_map/ppermute | solution.py:25
  30.8 3.6 %copy-start.3 = (bf16[2048,512]{1,0:T(8,128)(2,1)S(1)}, bf16[2048,512]{1,0:T(8,128)(2,1)}, u32[]{:S(2)}) copy-start(bf16[2048,512]{1,0:T(8,128)(2,1)} %weight_ref.3) | copy-start | bytes 6291460
  30.9 3.6 %copy-start.9 = (bf16[40,512]{1,0:T(8,128)(2,1)S(1)}, bf16[40,512]{1,0:T(8,128)(2,1)}, u32[]{:S(2)}) copy-start(bf16[40,512]{1,0:T(8,128)(2,1)} %hidden_ref.1) | copy-start | bytes 122884
  34.4 1.3 %collective-permute-start.10 = (bf16[120,256]{1,0:T(8,128)(2,1)S(1)}, bf16[120,256]{1,0:T(8,128)(2,1)S(1)}, u32[]{:S(2)}, u32[]{:S(2)}) collective-permute-start(bf16[120,256]{1,0:T(8,128)(2,1)S(1)} %constant_dynamic-update-slice_fusion.2.rest), channel_id=1, source_target_pairs={{0,1},{1,0},{2,3},{3,2},{4,5},{5,4},{6,7},{7,6},{8,9},{9,8},{10,11... | collective-permute-start | bytes 184328 | tf_op jit(solution)/shard_map/ppermute | solution.py:25
  36.1 6.2 %collective-permute-start.12 = (bf16[10,640]{1,0:T(8,128)(2,1)S(1)}, bf16[10,640]{1,0:T(8,128)(2,1)S(1)}, u32[]{:S(2)}, u32[]{:S(2)}) collective-permute-start(bf16[10,640]{1,0:T(8,128)(2,1)S(1)} %get-tuple-element.90), channel_id=1, source_target_pairs={{0,8},{8,0},{16,24},{24,16},{1,9},{9,1},{17,25},{25,17},{2,10},{10... | collective-permute-start | bytes 38408 | tf_op jit(solution)/shard_map/ppermute | solution.py:40
  37.7 4.6 %collective-permute-start.13 = (bf16[10,640]{1,0:T(8,128)(2,1)S(1)}, bf16[10,640]{1,0:T(8,128)(2,1)S(1)}, u32[]{:S(2)}, u32[]{:S(2)}) collective-permute-start(bf16[10,640]{1,0:T(8,128)(2,1)S(1)} %get-tuple-element.91), channel_id=1, source_target_pairs={{0,16},{8,24},{16,0},{24,8},{1,17},{9,25},{17,1},{25,9},{2,18},{10... | collective-permute-start | bytes 38408 | tf_op jit(solution)/shard_map/ppermute | solution.py:40
  38.6 4.7 %collective-permute-start.14 = (bf16[10,640]{1,0:T(8,128)(2,1)S(1)}, bf16[10,640]{1,0:T(8,128)(2,1)S(1)}, u32[]{:S(2)}, u32[]{:S(2)}) collective-permute-start(bf16[10,640]{1,0:T(8,128)(2,1)S(1)} %get-tuple-element.92), channel_id=1, source_target_pairs={{0,24},{8,16},{16,8},{24,0},{1,25},{9,17},{17,9},{25,1},{2,26},{10... | collective-permute-start | bytes 38408 | tf_op jit(solution)/shard_map/ppermute | solution.py:40
  39.6 11.4 %copy-start = (bf16[2,4096,256]{2,1,0:T(8,128)(2,1)S(1)}, bf16[2,4096,256]{2,1,0:T(8,128)(2,1)}, u32[]{:S(2)}) copy-start(bf16[2,4096,256]{2,1,0:T(8,128)(2,1)} %gate_ref.3) | copy-start | bytes 12582916
  39.6 11.4 %copy-start.1 = (bf16[2,4096,256]{2,1,0:T(8,128)(2,1)S(1)}, bf16[2,4096,256]{2,1,0:T(8,128)(2,1)}, u32[]{:S(2)}) copy-start(bf16[2,4096,256]{2,1,0:T(8,128)(2,1)} %up_ref.3) | copy-start | bytes 12582916
  39.6 11.4 %copy-start.11 = (f32[4096]{0:T(1024)S(1)}, f32[4096]{0:T(1024)}, u32[]{:S(2)}) copy-start(f32[4096]{0:T(1024)} %param.26) | copy-start | bytes 49156
  43.3 4.5 %collective-permute-start.15 = (bf16[40,512]{1,0:T(8,128)(2,1)S(1)}, bf16[40,512]{1,0:T(8,128)(2,1)S(1)}, u32[]{:S(2)}, u32[]{:S(2)}) collective-permute-start(bf16[40,512]{1,0:T(8,128)(2,1)S(1)} %pad_maximum_fusion.own), channel_id=1, source_target_pairs={{0,2},{1,3},{2,0},{3,1},{4,6},{5,7},{6,4},{7,5},{8,10},{9,11},{10,... | collective-permute-start | bytes 122888 | tf_op jit(solution)/shard_map/ppermute | solution.py:32
  43.4 5.4 %collective-permute-start.16 = (bf16[40,512]{1,0:T(8,128)(2,1)S(1)}, bf16[40,512]{1,0:T(8,128)(2,1)S(1)}, u32[]{:S(2)}, u32[]{:S(2)}) collective-permute-start(bf16[40,512]{1,0:T(8,128)(2,1)S(1)} %pad_maximum_fusion.own), channel_id=1, source_target_pairs={{0,4},{1,5},{2,6},{3,7},{4,0},{5,1},{6,2},{7,3},{8,12},{9,13},{10,... | collective-permute-start | bytes 122888 | tf_op jit(solution)/shard_map/ppermute | solution.py:32
  45.2 5.8 %collective-permute-start.17 = (bf16[40,512]{1,0:T(8,128)(2,1)S(1)}, bf16[40,512]{1,0:T(8,128)(2,1)S(1)}, u32[]{:S(2)}, u32[]{:S(2)}) collective-permute-start(bf16[40,512]{1,0:T(8,128)(2,1)S(1)} %pad_maximum_fusion.own), channel_id=1, source_target_pairs={{0,6},{1,7},{2,4},{3,5},{4,2},{5,3},{6,0},{7,1},{8,14},{9,15},{10,... | collective-permute-start | bytes 122888 | tf_op jit(solution)/shard_map/ppermute | solution.py:32
  47.7 3.2 %collective-permute-start.19 = (bf16[40,512]{1,0:T(8,128)(2,1)S(1)}, bf16[40,512]{1,0:T(8,128)(2,1)S(1)}, u32[]{:S(2)}, u32[]{:S(2)}) collective-permute-start(bf16[40,512]{1,0:T(8,128)(2,1)S(1)} %pad_maximum_fusion.own), channel_id=1, source_target_pairs={{0,1},{1,0},{2,3},{3,2},{4,5},{5,4},{6,7},{7,6},{8,9},{9,8},{10,11... | collective-permute-start | bytes 122888 | tf_op jit(solution)/shard_map/ppermute | solution.py:25
  51.0 1.3 %collective-permute-start.18 = (bf16[120,512]{1,0:T(8,128)(2,1)S(1)}, bf16[120,512]{1,0:T(8,128)(2,1)S(1)}, u32[]{:S(2)}, u32[]{:S(2)}) collective-permute-start(bf16[120,512]{1,0:T(8,128)(2,1)S(1)} %constant_dynamic-update-slice_fusion.5.rest), channel_id=1, source_target_pairs={{0,1},{1,0},{2,3},{3,2},{4,5},{5,4},{6,7},{7,6},{8,9},{9,8},{10,11... | collective-permute-start | bytes 368648 | tf_op jit(solution)/shard_map/ppermute | solution.py:25
  52.3 9.7 %copy-start.2 = (bf16[2,2048,512]{2,1,0:T(8,128)(2,1)S(1)}, bf16[2,2048,512]{2,1,0:T(8,128)(2,1)}, u32[]{:S(2)}) copy-start(bf16[2,2048,512]{2,1,0:T(8,128)(2,1)} %down_ref.3) | copy-start | bytes 12582916
  53.0 4.5 %collective-permute-start.20 = (bf16[2,40,256]{2,1,0:T(8,128)(2,1)S(1)}, bf16[2,40,256]{2,1,0:T(8,128)(2,1)S(1)}, u32[]{:S(2)}, u32[]{:S(2)}) collective-permute-start(bf16[2,40,256]{2,1,0:T(8,128)(2,1)S(1)} %shard_map.170.own), channel_id=1, source_target_pairs={{0,2},{1,3},{2,0},{3,1},{4,6},{5,7},{6,4},{7,5},{8,10},{9,11},{10,... | collective-permute-start | bytes 122888 | tf_op jit(solution)/shard_map/ppermute | solution.py:32
  53.1 5.6 %collective-permute-start.21 = (bf16[2,40,256]{2,1,0:T(8,128)(2,1)S(1)}, bf16[2,40,256]{2,1,0:T(8,128)(2,1)S(1)}, u32[]{:S(2)}, u32[]{:S(2)}) collective-permute-start(bf16[2,40,256]{2,1,0:T(8,128)(2,1)S(1)} %shard_map.170.own), channel_id=1, source_target_pairs={{0,4},{1,5},{2,6},{3,7},{4,0},{5,1},{6,2},{7,3},{8,12},{9,13},{10,... | collective-permute-start | bytes 122888 | tf_op jit(solution)/shard_map/ppermute | solution.py:32
  56.2 5.8 %collective-permute-start.22 = (bf16[2,40,256]{2,1,0:T(8,128)(2,1)S(1)}, bf16[2,40,256]{2,1,0:T(8,128)(2,1)S(1)}, u32[]{:S(2)}, u32[]{:S(2)}) collective-permute-start(bf16[2,40,256]{2,1,0:T(8,128)(2,1)S(1)} %shard_map.170.own), channel_id=1, source_target_pairs={{0,6},{1,7},{2,4},{3,5},{4,2},{5,3},{6,0},{7,1},{8,14},{9,15},{10,... | collective-permute-start | bytes 122888 | tf_op jit(solution)/shard_map/ppermute | solution.py:32
  57.4 4.6 %collective-permute-start.24 = (bf16[2,40,256]{2,1,0:T(8,128)(2,1)S(1)}, bf16[2,40,256]{2,1,0:T(8,128)(2,1)S(1)}, u32[]{:S(2)}, u32[]{:S(2)}) collective-permute-start(bf16[2,40,256]{2,1,0:T(8,128)(2,1)S(1)} %shard_map.170.own), channel_id=1, source_target_pairs={{0,1},{1,0},{2,3},{3,2},{4,5},{5,4},{6,7},{7,6},{8,9},{9,8},{10,11... | collective-permute-start | bytes 122888 | tf_op jit(solution)/shard_map/ppermute | solution.py:25
  62.0 1.3 %collective-permute-start.23 = (bf16[2,120,256]{2,1,0:T(8,128)(2,1)S(1)}, bf16[2,120,256]{2,1,0:T(8,128)(2,1)S(1)}, u32[]{:S(2)}, u32[]{:S(2)}) collective-permute-start(bf16[2,120,256]{2,1,0:T(8,128)(2,1)S(1)} %constant_dynamic-update-slice_fusion.8.rest), channel_id=1, source_target_pairs={{0,1},{1,0},{2,3},{3,2},{4,5},{5,4},{6,7},{7,6},{8,9},{9,8},{10,11... | collective-permute-start | bytes 368648 | tf_op jit(solution)/shard_map/ppermute | solution.py:25
  63.7 3.8 %collective-permute-start.25 = (bf16[10,512]{1,0:T(8,128)(2,1)S(1)}, bf16[10,512]{1,0:T(8,128)(2,1)S(1)}, u32[]{:S(2)}, u32[]{:S(2)}) collective-permute-start(bf16[10,512]{1,0:T(8,128)(2,1)S(1)} %get-tuple-element.102), channel_id=1, source_target_pairs={{0,8},{8,0},{16,24},{24,16},{1,9},{9,1},{17,25},{25,17},{2,10},{10... | collective-permute-start | bytes 30728 | tf_op jit(solution)/shard_map/ppermute | solution.py:40
  64.7 3.7 %collective-permute-start.26 = (bf16[10,512]{1,0:T(8,128)(2,1)S(1)}, bf16[10,512]{1,0:T(8,128)(2,1)S(1)}, u32[]{:S(2)}, u32[]{:S(2)}) collective-permute-start(bf16[10,512]{1,0:T(8,128)(2,1)S(1)} %get-tuple-element.103), channel_id=1, source_target_pairs={{0,16},{8,24},{16,0},{24,8},{1,17},{9,25},{17,1},{25,9},{2,18},{10... | collective-permute-start | bytes 30728 | tf_op jit(solution)/shard_map/ppermute | solution.py:40
  65.4 4.6 %collective-permute-start.27 = (bf16[10,512]{1,0:T(8,128)(2,1)S(1)}, bf16[10,512]{1,0:T(8,128)(2,1)S(1)}, u32[]{:S(2)}, u32[]{:S(2)}) collective-permute-start(bf16[10,512]{1,0:T(8,128)(2,1)S(1)} %get-tuple-element.104), channel_id=1, source_target_pairs={{0,24},{8,16},{16,8},{24,0},{1,25},{9,17},{17,9},{25,1},{2,26},{10... | collective-permute-start | bytes 30728 | tf_op jit(solution)/shard_map/ppermute | solution.py:40
